TPU v7x, 32 devices: a whole 2x2x4 slice. The times are simulated.
32 devices in a mesh: ep: 8 (over z, y), tp: 4 (over x, core).
Axes of the slice: x: 2, y: 2, z: 4, core: 2. Of those that a mesh axis runs over, the one named last changes fastest.
Arguments:
- tokens: bfloat16 [256, 2048], P('ep'), may hold values from -6 to 6
- gain_mix: bfloat16 [2048], replicated, may hold values from 0.099609375 to 1.8984375
- gain_ffn: bfloat16 [2048], replicated, may hold values from 0.099609375 to 1.8984375
- w_query: bfloat16 [2048, 1024], P('ep', 'tp'), may hold values from -0.125 to 0.125
- w_key: bfloat16 [2048, 1024], P('ep', 'tp'), may hold values from -0.125 to 0.125
- w_value: bfloat16 [2048, 1024], P('ep', 'tp'), may hold values from -0.125 to 0.125
- w_outgate: bfloat16 [2048, 1024], P('ep', 'tp'), may hold values from -0.125 to 0.125
- w_ingate: bfloat16 [2048, 8], replicated, may hold values from -0.125 to 0.125
- w_forget: bfloat16 [2048, 8], replicated, may hold values from -0.125 to 0.125
- bias_in: float32 [8], replicated, may hold values from -2 to 2
- bias_forget: float32 [8], replicated, may hold values from -1 to 3
- w_proj: bfloat16 [1024, 2048], P('tp'), may hold values from -0.1875 to 0.1875
- matrix_state: float32 [256, 8, 128, 128], P('ep', 'tp'), may hold values from -0.6 to 0.6
- normal_state: float32 [256, 8, 128], P('ep', 'tp'), may hold values from -0.6 to 0.6
- stab_state: float32 [256, 8], P('ep', 'tp'), may hold values from -1 to 1
- route_ids: int32 [256, 2], P('ep'), may hold values from 0 to 3, all different within a row; in each aligned block of 32 rows (0 to 31, 32 to 63, ...) at most 32 rows name the same one
- route_weights: float32 [256, 2], P('ep'), may hold values from 0.1 to 1
- w_exp_gate: bfloat16 [8, 2048, 1536], P('ep', None, 'tp'), may hold values from -0.125 to 0.125
- w_exp_up: bfloat16 [8, 2048, 1536], P('ep', None, 'tp'), may hold values from -0.125 to 0.125
- w_exp_down: bfloat16 [8, 1536, 2048], P('ep', 'tp'), may hold values from -0.109375 to 0.109375
Outputs:
- mixed_out: bfloat16 [256, 2048], P('ep', 'tp')
- matrix_out: float32 [256, 8, 128, 128], P('ep', 'tp')
- normal_out: float32 [256, 8, 128], P('ep', 'tp')
- stab_out: float32 [256, 8], P('ep', 'tp')
Inputs may be any that keep to these rules, and one draw needn't show every extreme that they name: `route_ids`: each row names 2 different experts; among the rows of one index of ep no expert is named by more than 32 rows, and in every draw some expert is named by exactly 32 of them.
All inputs are finite; a program needn't handle non-finite values.
Results may differ from a plain program's by a relative error of at most 0.015.
Values may be sent and summed in bfloat16 or wider, within the bound.
No kernel may reach another device: no remote copies, remote signals or barrier semaphores. Data moves between devices by JAX's collectives and lax.ppermute only.
A program may use at most 64 MiB of HBM per device.

v0:
```python
import jax
import jax.numpy as jnp
from jax import lax
from jax.sharding import PartitionSpec as P

norm_epsilon = 1e-06


def rms_scale(row_block, gain):
    wide = row_block.astype(jnp.float32)
    factor = lax.rsqrt(jnp.mean(wide * wide, axis=-1, keepdims=True) + norm_epsilon)
    return (wide * factor * gain.astype(jnp.float32)).astype(jnp.bfloat16)


def memory_step(
    query,
    key_rows,
    value_rows,
    gate_rows,
    in_pre,
    forget_pre,
    matrix_state,
    normal_state,
    stab_state,
):
    log_forget = jax.nn.log_sigmoid(forget_pre)
    stab_new = jnp.maximum(log_forget + stab_state, in_pre)
    carry = jnp.exp(log_forget + stab_state - stab_new)
    inflow = jnp.exp(in_pre - stab_new)
    scaled_keys = key_rows.astype(jnp.float32) * query.shape[-1] ** (-0.5)
    value_wide = value_rows.astype(jnp.float32)
    matrix_new = (
        carry[..., None, None] * matrix_state
        + inflow[..., None, None] * scaled_keys[..., :, None] * value_wide[..., None, :]
    )
    normal_new = carry[..., None] * normal_state + inflow[..., None] * scaled_keys
    query_wide = query.astype(jnp.float32)
    numer = jnp.einsum("shd,shde->she", query_wide, matrix_new, precision=lax.Precision.HIGHEST)
    denom = jnp.maximum(jnp.abs(jnp.sum(query_wide * normal_new, axis=-1)), 1.0)
    hidden = numer / denom[..., None] * jax.nn.sigmoid(gate_rows.astype(jnp.float32))
    return (hidden, matrix_new, normal_new, stab_new)


def dispatch_table(route_ids, experts, capacity):
    flat_ids = route_ids.reshape(-1)
    expert_hot = (flat_ids[:, None] == jnp.arange(experts, dtype=jnp.int32)[None, :]).astype(
        jnp.int32
    )
    slot_rank = jnp.sum((jnp.cumsum(expert_hot, axis=0) - 1) * expert_hot, axis=1)
    slot_hot = (slot_rank[:, None] == jnp.arange(capacity, dtype=jnp.int32)[None, :]).astype(
        jnp.float32
    )
    table = expert_hot.astype(jnp.float32)[:, :, None] * slot_hot[:, None, :]
    return table.reshape(flat_ids.shape[0], experts * capacity)


def send_rows(table, row_block, top_count, experts, capacity):
    repeated = jnp.repeat(row_block, top_count, axis=0)
    packed = jnp.einsum(
        "as,aw->sw", table.astype(jnp.bfloat16), repeated, preferred_element_type=jnp.float32
    ).astype(jnp.bfloat16)
    row_width = row_block.shape[1]
    doubled = jnp.broadcast_to(
        packed.reshape(experts, 1, capacity, row_width), (experts, 2, capacity, row_width)
    )
    return doubled.reshape(experts * 2 * capacity, row_width)


def body(
    tokens,
    gain_mix,
    gain_ffn,
    w_query,
    w_key,
    w_value,
    w_outgate,
    w_ingate,
    w_forget,
    bias_in,
    bias_forget,
    w_proj,
    matrix_state,
    normal_state,
    stab_state,
    route_ids,
    route_weights,
    w_exp_gate,
    w_exp_up,
    w_exp_down,
):
    ep_count = lax.axis_size("ep")
    tp_count = lax.axis_size("tp")
    tp_index = lax.axis_index("tp")
    seq_dev = tokens.shape[0]
    model_width = tokens.shape[1]
    heads_dev = matrix_state.shape[1]
    head_dim = matrix_state.shape[2]
    head_cols = w_query.shape[1]
    top_count = route_ids.shape[1]
    experts = ep_count // 2
    capacity = min(seq_dev, max(2, 2 * seq_dev * top_count // experts))
    col_width = model_width // tp_count
    normed = rms_scale(tokens, gain_mix)
    foreign = lax.all_to_all(normed, "ep", split_axis=1, concat_axis=0, tiled=True)
    summed = lax.psum_scatter(
        jnp.concatenate(
            [
                jnp.dot(foreign, weight, preferred_element_type=jnp.float32)
                for weight in (w_query, w_key, w_value, w_outgate)
            ],
            axis=1,
        ),
        "ep",
        scatter_dimension=0,
        tiled=True,
    )
    partials = [summed[:, offset * head_cols : (offset + 1) * head_cols] for offset in range(4)]
    query, key_rows, value_rows, gate_rows = [
        partial_value.astype(jnp.bfloat16).reshape(seq_dev, heads_dev, head_dim)
        for partial_value in partials
    ]
    head_first = tp_index * heads_dev
    in_pre = lax.dynamic_slice_in_dim(
        jnp.dot(normed, w_ingate, preferred_element_type=jnp.float32) + bias_in,
        head_first,
        heads_dev,
        1,
    )
    forget_pre = lax.dynamic_slice_in_dim(
        jnp.dot(normed, w_forget, preferred_element_type=jnp.float32) + bias_forget,
        head_first,
        heads_dev,
        1,
    )
    hidden, matrix_new, normal_new, stab_new = memory_step(
        query,
        key_rows,
        value_rows,
        gate_rows,
        in_pre,
        forget_pre,
        matrix_state,
        normal_state,
        stab_state,
    )
    cell = hidden.reshape(seq_dev, head_cols).astype(jnp.bfloat16)
    partial_out = jnp.dot(cell, w_proj, preferred_element_type=jnp.float32)
    table = dispatch_table(route_ids, experts, capacity)
    gate_local = w_exp_gate[0]
    up_local = w_exp_up[0]
    attended = lax.psum(partial_out.astype(jnp.bfloat16), "tp").astype(jnp.float32)
    resid = (tokens.astype(jnp.float32) + attended).astype(jnp.bfloat16)
    normed_ffn = rms_scale(resid, gain_ffn)
    own_resid = lax.dynamic_slice_in_dim(resid, tp_index * col_width, col_width, 1)
    outgoing = send_rows(table, normed_ffn, top_count, experts, capacity)
    received = lax.all_to_all(outgoing, "ep", split_axis=0, concat_axis=0, tiled=True)
    gate_sum = jnp.dot(received, gate_local, preferred_element_type=jnp.float32)
    up_sum = jnp.dot(received, up_local, preferred_element_type=jnp.float32)
    inner = (jax.nn.silu(gate_sum) * up_sum).astype(jnp.bfloat16)
    expert_terms = jnp.dot(inner, w_exp_down[0], preferred_element_type=jnp.float32)
    half_share = lax.psum_scatter(
        expert_terms.astype(jnp.bfloat16), "tp", scatter_dimension=1, tiled=True
    )
    returned = lax.all_to_all(half_share, "ep", split_axis=0, concat_axis=0, tiled=True)
    halves_summed = jnp.sum(
        returned.astype(jnp.float32).reshape(experts, 2, capacity, col_width), axis=1
    ).reshape(experts * capacity, col_width)
    weights = route_weights / jnp.sum(route_weights, axis=-1, keepdims=True)
    combine = jnp.sum(
        (table * weights.reshape(-1)[:, None]).reshape(seq_dev, top_count, experts * capacity),
        axis=1,
    )
    routed = jnp.dot(combine, halves_summed, precision=lax.Precision.HIGHEST)
    mixed_out = (own_resid.astype(jnp.float32) + routed).astype(jnp.bfloat16)
    return (mixed_out, matrix_new, normal_new, stab_new)


def solution(mesh):
    placed = (
        P("ep", None),
        P(),
        P(),
        P("ep", "tp"),
        P("ep", "tp"),
        P("ep", "tp"),
        P("ep", "tp"),
        P(),
        P(),
        P(),
        P(),
        P("tp", None),
        P("ep", "tp", None, None),
        P("ep", "tp", None),
        P("ep", "tp"),
        P("ep", None),
        P("ep", None),
        P("ep", None, "tp"),
        P("ep", None, "tp"),
        P("ep", "tp", None),
    )
    return jax.shard_map(
        body,
        mesh=mesh,
        in_specs=placed,
        out_specs=(P("ep", "tp"), P("ep", "tp", None, None), P("ep", "tp", None), P("ep", "tp")),
        check_vma=False,
    )
```

profile of v0, /device:TPU:0, one launch (start us, length us, event | category | flops | bytes accessed | tf_op | source)
XLA Modules:
  0.0 213.6 jit_solution(9406941949861868896)
XLA Ops:
  7.2 0.0 copy-start
  7.2 0.0 reduce-scatter.7.cloned.1.call-start
  7.2 1.2 fusion.22
  8.4 0.7 convert_element_type.121
  9.1 1.0 fusion.24
  10.1 14.5 %all_to_all.40 = bf16[32,8,256]{2,0,1:T(8,128)(2,1)S(1)} all-to-all(bf16[32,8,256]{2,0,1:T(8,128)(2,1)S(1)} %bitcast.72), channel_id=1, replica_groups=mesh['ep'=8,'tp'=4] {'ep'}, dimensions={1} | all-to-all | bytes 262144 | tf_op jit(solution)/shard_map/all_to_all | solution.py:104
  24.6 1.1 fusion.41
  25.7 1.1 fusion.40
  26.9 0.2 fusion.39
  27.1 0.2 fusion.38
  27.3 0.1 pad_maximum_fusion
  27.4 0.0 copy-start.10
  27.5 0.0 copy-start.13
  27.5 0.0 copy-start.15
  27.5 1.3 copy.72
  28.8 0.0 reduce-scatter.7.cloned.1.call-update
  28.8 0.0 all-reduce.2.cloned.1.call-start
  28.9 0.1 copy.63
  29.0 0.1 eq.36
  29.1 0.1 fusion.29
  29.2 0.1 copy.64
  29.2 0.1 reduce_window_sum.11
  29.4 0.1 convolution_add_fusion.1
  29.5 0.0 copy-done.13
  29.5 0.1 convolution_add_fusion.2
  29.7 0.0 copy-done.11
  29.7 0.0 copy-start.9
  29.7 0.1 copy.56
  29.8 0.1 copy.57
  29.9 0.2 select_reduce_fusion
  30.1 61.5 %reduce-scatter.7.cloned.1.call-done = f32[32,1024]{1,0:T(8,128)} async-done(((f32[256,1024]{1,0:T(8,128)}), f32[32,1024]{1,0:T(8,128)}) %reduce-scatter.7.cloned.1.call-update) | async-done | bytes 131088
  91.6 1.1 copy.73
  92.7 0.1 copy.60
  92.8 0.1 copy.74
  92.9 0.1 copy.58
  93.0 0.1 copy.59
  93.1 0.8 multiply_reduce_fusion.2
  93.9 0.1 copy.62
  94.0 6.0 %multiply_reduce_fusion = (f32[32,2,128]{2,1,0:T(2,128)S(1)}, f32[32,2,128,128]{3,2,1,0:T(8,128)}) fusion(f32[32,2,128]{2,1,0:T(2,128)S(1)} %copy.74, f32[32,2,128]{2,1,0:T(2,128)S(1)} %copy.59, f32[32,2,128]{2,1,0:T(2,128)S(1)} %get-tuple-element.8, f32[32,2,128,128]{3,2,1,0:T(8,128)} %param.32, f32[32,2]{1,0:T(8,128)S(1)} %copy.56), kind=kLoop, calls=%fused_computation | loop fusion | flops 5234688 | bytes 8519936
  100.0 0.0 copy-start.2
  100.0 0.1 copy.71
  100.1 1.0 convolution_convert_fusion.2
  101.1 0.0 all-reduce.2.cloned.1.call-update
  101.1 0.0 reduce-scatter.5.cloned.1.call-start
  101.2 30.9 %all-reduce.2.cloned.1.call-done = bf16[32,2048]{1,0:T(8,128)(2,1)} async-done(((bf16[32,2048]{1,0:T(8,128)(2,1)}), bf16[32,2048]{1,0:T(8,128)(2,1)}) %all-reduce.2.cloned.1.call-update) | async-done | bytes 131088 | tf_op jit(solution)/shard_map/psum | solution.py:151
  132.1 1.1 fusion.19
  133.1 0.1 fusion.21
  133.3 0.1 broadcast_in_dim.6
  133.4 0.1 reshape.157
  133.5 0.3 convolution_convert_fusion.1
  133.8 0.0 copy-start.1
  133.8 0.1 broadcast_in_dim.8
  133.9 30.2 %all_to_all.41 = bf16[8,32,2048]{2,1,0:T(8,128)(2,1)S(1)} all-to-all(bf16[8,32,2048]{2,1,0:T(8,128)(2,1)S(1)} %bitcast.61), channel_id=1, replica_groups=mesh['ep'=8,'tp'=4] {'ep'}, dimensions={0} | all-to-all | bytes 2097152 | tf_op jit(solution)/shard_map/all_to_all | solution.py:156
  164.1 0.7 fusion.3
  164.9 3.7 %convolution_convert_fusion = bf16[256,2048]{1,0:T(8,128)(2,1)} fusion(bf16[1,384,2048]{2,1,0:T(8,128)(2,1)S(1)} %copy-done, bf16[256,2048]{1,0:T(8,128)(2,1)S(1)} %bitcast.60, bf16[1,2048,384]{2,1,0:T(8,128)(2,1)} %param.38, f32[256,384]{1,0:T(8,128)S(1)} %fusion.3), kind=kOutput, calls=%fused_computation.2 | convolution fusion | flops 806420480 | bytes 5636096 | tf_op jit(solution)/shard_map/dot_general | solution.py:160
  168.6 0.0 reduce-scatter.5.cloned.1.call-update
  168.6 23.2 %reduce-scatter.5.cloned.1.call-done = bf16[256,512]{1,0:T(8,128)(2,1)} async-done(((bf16[256,2048]{1,0:T(8,128)(2,1)}), bf16[256,512]{1,0:T(8,128)(2,1)}) %reduce-scatter.5.cloned.1.call-update) | async-done | bytes 262160 | tf_op jit(solution)/shard_map/reduce_scatter | solution.py:161
  191.8 5.5 %all-to-all-start.2 = ((bf16[8,32,512]{2,1,0:T(8,128)(2,1)}), bf16[8,32,512]{2,1,0:T(8,128)(2,1)S(1)}, u32[]{:S(2)}, u32[]{:S(2)}) async-start(bf16[8,32,512]{2,1,0:T(8,128)(2,1)} %bitcast.74), calls=%async_computation.3 | async-start | bytes 524288 | tf_op jit(solution)/shard_map/all_to_all | solution.py:164
  197.4 0.1 copy.66
  197.5 0.1 copy.65
  197.6 0.1 mul.171
  197.7 0.1 multiply_reduce_fusion.1
  197.8 8.3 %all-to-all-done.2 = bf16[8,32,512]{2,1,0:T(8,128)(2,1)S(1)} async-done(((bf16[8,32,512]{2,1,0:T(8,128)(2,1)}), bf16[8,32,512]{2,1,0:T(8,128)(2,1)S(1)}, u32[]{:S(2)}, u32[]{:S(2)}) %all-to-all-start.2) | async-done | bytes 262176 | tf_op jit(solution)/shard_map/all_to_all | solution.py:164
  206.2 0.9 fusion.13
  (38 shorter events, 0.3 us)
Async XLA Ops:
  7.2 157.7 %copy-start = (bf16[1,384,2048]{2,1,0:T(8,128)(2,1)S(1)}, bf16[1,384,2048]{2,1,0:T(8,128)(2,1)}, u32[]{:S(2)}) copy-start(bf16[1,384,2048]{2,1,0:T(8,128)(2,1)} %param.39) | copy-start | bytes 4718596
  7.2 19.7 %copy-start.4 = (bf16[256,256]{1,0:T(8,128)(2,1)S(1)}, bf16[256,256]{1,0:T(8,128)(2,1)}, u32[]{:S(2)}) copy-start(bf16[256,256]{1,0:T(8,128)(2,1)} %param.24) | copy-start | bytes 393220
  7.2 19.9 %copy-start.5 = (bf16[256,256]{1,0:T(8,128)(2,1)S(1)}, bf16[256,256]{1,0:T(8,128)(2,1)}, u32[]{:S(2)}) copy-start(bf16[256,256]{1,0:T(8,128)(2,1)} %param.23) | copy-start | bytes 393220
  7.2 84.4 %reduce-scatter.7.cloned.1.call-start = ((), (), s32[]{:S(2)}) async-start(), calls=%async_computation.7 | async-start | bytes 1179648
  27.4 1.5 copy-start.10
  27.4 1.9 copy-start.12
  27.4 1.9 copy-start.14
  27.5 2.0 copy-start.13
  27.5 2.0 copy-start.15
  27.5 2.2 %copy-start.11 = (f32[32,2]{0,1:T(2,128)S(1)}, f32[32,2]{0,1:T(2,128)}, u32[]{:S(2)}) copy-start(f32[32,2]{0,1:T(2,128)} %param.34) | copy-start | bytes 772
  28.8 64.3 %copy-start.6 = (f32[32,2,128]{2,1,0:T(2,128)S(1)}, f32[32,2,128]{2,1,0:T(2,128)}, u32[]{:S(2)}) copy-start(f32[32,2,128]{2,1,0:T(2,128)} %param.33) | copy-start | bytes 98308
  28.8 103.2 %all-reduce.2.cloned.1.call-start = ((), (), s32[]{:S(2)}) async-start(), calls=%async_computation.5 | async-start | bytes 262144 | tf_op jit(solution)/shard_map/psum | solution.py:151
  29.7 70.2 %copy-start.9 = (f32[32,2]{0,1:T(2,128)}, f32[32,2]{0,1:T(2,128)S(1)}, u32[]{:S(2)}) copy-start(f32[32,2]{0,1:T(2,128)S(1)} %get-tuple-element.12) | copy-start | bytes 772
  94.0 6.1 %copy-start.3 = (bf16[256,2048]{1,0:T(8,128)(2,1)S(1)}, bf16[256,2048]{1,0:T(8,128)(2,1)}, u32[]{:S(2)}) copy-start(bf16[256,2048]{1,0:T(8,128)(2,1)} %param.31) | copy-start | bytes 3145732
  99.9 1.2 copy-start.7
  100.0 32.1 %copy-start.2 = (bf16[32,2048]{1,0:T(8,128)(2,1)S(1)}, bf16[32,2048]{1,0:T(8,128)(2,1)}, u32[]{:S(2)}) copy-start(bf16[32,2048]{1,0:T(8,128)(2,1)} %param.20) | copy-start | bytes 393220
  101.1 90.7 %reduce-scatter.5.cloned.1.call-start = ((), (), s32[]{:S(2)}) async-start(), calls=%async_computation.6 | async-start | bytes 1310720 | tf_op jit(solution)/shard_map/reduce_scatter | solution.py:161
  133.8 30.3 %copy-start.1 = (bf16[1,2048,384]{2,1,0:T(8,128)(2,1)S(1)}, bf16[1,2048,384]{2,1,0:T(8,128)(2,1)}, u32[]{:S(2)}) copy-start(bf16[1,2048,384]{2,1,0:T(8,128)(2,1)} %param.37) | copy-start | bytes 4718596
  168.6 28.7 %copy-start.8 = (f32[32,2]{0,1:T(2,128)S(1)}, f32[32,2]{0,1:T(2,128)}, u32[]{:S(2)}) copy-start(f32[32,2]{0,1:T(2,128)} %param.36) | copy-start | bytes 772
  191.8 14.3 %all-to-all-start.2 = ((bf16[8,32,512]{2,1,0:T(8,128)(2,1)}), bf16[8,32,512]{2,1,0:T(8,128)(2,1)S(1)}, u32[]{:S(2)}, u32[]{:S(2)}) async-start(bf16[8,32,512]{2,1,0:T(8,128)(2,1)} %bitcast.74), calls=%async_computation.3 | async-start | bytes 524288 | tf_op jit(solution)/shard_map/all_to_all | solution.py:164
Sparse Core Ops, SparseCore 0:
  29.0 62.5 reduce-scatter.6
  101.2 30.8 all-reduce.1
  168.8 23.0 reduce-scatter.4
where the time goes:
time: 214 us
  waiting for transfers between devices  124 us (58%)
  blocking collectives  44.6 us (21%)
  between operations  14.2 us (7%)
  other arithmetic  11.5 us (5%)
  matrix products  9.5 us (4%)
  starting transfers between devices  5.62 us (3%)
  local copies, waits for them, and re-layouts  4.18 us (2%)
    unnamed x4, waiting for transfers between devices  61.5 us
    psum x1, waiting for transfers between devices, body(): lax.psum(partial_out.astype(jnp.bfloat16), 'tp').astype(jnp.float32)  30.9 us
    all_to_all x1, blocking collectives, body(): lax.all_to_all(outgoing, 'ep', split_axis=0, concat_axis=0, tiled=True)  30.2 us
    reduce_scatter x1, waiting for transfers between devices, body(): lax.psum_scatter(expert_terms.astype(jnp.bfloat16), 'tp', scatter_dimensi...  23.2 us
    all_to_all x1, blocking collectives, body(): lax.all_to_all(normed, 'ep', split_axis=1, concat_axis=0, tiled=True)  14.5 us
    all_to_all x1, waiting for transfers between devices, body(): lax.all_to_all(half_share, 'ep', split_axis=0, concat_axis=0, tiled=True)  8.28 us
    unnamed x1, other arithmetic  5.95 us
    all_to_all x1, starting transfers between devices, body(): lax.all_to_all(half_share, 'ep', split_axis=0, concat_axis=0, tiled=True)  5.5 us
  transfers between devices with their start and end apart: 4, of which 4 were waited for; matrix products, arithmetic and copies ran while one was open for 1% of the time, Pallas kernels for 0%

commit v1 on v0

--- a/solution.py
+++ b/solution.py
@@ -54,16 +54,62 @@
     return table.reshape(flat_ids.shape[0], experts * capacity)
 
 
-def send_rows(table, row_block, top_count, experts, capacity):
+def pack_rows(table, row_block, top_count, experts, capacity):
     repeated = jnp.repeat(row_block, top_count, axis=0)
     packed = jnp.einsum(
         "as,aw->sw", table.astype(jnp.bfloat16), repeated, preferred_element_type=jnp.float32
     ).astype(jnp.bfloat16)
-    row_width = row_block.shape[1]
-    doubled = jnp.broadcast_to(
-        packed.reshape(experts, 1, capacity, row_width), (experts, 2, capacity, row_width)
-    )
-    return doubled.reshape(experts * 2 * capacity, row_width)
+    return packed.reshape(experts, capacity, row_block.shape[1])
+
+
+def swap(value, axis, bit):
+    count = lax.axis_size(axis)
+    return lax.ppermute(value, axis, [(i, i ^ bit) for i in range(count)])
+
+
+def bits_of(count):
+    return [1 << place for place in range(count.bit_length() - 1)]
+
+
+def scatter_columns(terms, axis):
+    count = lax.axis_size(axis)
+    index = lax.axis_index(axis)
+    width = terms.shape[1] // count
+
+    def block(peer):
+        return lax.dynamic_slice_in_dim(terms, (index ^ peer) * width, width, 1)
+
+    total = block(0)
+    for peer in range(1, count):
+        total = total + swap(block(peer).astype(jnp.bfloat16), axis, peer).astype(jnp.float32)
+    return total
+
+
+def halve_columns(terms, axis):
+    count = lax.axis_size(axis)
+    index = lax.axis_index(axis)
+    rows, columns = terms.shape
+    blocks = terms.reshape(rows, count, columns // count)
+    for bit in bits_of(count):
+        pairs = blocks.reshape(rows, -1, 2, blocks.shape[-1])
+        own = (index // bit) % 2
+        kept = jnp.where(own == 0, pairs[:, :, 0], pairs[:, :, 1])
+        sent = jnp.where(own == 0, pairs[:, :, 1], pairs[:, :, 0]).astype(jnp.bfloat16)
+        blocks = kept + swap(sent, axis, bit).astype(jnp.float32)
+    return blocks.reshape(rows, columns // count)
+
+
+def gather_columns(own, axis):
+    count = lax.axis_size(axis)
+    index = lax.axis_index(axis)
+    held = own[None]
+    for bit in reversed(bits_of(count)):
+        other = swap(held, axis, bit)
+        first = (index // bit) % 2 == 0
+        low = jnp.where(first, held, other)
+        high = jnp.where(first, other, held)
+        held = jnp.stack([low, high], axis=1).reshape((-1,) + own.shape)
+    return held
 
 
 def body(
@@ -90,35 +136,42 @@
 ):
     ep_count = lax.axis_size("ep")
     tp_count = lax.axis_size("tp")
+    ep_index = lax.axis_index("ep")
     tp_index = lax.axis_index("tp")
     seq_dev = tokens.shape[0]
     model_width = tokens.shape[1]
     heads_dev = matrix_state.shape[1]
     head_dim = matrix_state.shape[2]
     head_cols = w_query.shape[1]
+    feature_rows = w_query.shape[0]
     top_count = route_ids.shape[1]
     experts = ep_count // 2
     capacity = min(seq_dev, max(2, 2 * seq_dev * top_count // experts))
+    every_row = capacity == seq_dev
     col_width = model_width // tp_count
-    normed = rms_scale(tokens, gain_mix)
-    foreign = lax.all_to_all(normed, "ep", split_axis=1, concat_axis=0, tiled=True)
-    summed = lax.psum_scatter(
-        jnp.concatenate(
-            [
-                jnp.dot(foreign, weight, preferred_element_type=jnp.float32)
-                for weight in (w_query, w_key, w_value, w_outgate)
-            ],
-            axis=1,
-        ),
-        "ep",
-        scatter_dimension=0,
-        tiled=True,
-    )
-    partials = [summed[:, offset * head_cols : (offset + 1) * head_cols] for offset in range(4)]
+    foreign = lax.all_to_all(tokens, "ep", split_axis=1, concat_axis=0, tiled=True)
+    own_gain = lax.dynamic_slice_in_dim(gain_mix, ep_index * feature_rows, feature_rows, 0)
+    scaled = (foreign.astype(jnp.float32) * own_gain.astype(jnp.float32)).astype(jnp.bfloat16)
+    terms = jnp.concatenate(
+        [
+            jnp.dot(scaled, weight, preferred_element_type=jnp.float32).astype(jnp.bfloat16)
+            for weight in (w_query, w_key, w_value, w_outgate)
+        ],
+        axis=1,
+    )
+    arrived = lax.all_to_all(terms, "ep", split_axis=0, concat_axis=0, tiled=True)
+    wide = tokens.astype(jnp.float32)
+    factor = lax.rsqrt(jnp.mean(wide * wide, axis=-1, keepdims=True) + norm_epsilon)
+    summed = factor * jnp.sum(
+        arrived.astype(jnp.float32).reshape(ep_count, seq_dev, 4 * head_cols), axis=0
+    )
     query, key_rows, value_rows, gate_rows = [
-        partial_value.astype(jnp.bfloat16).reshape(seq_dev, heads_dev, head_dim)
-        for partial_value in partials
+        summed[:, offset * head_cols : (offset + 1) * head_cols]
+        .astype(jnp.bfloat16)
+        .reshape(seq_dev, heads_dev, head_dim)
+        for offset in range(4)
     ]
+    normed = (wide * factor * gain_mix.astype(jnp.float32)).astype(jnp.bfloat16)
     head_first = tp_index * heads_dev
     in_pre = lax.dynamic_slice_in_dim(
         jnp.dot(normed, w_ingate, preferred_element_type=jnp.float32) + bias_in,
@@ -145,32 +198,41 @@
     )
     cell = hidden.reshape(seq_dev, head_cols).astype(jnp.bfloat16)
     partial_out = jnp.dot(cell, w_proj, preferred_element_type=jnp.float32)
-    table = dispatch_table(route_ids, experts, capacity)
-    gate_local = w_exp_gate[0]
-    up_local = w_exp_up[0]
-    attended = lax.psum(partial_out.astype(jnp.bfloat16), "tp").astype(jnp.float32)
-    resid = (tokens.astype(jnp.float32) + attended).astype(jnp.bfloat16)
-    normed_ffn = rms_scale(resid, gain_ffn)
-    own_resid = lax.dynamic_slice_in_dim(resid, tp_index * col_width, col_width, 1)
-    outgoing = send_rows(table, normed_ffn, top_count, experts, capacity)
-    received = lax.all_to_all(outgoing, "ep", split_axis=0, concat_axis=0, tiled=True)
-    gate_sum = jnp.dot(received, gate_local, preferred_element_type=jnp.float32)
-    up_sum = jnp.dot(received, up_local, preferred_element_type=jnp.float32)
+    own_tokens = lax.dynamic_slice_in_dim(tokens, tp_index * col_width, col_width, 1)
+    attended = scatter_columns(partial_out, "tp")
+    own_resid = (own_tokens.astype(jnp.float32) + attended).astype(jnp.bfloat16)
+    if every_row:
+        packed = jnp.broadcast_to(own_resid, (experts, seq_dev, col_width))
+    else:
+        table = dispatch_table(route_ids, experts, capacity)
+        packed = pack_rows(table, own_resid, top_count, experts, capacity)
+    outgoing = jnp.broadcast_to(packed[:, None], (experts, 2, capacity, col_width))
+    received = lax.all_to_all(
+        outgoing.reshape(ep_count * capacity, col_width), "ep", split_axis=0, concat_axis=0, tiled=True
+    )
+    rows = gather_columns(received, "tp").transpose(1, 0, 2).reshape(-1, model_width)
+    normed_ffn = rms_scale(rows, gain_ffn)
+    gate_sum = jnp.dot(normed_ffn, w_exp_gate[0], preferred_element_type=jnp.float32)
+    up_sum = jnp.dot(normed_ffn, w_exp_up[0], preferred_element_type=jnp.float32)
     inner = (jax.nn.silu(gate_sum) * up_sum).astype(jnp.bfloat16)
     expert_terms = jnp.dot(inner, w_exp_down[0], preferred_element_type=jnp.float32)
-    half_share = lax.psum_scatter(
-        expert_terms.astype(jnp.bfloat16), "tp", scatter_dimension=1, tiled=True
-    )
+    half_share = halve_columns(expert_terms, "tp").astype(jnp.bfloat16)
     returned = lax.all_to_all(half_share, "ep", split_axis=0, concat_axis=0, tiled=True)
-    halves_summed = jnp.sum(
-        returned.astype(jnp.float32).reshape(experts, 2, capacity, col_width), axis=1
-    ).reshape(experts * capacity, col_width)
+    halves = returned.astype(jnp.float32).reshape(experts, 2, capacity, col_width)
     weights = route_weights / jnp.sum(route_weights, axis=-1, keepdims=True)
-    combine = jnp.sum(
-        (table * weights.reshape(-1)[:, None]).reshape(seq_dev, top_count, experts * capacity),
-        axis=1,
-    )
-    routed = jnp.dot(combine, halves_summed, precision=lax.Precision.HIGHEST)
+    if every_row:
+        chosen = route_ids[:, :, None] == jnp.arange(experts, dtype=jnp.int32)
+        shares = jnp.sum(jnp.where(chosen, weights[:, :, None], 0.0), axis=1)
+        routed = jnp.sum(halves * shares.T[:, None, :, None], axis=(0, 1))
+    else:
+        combine = jnp.sum(
+            (table * weights.reshape(-1)[:, None]).reshape(
+                seq_dev, top_count, experts * capacity
+            ),
+            axis=1,
+        )
+        halves_summed = jnp.sum(halves, axis=1).reshape(experts * capacity, col_width)
+        routed = jnp.dot(combine, halves_summed, precision=lax.Precision.HIGHEST)
     mixed_out = (own_resid.astype(jnp.float32) + routed).astype(jnp.bfloat16)
     return (mixed_out, matrix_new, normal_new, stab_new)
 

time: 214 us -> 113 us (0.53)
  waiting for transfers between devices: 124 us -> 44.6 us
  blocking collectives: 44.6 us -> 12.7 us
  starting transfers between devices: 5.62 us -> 19.9 us
  between operations: 14.2 us -> 1.13 us
  matrix products: 9.5 us -> 12.7 us
  local copies, waits for them, and re-layouts: 4.18 us -> 7.19 us
  other arithmetic: 11.5 us -> 13.7 us
    unnamed x4 -> x0, waiting for transfers between devices: 61.5 us -> none
    all_to_all x2 -> x1, blocking collectives: 44.6 us -> 12.7 us  [body(): lax.all_to_all(outgoing.reshape(ep_count * capacity, col_width), 'ep', sp...]
    psum x1 -> x0, waiting for transfers between devices: 30.9 us -> none  [body(): lax.psum(partial_out.astype(jnp.bfloat16), 'tp').astype(jnp.float32)]
    reduce_scatter x1 -> x0, waiting for transfers between devices: 23.2 us -> none  [body(): lax.psum_scatter(expert_terms.astype(jnp.bfloat16), 'tp', scatter_dimensi...]
    all_to_all x0 -> x2, waiting for transfers between devices: none -> 18 us  [the longest x1 12.5 us: body(): lax.all_to_all(terms, 'ep', split_axis=0, concat_axis=0, tiled=True)]
    ppermute x0 -> x7, waiting for transfers between devices: none -> 18 us  [swap(): return lax.ppermute(value, axis, [(i, i ^ bit) for i in range(count)])]
    all_to_all x0 -> x2, starting transfers between devices: none -> 10.8 us  [the longest x1 7.31 us: body(): lax.all_to_all(tokens, 'ep', split_axis=1, concat_axis=0, tiled=True)]
    unnamed x1 -> x0, other arithmetic: 5.95 us -> none
  transfers between devices with their start and end apart: 4 -> 10, of which waited for: 4 -> 8; matrix products, arithmetic and copies ran while one was open for 1% -> 5% of each run, Pallas kernels for 0% -> 0%
where the time goes in v1:
time: 113 us; the launch traced here: 112 us
  waiting for transfers between devices  44.6 us (39%)
  starting transfers between devices  19.9 us (18%)
  other arithmetic  13.7 us (12%)
  matrix products  12.7 us (11%)
  blocking collectives  12.7 us (11%)
  local copies, waits for them, and re-layouts  7.19 us (6%)
    ppermute x7, waiting for transfers between devices, swap(): return lax.ppermute(value, axis, [(i, i ^ bit) for i in range(count)])  18 us
    all_to_all x1, blocking collectives, body(): lax.all_to_all(outgoing.reshape(ep_count * capacity, col_width), 'ep', sp...  12.7 us
    all_to_all x1, waiting for transfers between devices, body(): lax.all_to_all(terms, 'ep', split_axis=0, concat_axis=0, tiled=True)  12.5 us
    all_to_all x1, waiting for transfers between devices, body(): lax.all_to_all(half_share, 'ep', split_axis=0, concat_axis=0, tiled=True)  8.54 us
    all_to_all x1, starting transfers between devices, body(): lax.all_to_all(tokens, 'ep', split_axis=1, concat_axis=0, tiled=True)  7.31 us
    all_to_all x1, waiting for transfers between devices, body(): lax.all_to_all(tokens, 'ep', split_axis=1, concat_axis=0, tiled=True)  5.55 us
    all_to_all x1, starting transfers between devices, body(): lax.all_to_all(half_share, 'ep', split_axis=0, concat_axis=0, tiled=True)  4.7 us
    ppermute x7, starting transfers between devices, swap(): return lax.ppermute(value, axis, [(i, i ^ bit) for i in range(count)])  4.37 us
  transfers between devices with their start and end apart: 10, of which 8 were waited for; matrix products, arithmetic and copies ran while one was open for 5% of the time, Pallas kernels for 0%

profile of v1, /device:TPU:0, one launch (start us, length us, event | category | flops | bytes accessed | tf_op | source)
XLA Modules:
  0.0 111.9 jit_solution(5496403255579965468)
XLA Ops:
  0.6 0.0 copy-start
  0.7 1.7 %copy.99 = bf16[4,8,8,256]{3,2,0,1:T(8,128)(2,1)} copy(bf16[4,8,8,256]{3,2,1,0:T(8,128)(2,1)} %bitcast.125) | data formatting | bytes 262144 | tf_op jit(solution)/shard_map/all_to_all | solution.py:152
  2.4 7.3 %all-to-all-start = ((bf16[32,8,256]{2,0,1:T(8,128)(2,1)}), bf16[32,8,256]{2,0,1:T(8,128)(2,1)S(1)}, u32[]{:S(2)}, u32[]{:S(2)}) async-start(bf16[32,8,256]{2,0,1:T(8,128)(2,1)} %bitcast.117), calls=%async_computation | async-start | bytes 262144 | tf_op jit(solution)/shard_map/all_to_all | solution.py:152
  9.7 0.8 dynamic-slice_convert_fusion.3
  10.4 1.0 fusion.30
  11.5 5.6 %all-to-all-done = bf16[32,8,256]{2,0,1:T(8,128)(2,1)S(1)} async-done(((bf16[32,8,256]{2,0,1:T(8,128)(2,1)}), bf16[32,8,256]{2,0,1:T(8,128)(2,1)S(1)}, u32[]{:S(2)}, u32[]{:S(2)}) %all-to-all-start) | async-done | bytes 131104 | tf_op jit(solution)/shard_map/all_to_all | solution.py:152
  17.0 1.1 %convolution_convert_fusion = bf16[256,256]{0,1:T(8,128)(2,1)S(1)} fusion(bf16[256,256]{1,0:T(8,128)(2,1)S(1)} %fusion.34, bf16[256,256]{1,0:T(8,128)(2,1)} %param.26), kind=kOutput, calls=%fused_computation.13 | convolution fusion | flops 33619968 | bytes 393216 | tf_op jit(solution)/shard_map/dot_general | solution.py:157
  18.2 0.0 copy-start.6
  18.2 0.0 copy-start.3
  18.2 0.0 copy-start.12
  18.2 0.0 copy-start.14
  18.2 1.2 %convolution_convert_fusion.1 = bf16[256,256]{0,1:T(8,128)(2,1)S(1)} fusion(bf16[256,256]{1,0:T(8,128)(2,1)S(1)} %fusion.34, bf16[256,256]{1,0:T(8,128)(2,1)} %param.25), kind=kOutput, calls=%fused_computation.14 | convolution fusion | flops 33619968 | bytes 393216 | tf_op jit(solution)/shard_map/dot_general | solution.py:157
  19.4 0.0 copy-start.13
  19.5 1.1 %convolution_convert_fusion.2 = bf16[256,256]{0,1:T(8,128)(2,1)S(1)} fusion(bf16[256,256]{1,0:T(8,128)(2,1)S(1)} %fusion.34, bf16[256,256]{1,0:T(8,128)(2,1)} %param.24), kind=kOutput, calls=%fused_computation.15 | convolution fusion | flops 33619968 | bytes 393216 | tf_op jit(solution)/shard_map/dot_general | solution.py:157
  20.6 0.0 copy-start.10
  20.6 0.2 convolution_convert_fusion.3
  20.9 0.0 copy-start.5
  20.9 1.0 copy.76
  21.9 3.5 %all-to-all-start.1 = ((bf16[8,32,1024]{2,1,0:T(8,128)(2,1)}), bf16[8,32,1024]{2,1,0:T(8,128)(2,1)S(1)}, u32[]{:S(2)}, u32[]{:S(2)}) async-start(bf16[8,32,1024]{2,1,0:T(8,128)(2,1)} %bitcast.2), calls=%async_computation.1 | async-start | bytes 1048576 | tf_op jit(solution)/shard_map/all_to_all | solution.py:162
  25.5 0.2 convolution_add_fusion
  25.7 0.2 convolution_add_fusion.1
  26.0 0.0 copy-start.9
  26.0 0.1 copy.78
  26.1 0.1 copy.77
  26.2 12.5 %all-to-all-done.1 = bf16[8,32,1024]{2,1,0:T(8,128)(2,1)S(1)} async-done(((bf16[8,32,1024]{2,1,0:T(8,128)(2,1)}), bf16[8,32,1024]{2,1,0:T(8,128)(2,1)S(1)}, u32[]{:S(2)}, u32[]{:S(2)}) %all-to-all-start.1) | async-done | bytes 524320 | tf_op jit(solution)/shard_map/all_to_all | solution.py:162
  38.7 0.1 convert_reduce_fusion
  38.8 0.1 multiply_convert_fusion
  39.0 0.8 multiply_reduce_fusion.1
  39.8 3.7 %multiply_add_fusion = f32[32,2,128,128]{3,2,1,0:T(8,128)S(1)} fusion(f32[32,2,128,128]{3,2,1,0:T(8,128)} %param.32, f32[32,2,128]{2,1,0:T(2,128)S(1)} %reshape.185, f32[32,2,128]{2,1,0:T(2,128)S(1)} %get-tuple-element.6, f32[32,2]{1,0:T(8,128)S(1)} %copy.77), kind=kLoop, calls=%fused_computation | loop fusion | flops 3145728 | bytes 8454400 | tf_op jit(solution)/shard_map/add | solution.py:33
  43.5 0.0 copy-start.1
  43.5 2.0 %fusion.48 = f32[32,2,1,128]{3,2,1,0:T(1,128)S(1)} fusion(bf16[32,2,128,1]{2,3,1,0:T(2,128)(2,1)S(1)} %reshape.194, f32[32,2,128,128]{3,2,1,0:T(8,128)S(1)} %multiply_add_fusion), kind=kOutput, calls=%fused_computation.88 | convolution fusion | flops 12582912 | bytes 4243456 | tf_op jit(solution)/shard_map/shd,shde->she/dot_general | solution.py:38
  45.5 0.1 fusion.38
  45.7 0.3 fusion.39
  46.0 0.1 collective-permute-start
  46.1 1.6 %collective-permute-start.1 = (bf16[32,512]{1,0:T(8,128)(2,1)S(1)}, bf16[32,512]{1,0:T(8,128)(2,1)S(1)}, u32[]{:S(2)}, u32[]{:S(2)}) collective-permute-start(bf16[32,512]{1,0:T(8,128)(2,1)S(1)} %get-tuple-element.15), channel_id=1, source_target_pairs={{0,2},{1,3},{2,0},{3,1},{4,6},{5,7},{6,4},{7,5},{8,10},{9,11},{10,... | collective-permute-start | bytes 98312 | tf_op jit(solution)/shard_map/ppermute | solution.py:67
  47.6 0.3 collective-permute-start.2
  47.9 2.1 %collective-permute-done.1 = bf16[32,512]{1,0:T(8,128)(2,1)S(1)} collective-permute-done((bf16[32,512]{1,0:T(8,128)(2,1)S(1)}, bf16[32,512]{1,0:T(8,128)(2,1)S(1)}, u32[]{:S(2)}, u32[]{:S(2)}) %collective-permute-start.1) | collective-permute-done | bytes 32800 | tf_op jit(solution)/shard_map/ppermute | solution.py:67
  50.0 0.9 collective-permute-done.2
  51.0 12.7 %all_to_all.37 = bf16[8,32,512]{2,1,0:T(8,128)(2,1)S(1)} all-to-all(bf16[8,32,512]{2,1,0:T(8,128)(2,1)S(1)} %all_to_all.30), channel_id=1, replica_groups=mesh['ep'=8,'tp'=4] {'ep'}, dimensions={0} | all-to-all | bytes 524288 | tf_op jit(solution)/shard_map/all_to_all | solution.py:210
  63.7 0.9 collective-permute-start.3
  64.6 5.7 %collective-permute-done.3 = bf16[1,256,512]{2,1,0:T(8,128)(2,1)S(1)} collective-permute-done((bf16[1,256,512]{2,1,0:T(8,128)(2,1)S(1)}, bf16[1,256,512]{2,1,0:T(8,128)(2,1)S(1)}, u32[]{:S(2)}, u32[]{:S(2)}) %collective-permute-start.3) | collective-permute-done | bytes 262176 | tf_op jit(solution)/shard_map/ppermute | solution.py:67
  70.4 0.1 maximum_bitcast_fusion
  70.4 0.1 collective-permute-start.4
  70.5 2.6 %copy.90 = bf16[2048,384]{1,0:T(8,128)(2,1)} copy(bf16[2048,384]{0,1:T(8,128)(2,1)} %bitcast.121) | data formatting | bytes 3145728 | tf_op jit(solution)/shard_map/dot_general | solution.py:218
  73.1 0.1 select_bitcast_fusion.1
  73.2 0.1 pad_maximum_fusion
  73.3 0.3 fusion
  73.6 1.3 %fusion.16 = bf16[256,4,512]{2,0,1:T(8,128)(2,1)} fusion(bf16[2,2,256,512]{3,2,1,0:T(8,128)(2,1)S(1)} %pad_maximum_fusion, f32[4,512]{1,0:T(4,128)S(1)} %reshape.189, f32[256]{0:T(256)S(1)} %add_rsqrt_fusion), kind=kLoop, calls=%fused_computation.19 | loop fusion | flops 2097152 | bytes 2106368 | tf_op jit(solution)/shard_map/convert_element_type | solution.py:12
  74.9 1.5 %copy.81 = bf16[256,4,512]{0,2,1:T(8,128)(2,1)S(1)} copy(bf16[256,4,512]{2,0,1:T(8,128)(2,1)} %fusion.16) | data formatting | bytes 2097152 | tf_op jit(solution)/shard_map/convert_element_type | solution.py:12
  76.4 2.1 %fusion.5 = f32[256,384]{1,0:T(8,128)S(1)} fusion(bf16[256,2048]{0,1:T(8,128)(2,1)S(1)} %bitcast.119, bf16[1,2048,384]{2,1,0:T(8,128)(2,1)} %param.37), kind=kOutput, calls=%fused_computation.8 | convolution fusion | flops 402653184 | bytes 3014656 | tf_op jit(solution)/shard_map/dot_general | solution.py:215
  78.6 4.1 %fusion.21 = f32[256,2,2,512]{3,0,2,1:T(8,128)} fusion(bf16[2,2,512,384]{3,2,1,0:T(8,128)(2,1)} %bitcast.122, bf16[256,2048]{0,1:T(8,128)(2,1)S(1)} %bitcast.120, bf16[1,2048,384]{2,1,0:T(8,128)(2,1)S(1)} %copy-done, f32[256,384]{1,0:T(8,128)S(1)} %fusion.5), kind=kOutput, calls=%fused_computation.27 | convolution fusion | flops 805896192 | bytes 6684672 | tf_op jit(solution)/shard_map/dot_general | solution.py:218
  82.7 1.6 %fusion.23 = bf16[256,2,512]{2,0,1:T(8,128)(2,1)S(1)} fusion(f32[256,2,2,512]{3,0,2,1:T(8,128)} %fusion.21, pred[]{:T(512)S(6)} %eq.29), kind=kLoop, calls=%fused_computation.28 | loop fusion | flops 262144 | bytes 1572865 | tf_op jit(solution)/shard_map/convert_element_type | solution.py:97
  84.3 0.5 collective-permute-start.5
  84.9 1.5 %collective-permute-done.5 = bf16[256,2,512]{2,0,1:T(8,128)(2,1)S(1)} collective-permute-done((bf16[256,2,512]{2,0,1:T(8,128)(2,1)S(1)}, bf16[256,2,512]{2,0,1:T(8,128)(2,1)S(1)}, u32[]{:S(2)}, u32[]{:S(2)}) %collective-permute-start.5) | collective-permute-done | bytes 524320 | tf_op jit(solution)/shard_map/ppermute | solution.py:67
  86.4 1.8 %fusion.19 = f32[256,1,2,512]{3,0,2,1:T(8,128)S(1)} fusion(bf16[256,2,512]{2,0,1:T(8,128)(2,1)S(1)} %collective-permute-done.5, f32[256,2,2,512]{3,0,2,1:T(8,128)} %fusion.21, pred[]{:T(512)S(6)} %eq.29), kind=kLoop, calls=%fused_computation.24 | loop fusion | flops 786432 | bytes 3670017 | tf_op jit(solution)/shard_map/reshape | solution.py:94
  88.3 0.0 copy-start.11
  88.3 0.1 fusion.33
  88.3 1.0 collective-permute-start.6
  89.3 7.7 %collective-permute-done.6 = bf16[256,1,512]{2,0,1:T(8,128)(2,1)S(1)} collective-permute-done((bf16[256,1,512]{2,0,1:T(8,128)(2,1)S(1)}, bf16[256,1,512]{2,0,1:T(8,128)(2,1)S(1)}, u32[]{:S(2)}, u32[]{:S(2)}) %collective-permute-start.6) | collective-permute-done | bytes 262176 | tf_op jit(solution)/shard_map/ppermute | solution.py:67
  97.0 0.8 fusion.24
  97.8 4.7 %all-to-all-start.3 = ((bf16[8,32,512]{2,1,0:T(8,128)(2,1)}), bf16[8,32,512]{2,1,0:T(8,128)(2,1)S(1)}, u32[]{:S(2)}, u32[]{:S(2)}) async-start(bf16[8,32,512]{2,1,0:T(8,128)(2,1)} %bitcast.31), calls=%async_computation.3 | async-start | bytes 524288 | tf_op jit(solution)/shard_map/all_to_all | solution.py:220
  102.6 8.5 %all-to-all-done.3 = bf16[8,32,512]{2,1,0:T(8,128)(2,1)S(1)} async-done(((bf16[8,32,512]{2,1,0:T(8,128)(2,1)}), bf16[8,32,512]{2,1,0:T(8,128)(2,1)S(1)}, u32[]{:S(2)}, u32[]{:S(2)}) %all-to-all-start.3) | async-done | bytes 262176 | tf_op jit(solution)/shard_map/all_to_all | solution.py:220
  111.1 0.1 multiply_reduce_fusion
  111.3 0.6 add_convert_fusion
  (47 shorter events, 0.5 us)
Async XLA Ops:
  0.6 77.9 %copy-start = (bf16[1,2048,384]{2,1,0:T(8,128)(2,1)S(1)}, bf16[1,2048,384]{2,1,0:T(8,128)(2,1)}, u32[]{:S(2)}) copy-start(bf16[1,2048,384]{2,1,0:T(8,128)(2,1)} %param.38) | copy-start | bytes 4718596
  0.6 20.0 %copy-start.4 = (bf16[256,256]{1,0:T(8,128)(2,1)S(1)}, bf16[256,256]{1,0:T(8,128)(2,1)}, u32[]{:S(2)}) copy-start(bf16[256,256]{1,0:T(8,128)(2,1)} %param.23) | copy-start | bytes 393220
  2.4 14.7 %all-to-all-start = ((bf16[32,8,256]{2,0,1:T(8,128)(2,1)}), bf16[32,8,256]{2,0,1:T(8,128)(2,1)S(1)}, u32[]{:S(2)}, u32[]{:S(2)}) async-start(bf16[32,8,256]{2,0,1:T(8,128)(2,1)} %bitcast.117), calls=%async_computation | async-start | bytes 262144 | tf_op jit(solution)/shard_map/all_to_all | solution.py:152
  18.2 7.3 %copy-start.6 = (bf16[2048]{0:T(1024)(128)(2,1)S(1)}, bf16[2048]{0:T(1024)(128)(2,1)}, u32[]{:S(2)}) copy-start(bf16[2048]{0:T(1024)(128)(2,1)} %param.21) | copy-start | bytes 12292
  18.2 7.3 %copy-start.3 = (bf16[32,2048]{1,0:T(8,128)(2,1)S(1)}, bf16[32,2048]{1,0:T(8,128)(2,1)}, u32[]{:S(2)}) copy-start(bf16[32,2048]{1,0:T(8,128)(2,1)} %param.20) | copy-start | bytes 393220
  18.2 7.3 %copy-start.12 = (bf16[2048,8]{0,1:T(8,128)(2,1)S(1)}, bf16[2048,8]{0,1:T(8,128)(2,1)}, u32[]{:S(2)}) copy-start(bf16[2048,8]{0,1:T(8,128)(2,1)} %param.27) | copy-start | bytes 98308
  18.2 7.3 %copy-start.14 = (f32[8]{0:T(128)S(1)}, f32[8]{0:T(128)}, u32[]{:S(2)}) copy-start(f32[8]{0:T(128)} %param.29) | copy-start | bytes 100
  19.4 6.3 %copy-start.13 = (bf16[2048,8]{0,1:T(8,128)(2,1)S(1)}, bf16[2048,8]{0,1:T(8,128)(2,1)}, u32[]{:S(2)}) copy-start(bf16[2048,8]{0,1:T(8,128)(2,1)} %param.28) | copy-start | bytes 98308
  19.5 6.3 %copy-start.15 = (f32[8]{0:T(128)S(1)}, f32[8]{0:T(128)}, u32[]{:S(2)}) copy-start(f32[8]{0:T(128)} %param.30) | copy-start | bytes 100
  20.6 5.3 %copy-start.10 = (f32[32,2]{0,1:T(2,128)S(1)}, f32[32,2]{0,1:T(2,128)}, u32[]{:S(2)}) copy-start(f32[32,2]{0,1:T(2,128)} %param.34) | copy-start | bytes 772
  20.9 18.1 %copy-start.5 = (f32[32,2,128]{2,1,0:T(2,128)S(1)}, f32[32,2,128]{2,1,0:T(2,128)}, u32[]{:S(2)}) copy-start(f32[32,2,128]{2,1,0:T(2,128)} %param.33) | copy-start | bytes 98308
  21.9 16.8 %all-to-all-start.1 = ((bf16[8,32,1024]{2,1,0:T(8,128)(2,1)}), bf16[8,32,1024]{2,1,0:T(8,128)(2,1)S(1)}, u32[]{:S(2)}, u32[]{:S(2)}) async-start(bf16[8,32,1024]{2,1,0:T(8,128)(2,1)} %bitcast.2), calls=%async_computation.1 | async-start | bytes 1048576 | tf_op jit(solution)/shard_map/all_to_all | solution.py:162
  26.0 17.5 %copy-start.9 = (f32[32,2]{0,1:T(2,128)}, f32[32,2]{0,1:T(2,128)S(1)}, u32[]{:S(2)}) copy-start(f32[32,2]{0,1:T(2,128)S(1)} %get-tuple-element.8) | copy-start | bytes 772
  43.5 2.0 %copy-start.1 = (f32[32,2,128,128]{3,2,1,0:T(8,128)}, f32[32,2,128,128]{3,2,1,0:T(8,128)S(1)}, u32[]{:S(2)}) copy-start(f32[32,2,128,128]{3,2,1,0:T(8,128)S(1)} %multiply_add_fusion) | copy-start | bytes 12582916
  43.5 2.2 %copy-start.2 = (bf16[256,2048]{1,0:T(8,128)(2,1)S(1)}, bf16[256,2048]{1,0:T(8,128)(2,1)}, u32[]{:S(2)}) copy-start(bf16[256,2048]{1,0:T(8,128)(2,1)} %param.31) | copy-start | bytes 3145732
  45.7 24.8 %copy-start.7 = (bf16[2048]{0:T(1024)(128)(2,1)S(1)}, bf16[2048]{0:T(1024)(128)(2,1)}, u32[]{:S(2)}) copy-start(bf16[2048]{0:T(1024)(128)(2,1)} %param.22) | copy-start | bytes 12292
  46.0 1.9 %collective-permute-start = (bf16[32,512]{1,0:T(8,128)(2,1)S(1)}, bf16[32,512]{1,0:T(8,128)(2,1)S(1)}, u32[]{:S(2)}, u32[]{:S(2)}) collective-permute-start(bf16[32,512]{1,0:T(8,128)(2,1)S(1)} %get-tuple-element.13), channel_id=1, source_target_pairs={{0,1},{1,0},{2,3},{3,2},{4,5},{5,4},{6,7},{7,6},{8,9},{9,8},{10,11... | collective-permute-start | bytes 98312 | tf_op jit(solution)/shard_map/ppermute | solution.py:67
  46.1 4.0 %collective-permute-start.1 = (bf16[32,512]{1,0:T(8,128)(2,1)S(1)}, bf16[32,512]{1,0:T(8,128)(2,1)S(1)}, u32[]{:S(2)}, u32[]{:S(2)}) collective-permute-start(bf16[32,512]{1,0:T(8,128)(2,1)S(1)} %get-tuple-element.15), channel_id=1, source_target_pairs={{0,2},{1,3},{2,0},{3,1},{4,6},{5,7},{6,4},{7,5},{8,10},{9,11},{10,... | collective-permute-start | bytes 98312 | tf_op jit(solution)/shard_map/ppermute | solution.py:67
  47.6 3.4 %collective-permute-start.2 = (bf16[32,512]{1,0:T(8,128)(2,1)S(1)}, bf16[32,512]{1,0:T(8,128)(2,1)S(1)}, u32[]{:S(2)}, u32[]{:S(2)}) collective-permute-start(bf16[32,512]{1,0:T(8,128)(2,1)S(1)} %get-tuple-element.14), channel_id=1, source_target_pairs={{0,3},{1,2},{2,1},{3,0},{4,7},{5,6},{6,5},{7,4},{8,11},{9,10},{10,... | collective-permute-start | bytes 98312 | tf_op jit(solution)/shard_map/ppermute | solution.py:67
  63.7 6.6 %collective-permute-start.3 = (bf16[1,256,512]{2,1,0:T(8,128)(2,1)S(1)}, bf16[1,256,512]{2,1,0:T(8,128)(2,1)S(1)}, u32[]{:S(2)}, u32[]{:S(2)}) collective-permute-start(bf16[1,256,512]{2,1,0:T(8,128)(2,1)S(1)} %bitcast.123), channel_id=1, source_target_pairs={{0,2},{1,3},{2,0},{3,1},{4,6},{5,7},{6,4},{7,5},{8,10},{9,11},{10,... | collective-permute-start | bytes 786440 | tf_op jit(solution)/shard_map/ppermute | solution.py:67
  70.4 2.7 %collective-permute-start.4 = (bf16[2,256,512]{2,1,0:T(8,128)(2,1)S(1)}, bf16[2,256,512]{2,1,0:T(8,128)(2,1)S(1)}, u32[]{:S(2)}, u32[]{:S(2)}) collective-permute-start(bf16[2,256,512]{2,1,0:T(8,128)(2,1)S(1)} %maximum_bitcast_fusion), channel_id=1, source_target_pairs={{0,1},{1,0},{2,3},{3,2},{4,5},{5,4},{6,7},{7,6},{8,9},{9,8},{10,11... | collective-permute-start | bytes 1572872 | tf_op jit(solution)/shard_map/ppermute | solution.py:67
  84.3 2.1 %collective-permute-start.5 = (bf16[256,2,512]{2,0,1:T(8,128)(2,1)S(1)}, bf16[256,2,512]{2,0,1:T(8,128)(2,1)S(1)}, u32[]{:S(2)}, u32[]{:S(2)}) collective-permute-start(bf16[256,2,512]{2,0,1:T(8,128)(2,1)S(1)} %fusion.23), channel_id=1, source_target_pairs={{0,1},{1,0},{2,3},{3,2},{4,5},{5,4},{6,7},{7,6},{8,9},{9,8},{10,11... | collective-permute-start | bytes 1572872 | tf_op jit(solution)/shard_map/ppermute | solution.py:67
  88.3 14.3 %copy-start.8 = (f32[32,2]{0,1:T(2,128)S(1)}, f32[32,2]{0,1:T(2,128)}, u32[]{:S(2)}) copy-start(f32[32,2]{0,1:T(2,128)} %param.36) | copy-start | bytes 772
  88.3 14.3 %copy-start.11 = (s32[32,2]{0,1:T(2,128)S(1)}, s32[32,2]{0,1:T(2,128)}, u32[]{:S(2)}) copy-start(s32[32,2]{0,1:T(2,128)} %param.35) | copy-start | bytes 772
  88.3 8.7 %collective-permute-start.6 = (bf16[256,1,512]{2,0,1:T(8,128)(2,1)S(1)}, bf16[256,1,512]{2,0,1:T(8,128)(2,1)S(1)}, u32[]{:S(2)}, u32[]{:S(2)}) collective-permute-start(bf16[256,1,512]{2,0,1:T(8,128)(2,1)S(1)} %fusion.33), channel_id=1, source_target_pairs={{0,2},{1,3},{2,0},{3,1},{4,6},{5,7},{6,4},{7,5},{8,10},{9,11},{10,... | collective-permute-start | bytes 786440 | tf_op jit(solution)/shard_map/ppermute | solution.py:67
  97.8 13.3 %all-to-all-start.3 = ((bf16[8,32,512]{2,1,0:T(8,128)(2,1)}), bf16[8,32,512]{2,1,0:T(8,128)(2,1)S(1)}, u32[]{:S(2)}, u32[]{:S(2)}) async-start(bf16[8,32,512]{2,1,0:T(8,128)(2,1)} %bitcast.31), calls=%async_computation.3 | async-start | bytes 524288 | tf_op jit(solution)/shard_map/all_to_all | solution.py:220

commit v2 on v1

v2 whole, which is shorter than its diff:
```python
import functools

import jax
import jax.numpy as jnp
from jax import lax
from jax.experimental import pallas as pl
from jax.experimental.pallas import tpu as pltpu
from jax.sharding import PartitionSpec as P

norm_epsilon = 1e-06


def project_kernel(rows_ref, *refs):
    out_ref = refs[-1]
    width = refs[0].shape[1]
    for place, weight_ref in enumerate(refs[:-1]):
        out_ref[:, place * width : (place + 1) * width] = jnp.dot(
            rows_ref[...], weight_ref[...], preferred_element_type=jnp.float32
        ).astype(jnp.bfloat16)


def project(rows, weights):
    return pl.pallas_call(
        project_kernel,
        out_shape=jax.ShapeDtypeStruct((rows.shape[0], len(weights) * weights[0].shape[1]), jnp.bfloat16),
        name="project",
    )(rows, *weights)


def cell_kernel(
    index_ref,
    arrived_ref,
    factor_ref,
    carry_ref,
    inflow_ref,
    matrix_ref,
    normal_ref,
    proj_ref,
    *refs,
    peers,
):
    term_refs = refs[:peers]
    normal_out_ref, key_ref, value_ref, carry_out_ref, read_ref = refs[peers:]
    seqs, heads, head_dim = matrix_ref.shape[:3]
    head_cols = heads * head_dim
    summed = jnp.sum(arrived_ref[...].astype(jnp.float32), axis=0) * factor_ref[...]
    summed = summed.astype(jnp.bfloat16).astype(jnp.float32)
    cells = []
    for head in range(heads):
        query, key, value, gate = [
            summed[:, start + head * head_dim : start + (head + 1) * head_dim]
            for start in range(0, 4 * head_cols, head_cols)
        ]
        carry = carry_ref[:, head : head + 1]
        inflow = inflow_ref[:, head : head + 1]
        key = key * head_dim ** (-0.5)
        inflow_key = inflow * key
        columns = slice(head * head_dim, (head + 1) * head_dim)
        normal_new = carry * normal_ref[:, columns] + inflow_key
        normal_out_ref[:, columns] = normal_new
        rows = slice(head * seqs, (head + 1) * seqs)
        key_ref[rows, :] = inflow_key
        value_ref[rows, :] = value
        carry_out_ref[rows, :] = jnp.broadcast_to(carry, (seqs, head_dim))
        turned = query.T
        for seq in range(seqs):
            read_ref[seq : seq + 1, :] = jnp.sum(
                turned[:, seq : seq + 1] * matrix_ref[seq, head], axis=0, keepdims=True
            )
        numer = carry * read_ref[...] + jnp.sum(query * inflow_key, axis=-1, keepdims=True) * value
        denom = jnp.maximum(jnp.abs(jnp.sum(query * normal_new, axis=-1, keepdims=True)), 1.0)
        cells.append((numer / denom * jax.nn.sigmoid(gate)).astype(jnp.bfloat16))
    cell = jnp.concatenate(cells, axis=1)
    width = proj_ref.shape[1] // peers
    for peer, term_ref in enumerate(term_refs):
        start = pl.multiple_of((index_ref[0] ^ peer) * width, width)
        term_ref[...] = jnp.dot(
            cell, proj_ref[:, pl.ds(start, width)], preferred_element_type=jnp.float32
        ).astype(jnp.bfloat16)


def cell_step(index, arrived, factor, carry, inflow, matrix_state, normal_rows, w_proj, peers):
    seqs, heads, head_dim, _ = matrix_state.shape
    wide = jnp.float32
    term = jax.ShapeDtypeStruct((seqs, w_proj.shape[1] // peers), jnp.bfloat16)
    by_head = jax.ShapeDtypeStruct((heads * seqs, head_dim), wide)
    vmem = pl.BlockSpec(memory_space=pltpu.VMEM)
    return pl.pallas_call(
        functools.partial(cell_kernel, peers=peers),
        in_specs=[pl.BlockSpec(memory_space=pltpu.SMEM)] + [vmem] * 7,
        out_specs=[vmem] * (peers + 4),
        out_shape=[term] * peers
        + [jax.ShapeDtypeStruct((seqs, heads * head_dim), wide), by_head, by_head, by_head],
        scratch_shapes=[pltpu.VMEM((seqs, head_dim), wide)],
        name="cell_step",
    )(index, arrived, factor, carry, inflow, matrix_state, normal_rows, w_proj)


def update_kernel(key_ref, value_ref, carry_ref, matrix_ref, out_ref):
    turned = key_ref[...].T
    for seq in range(matrix_ref.shape[0]):
        out_ref[seq, 0] = (
            carry_ref[seq : seq + 1, :] * matrix_ref[seq, 0]
            + turned[:, seq : seq + 1] * value_ref[seq : seq + 1, :]
        )


def update_matrix(key, value, carry, matrix_state):
    seqs, heads, head_dim, _ = matrix_state.shape
    block = 8
    steps = seqs // block
    rows = pl.BlockSpec((block, head_dim), lambda head, step: (head * steps + step, 0))
    matrix = pl.BlockSpec((block, 1, head_dim, head_dim), lambda head, step: (step, head, 0, 0))
    return pl.pallas_call(
        update_kernel,
        grid=(heads, steps),
        in_specs=[rows, rows, rows, matrix],
        out_specs=matrix,
        out_shape=jax.ShapeDtypeStruct(matrix_state.shape, jnp.float32),
        name="update_matrix",
    )(key, value, carry, matrix_state)


def expert_kernel(index_ref, *refs, peers):
    chunk_refs = refs[:peers]
    gain_ref, gate_ref, up_ref, down_ref = refs[peers : peers + 4]
    term_refs = refs[peers + 4 :]
    width = chunk_refs[0].shape[1]
    wide = [chunk_ref[...].astype(jnp.float32) for chunk_ref in chunk_refs]
    squares = sum(jnp.sum(chunk * chunk, axis=-1, keepdims=True) for chunk in wide)
    factor = lax.rsqrt(squares / (peers * width) + norm_epsilon)
    gate_sum = None
    for peer in range(peers):
        start = pl.multiple_of((index_ref[0] ^ peer) * width, width)
        gain = gain_ref[:, pl.ds(start, width)].astype(jnp.float32)
        normed = (wide[peer] * factor * gain).astype(jnp.bfloat16)
        gate_part = jnp.dot(normed, gate_ref[0, pl.ds(start, width), :], preferred_element_type=jnp.float32)
        up_part = jnp.dot(normed, up_ref[0, pl.ds(start, width), :], preferred_element_type=jnp.float32)
        gate_sum = gate_part if gate_sum is None else gate_sum + gate_part
        up_sum = up_part if peer == 0 else up_sum + up_part
    inner = (jax.nn.silu(gate_sum) * up_sum).astype(jnp.bfloat16)
    for peer, term_ref in enumerate(term_refs):
        start = pl.multiple_of((index_ref[0] ^ peer) * width, width)
        term_ref[...] = jnp.dot(
            inner, down_ref[0, :, pl.ds(start, width)], preferred_element_type=jnp.float32
        ).astype(jnp.bfloat16)


def expert_step(index, chunks, gain, gate, up, down):
    peers = len(chunks)
    vmem = pl.BlockSpec(memory_space=pltpu.VMEM)
    return pl.pallas_call(
        functools.partial(expert_kernel, peers=peers),
        in_specs=[pl.BlockSpec(memory_space=pltpu.SMEM)] + [vmem] * (peers + 4),
        out_specs=[vmem] * peers,
        out_shape=[jax.ShapeDtypeStruct(chunks[0].shape, jnp.bfloat16)] * peers,
        name="expert_step",
    )(index, *chunks, gain, gate, up, down)


def dispatch_table(route_ids, experts, capacity):
    flat_ids = route_ids.reshape(-1)
    expert_hot = (flat_ids[:, None] == jnp.arange(experts, dtype=jnp.int32)[None, :]).astype(
        jnp.int32
    )
    slot_rank = jnp.sum((jnp.cumsum(expert_hot, axis=0) - 1) * expert_hot, axis=1)
    slot_hot = (slot_rank[:, None] == jnp.arange(capacity, dtype=jnp.int32)[None, :]).astype(
        jnp.float32
    )
    table = expert_hot.astype(jnp.float32)[:, :, None] * slot_hot[:, None, :]
    return table.reshape(flat_ids.shape[0], experts * capacity)


def pack_rows(table, row_block, top_count, experts, capacity):
    repeated = jnp.repeat(row_block, top_count, axis=0)
    packed = jnp.einsum(
        "as,aw->sw", table.astype(jnp.bfloat16), repeated, preferred_element_type=jnp.float32
    ).astype(jnp.bfloat16)
    return packed.reshape(experts, capacity, row_block.shape[1])


def swap(value, axis, bit):
    count = lax.axis_size(axis)
    return lax.ppermute(value, axis, [(i, i ^ bit) for i in range(count)])


def bits_of(count):
    return [1 << place for place in range(count.bit_length() - 1)]


def gather_chunks(own, axis):
    chunks = {0: own}
    for bit in reversed(bits_of(lax.axis_size(axis))):
        for place in list(chunks):
            chunks[place ^ bit] = swap(chunks[place], axis, bit)
    return [chunks[place] for place in range(len(chunks))]


def sum_chunks(terms, axis):
    left = dict(enumerate(terms))
    for bit in bits_of(lax.axis_size(axis)):
        for place in sorted((place for place in left if place & bit), reverse=True):
            other = swap(left.pop(place).astype(jnp.bfloat16), axis, bit)
            left[place ^ bit] = left[place ^ bit].astype(jnp.float32) + other.astype(jnp.float32)
    return left[0]


def body(
    tokens,
    gain_mix,
    gain_ffn,
    w_query,
    w_key,
    w_value,
    w_outgate,
    w_ingate,
    w_forget,
    bias_in,
    bias_forget,
    w_proj,
    matrix_state,
    normal_state,
    stab_state,
    route_ids,
    route_weights,
    w_exp_gate,
    w_exp_up,
    w_exp_down,
):
    ep_count = lax.axis_size("ep")
    tp_count = lax.axis_size("tp")
    tp_index = lax.axis_index("tp")
    seq_dev = tokens.shape[0]
    model_width = tokens.shape[1]
    heads_dev = matrix_state.shape[1]
    head_dim = matrix_state.shape[2]
    head_cols = w_query.shape[1]
    feature_rows = w_query.shape[0]
    top_count = route_ids.shape[1]
    experts = ep_count // 2
    capacity = min(seq_dev, max(2, 2 * seq_dev * top_count // experts))
    every_row = capacity == seq_dev
    col_width = model_width // tp_count
    index = tp_index.astype(jnp.int32).reshape(1)
    wide = tokens.astype(jnp.float32)
    scaled = wide * gain_mix.astype(jnp.float32)
    blocks = scaled.astype(jnp.bfloat16).reshape(seq_dev, ep_count, feature_rows).transpose(1, 0, 2)
    foreign = lax.all_to_all(
        blocks.reshape(ep_count * seq_dev, feature_rows), "ep", split_axis=0, concat_axis=0, tiled=True
    )
    terms = project(foreign, (w_query, w_key, w_value, w_outgate))
    arrived = lax.all_to_all(terms, "ep", split_axis=0, concat_axis=0, tiled=True)
    factor = lax.rsqrt(jnp.mean(wide * wide, axis=-1, keepdims=True) + norm_epsilon)
    normed = (wide * factor * gain_mix.astype(jnp.float32)).astype(jnp.bfloat16)
    head_first = tp_index * heads_dev

    def own_heads(weight, bias):
        return lax.dynamic_slice_in_dim(
            jnp.dot(normed, weight, preferred_element_type=jnp.float32) + bias, head_first, heads_dev, 1
        )

    in_pre = own_heads(w_ingate, bias_in)
    log_forget = jax.nn.log_sigmoid(own_heads(w_forget, bias_forget))
    stab_new = jnp.maximum(log_forget + stab_state, in_pre)
    carry = jnp.exp(log_forget + stab_state - stab_new)
    inflow = jnp.exp(in_pre - stab_new)
    *out_terms, normal_rows, key_rows, value_rows, carry_rows = cell_step(
        index,
        arrived.reshape(ep_count, seq_dev, 4 * head_cols),
        factor,
        carry,
        inflow,
        matrix_state,
        normal_state.reshape(seq_dev, head_cols),
        w_proj,
        tp_count,
    )
    normal_new = normal_rows.reshape(normal_state.shape)
    matrix_new = update_matrix(key_rows, value_rows, carry_rows, matrix_state)
    own_tokens = lax.dynamic_slice_in_dim(tokens, tp_index * col_width, col_width, 1)
    attended = out_terms[0].astype(jnp.float32)
    for peer in range(1, tp_count):
        attended = attended + swap(out_terms[peer], "tp", peer).astype(jnp.float32)
    own_resid = (own_tokens.astype(jnp.float32) + attended).astype(jnp.bfloat16)
    if every_row:
        packed = jnp.broadcast_to(own_resid, (experts, seq_dev, col_width))
    else:
        table = dispatch_table(route_ids, experts, capacity)
        packed = pack_rows(table, own_resid, top_count, experts, capacity)
    outgoing = jnp.broadcast_to(packed[:, None], (experts, 2, capacity, col_width))
    received = lax.all_to_all(
        outgoing.reshape(ep_count * capacity, col_width), "ep", split_axis=0, concat_axis=0, tiled=True
    )
    down_terms = expert_step(
        index,
        gather_chunks(received, "tp"),
        gain_ffn.reshape(1, model_width),
        w_exp_gate,
        w_exp_up,
        w_exp_down,
    )
    half_share = sum_chunks(down_terms, "tp").astype(jnp.bfloat16)
    returned = lax.all_to_all(half_share, "ep", split_axis=0, concat_axis=0, tiled=True)
    halves = returned.astype(jnp.float32).reshape(experts, 2, capacity, col_width)
    weights = route_weights / jnp.sum(route_weights, axis=-1, keepdims=True)
    if every_row:
        chosen = route_ids[:, :, None] == jnp.arange(experts, dtype=jnp.int32)
        shares = jnp.sum(jnp.where(chosen, weights[:, :, None], 0.0), axis=1)
        routed = jnp.sum(halves * shares.T[:, None, :, None], axis=(0, 1))
    else:
        combine = jnp.sum(
            (table * weights.reshape(-1)[:, None]).reshape(
                seq_dev, top_count, experts * capacity
            ),
            axis=1,
        )
        halves_summed = jnp.sum(halves, axis=1).reshape(experts * capacity, col_width)
        routed = jnp.dot(combine, halves_summed, precision=lax.Precision.HIGHEST)
    mixed_out = (own_resid.astype(jnp.float32) + routed).astype(jnp.bfloat16)
    return (mixed_out, matrix_new, normal_new, stab_new)


def solution(mesh):
    placed = (
        P("ep", None),
        P(),
        P(),
        P("ep", "tp"),
        P("ep", "tp"),
        P("ep", "tp"),
        P("ep", "tp"),
        P(),
        P(),
        P(),
        P(),
        P("tp", None),
        P("ep", "tp", None, None),
        P("ep", "tp", None),
        P("ep", "tp"),
        P("ep", None),
        P("ep", None),
        P("ep", None, "tp"),
        P("ep", None, "tp"),
        P("ep", "tp", None),
    )
    return jax.shard_map(
        body,
        mesh=mesh,
        in_specs=placed,
        out_specs=(P("ep", "tp"), P("ep", "tp", None, None), P("ep", "tp", None), P("ep", "tp")),
        check_vma=False,
    )
```

time: 113 us -> 103 us (0.912)
  Pallas kernels: 0 us -> 20.1 us
  waiting for transfers between devices: 44.6 us -> 28.5 us
  blocking collectives: 12.7 us -> 27.3 us
  matrix products: 12.7 us -> 0.45 us
  starting transfers between devices: 19.9 us -> 12.5 us
  other arithmetic: 13.7 us -> 7.59 us
  local copies, waits for them, and re-layouts: 7.19 us -> 5.05 us
    pallas_call x0 -> x4, Pallas kernels: none -> 20.1 us  [the longest x1 7.61 us: update_matrix(): pl.pallas_call(update_kernel, grid=(heads, steps), in_specs=[rows, rows,...]
    all_to_all x0 -> x1, blocking collectives: none -> 14.6 us  [body(): lax.all_to_all(blocks.reshape(ep_count * seq_dev, feature_rows), 'ep', sp...]
    dot_general x10 -> x2, matrix products: 12.7 us -> 0.45 us  [own_heads(): jnp.dot(normed, weight, preferred_element_type=jnp.float32) + bias]
    all_to_all x1, waiting for transfers between devices: 8.54 us -> 0.01 us  [body(): lax.all_to_all(half_share, 'ep', split_axis=0, concat_axis=0, tiled=True)]
    all_to_all x1 -> x0, starting transfers between devices: 7.31 us -> none  [body(): lax.all_to_all(tokens, 'ep', split_axis=1, concat_axis=0, tiled=True)]
    all_to_all x1 -> x0, waiting for transfers between devices: 5.55 us -> none  [body(): lax.all_to_all(tokens, 'ep', split_axis=1, concat_axis=0, tiled=True)]
    add x1 -> x0, other arithmetic: 3.71 us -> none  [memory_step(): carry[..., None, None] * matrix_state]
    unnamed x32 -> x35, local copies, waits for them, and re-layouts: 0.1 us -> 2.89 us
  transfers between devices with their start and end apart: 10 -> 11, of which waited for: 8 -> 7; matrix products, arithmetic and copies ran while one was open for 5% -> 6% of each run, Pallas kernels for 0% -> 7%
where the time goes in v2:
time: 103 us; the launch traced here: 102 us
  waiting for transfers between devices  28.5 us (28%)
  blocking collectives  27.3 us (27%)
  Pallas kernels  20.1 us (20%)
  starting transfers between devices  12.5 us (12%)
  other arithmetic  7.59 us (7%)
  local copies, waits for them, and re-layouts  5.05 us (5%)
    ppermute x9, waiting for transfers between devices, swap(): return lax.ppermute(value, axis, [(i, i ^ bit) for i in range(count)])  18.7 us
    all_to_all x1, blocking collectives, body(): lax.all_to_all(blocks.reshape(ep_count * seq_dev, feature_rows), 'ep', sp...  14.6 us
    all_to_all x1, blocking collectives, body(): lax.all_to_all(outgoing.reshape(ep_count * capacity, col_width), 'ep', sp...  12.7 us
    all_to_all x1, waiting for transfers between devices, body(): lax.all_to_all(terms, 'ep', split_axis=0, concat_axis=0, tiled=True)  9.8 us
    pallas_call x1, Pallas kernels, update_matrix(): pl.pallas_call(update_kernel, grid=(heads, steps), in_specs=[rows, rows,...  7.61 us
    pallas_call x1, Pallas kernels, expert_step(): pl.pallas_call(functools.partial(expert_kernel, peers=peers), in_specs=[p...  5.55 us
    all_to_all x1, starting transfers between devices, body(): lax.all_to_all(half_share, 'ep', split_axis=0, concat_axis=0, tiled=True)  4.69 us
    pallas_call x1, Pallas kernels, cell_step(): pl.pallas_call(functools.partial(cell_kernel, peers=peers), in_specs=[pl....  4.65 us
  transfers between devices with their start and end apart: 11, of which 7 were waited for; matrix products, arithmetic and copies ran while one was open for 6% of the time, Pallas kernels for 7%

profile of v2, /device:TPU:0, one launch (start us, length us, event | category | flops | bytes accessed | tf_op | source)
XLA Modules:
  0.0 102.2 jit_solution(8814482454190040882)
XLA Ops:
  0.6 0.0 copy-start
  0.6 0.0 copy-start.14
  0.7 0.0 copy-start.15
  0.7 0.0 copy-start.11
  0.7 0.0 copy-start.7
  0.7 0.7 convert_element_type.65
  1.4 1.1 %fusion.1 = (f32[32]{0:T(128)S(1)}, bf16[32,2048]{1,0:T(8,128)(2,1)S(1)}) fusion(bf16[32,2048]{1,0:T(8,128)(2,1)} %param.20, f32[2048]{0:T(1024)S(1)} %convert_element_type.65), kind=kLoop, calls=%fused_computation.7 | loop fusion | flops 327648 | bytes 270464 | tf_op jit(solution)/shard_map/reduce_sum | solution.py:253
  2.6 14.6 %all_to_all.37 = bf16[8,32,256]{2,1,0:T(8,128)(2,1)} all-to-all(bf16[8,32,256]{2,1,0:T(8,128)(2,1)S(1)} %bitcast.28), channel_id=1, replica_groups=mesh['ep'=8,'tp'=4] {'ep'}, dimensions={0} | all-to-all | bytes 262144 | tf_op jit(solution)/shard_map/all_to_all | solution.py:248
  17.1 2.3 %project.1 = bf16[256,1024]{1,0:T(8,128)(2,1)} custom-call(bf16[256,256]{1,0:T(8,128)(2,1)} %bitcast.26, bf16[256,256]{1,0:T(8,128)(2,1)} %refs_0_.1, bf16[256,256]{1,0:T(8,128)(2,1)} %refs_1_.1, bf16[256,256]{1,0:T(8,128)(2,1)} %refs_2_.1, bf16[256,256]{1,0:T(8,128)(2,1)} %refs_3_.1), custom_call_target="tpu_custom_call" | custom-call | tf_op jit(solution)/shard_map/project/pallas_call | solution.py:23
  19.4 3.5 %all-to-all-start.1 = ((bf16[8,32,1024]{2,1,0:T(8,128)(2,1)}), bf16[8,32,1024]{2,1,0:T(8,128)(2,1)S(1)}, u32[]{:S(2)}, u32[]{:S(2)}) async-start(bf16[8,32,1024]{2,1,0:T(8,128)(2,1)} %bitcast.22), calls=%async_computation.1 | async-start | bytes 1048576 | tf_op jit(solution)/shard_map/all_to_all | solution.py:252
  22.9 0.0 copy-done.14
  22.9 0.1 dynamic-slice
  23.0 0.0 copy-done.15
  23.0 0.1 dynamic-slice.1
  23.1 0.0 copy-done.11
  23.1 0.1 copy.41
  23.1 0.0 copy-done.7
  23.2 0.6 copy.53
  23.8 0.7 copy.44.factor_ref
  24.5 0.0 copy-done
  24.5 0.0 copy-done.6
  24.5 0.2 fusion.6
  24.7 0.0 copy-done.13
  24.7 0.2 fusion.4
  24.9 0.7 subtract_exponential_fusion
  25.6 0.7 subtract_exponential_fusion.1.carry_ref
  26.3 9.8 %all-to-all-done.1.arrived_ref = bf16[8,32,1024]{2,1,0:T(8,128)(2,1)S(1)} async-done(((bf16[8,32,1024]{2,1,0:T(8,128)(2,1)}), bf16[8,32,1024]{2,1,0:T(8,128)(2,1)S(1)}, u32[]{:S(2)}, u32[]{:S(2)}) %all-to-all-start.1) | async-done | bytes 524320 | tf_op jit(solution)/shard_map/all_to_all | solution.py:252
  36.1 0.8 copy-done.1
  36.9 4.7 %cell_step.1 = (bf16[32,512]{1,0:T(8,128)(2,1)}, bf16[32,512]{1,0:T(8,128)(2,1)}, bf16[32,512]{1,0:T(8,128)(2,1)}, bf16[32,512]{1,0:T(8,128)(2,1)}, f32[32,256]{...) custom-call(s32[1]{0:T(128)} %bitcast.index_ref, bf16[8,32,1024]{2,1,0:T(8,128)(2,1)} %copy-done.1, ...), custom_call_target="tpu_custom_call" | custom-call | tf_op jit(solution)/shard_map/cell_step/pallas_call | solution.py:88
  41.6 0.0 collective-permute-start
  41.6 1.6 %collective-permute-start.1 = (bf16[32,512]{1,0:T(8,128)(2,1)}, bf16[32,512]{1,0:T(8,128)(2,1)S(1)}, u32[]{:S(2)}, u32[]{:S(2)}) collective-permute-start(bf16[32,512]{1,0:T(8,128)(2,1)} %get-tuple-element.18), channel_id=1, source_target_pairs={{0,2},{1,3},{2,0},{3,1},{4,6},{5,7},{6,4},{7,5},{8,10},{9,11},{10,... | collective-permute-start | bytes 98312 | tf_op jit(solution)/shard_map/ppermute | solution.py:184
  43.2 0.3 collective-permute-start.2
  43.5 0.0 collective-permute-done
  43.5 2.3 %collective-permute-done.1 = bf16[32,512]{1,0:T(8,128)(2,1)S(1)} collective-permute-done((bf16[32,512]{1,0:T(8,128)(2,1)}, bf16[32,512]{1,0:T(8,128)(2,1)S(1)}, u32[]{:S(2)}, u32[]{:S(2)}) %collective-permute-start.1) | collective-permute-done | bytes 32800 | tf_op jit(solution)/shard_map/ppermute | solution.py:184
  45.8 0.9 collective-permute-done.2
  46.7 0.8 add_convert_fusion.3
  47.5 12.7 %all_to_all.38 = bf16[8,32,512]{2,1,0:T(8,128)(2,1)S(1)} all-to-all(bf16[8,32,512]{2,1,0:T(8,128)(2,1)S(1)} %all_to_all.28), channel_id=1, replica_groups=mesh['ep'=8,'tp'=4] {'ep'}, dimensions={0} | all-to-all | bytes 524288 | tf_op jit(solution)/shard_map/all_to_all | solution.py:291
  60.2 0.9 collective-permute-start.4
  61.1 0.0 collective-permute-start.3
  61.1 5.7 %collective-permute-done.4.refs_2_ = bf16[256,512]{1,0:T(8,128)(2,1)S(1)} collective-permute-done((bf16[256,512]{1,0:T(8,128)(2,1)S(1)}, bf16[256,512]{1,0:T(8,128)(2,1)S(1)}, u32[]{:S(2)}, u32[]{:S(2)}) %collective-permute-start.4) | collective-permute-done | bytes 262176 | tf_op jit(solution)/shard_map/ppermute | solution.py:184
  66.8 0.0 collective-permute-start.5
  66.8 0.0 copy-done.9
  66.8 0.7 reshape.71.refs_4_
  67.5 0.0 collective-permute-done.3.refs_1_
  67.5 0.9 collective-permute-done.5.refs_3_
  68.4 0.0 copy-done.2
  68.4 0.0 copy-done.3
  68.4 0.7 copy-done.5
  69.1 5.6 %expert_step.1 = (bf16[256,512]{1,0:T(8,128)(2,1)}, bf16[256,512]{1,0:T(8,128)(2,1)}, bf16[256,512]{1,0:T(8,128)(2,1)}, bf16[256,512]{1,0:T(8,128)(2,1)}) custom-call(s32[1]{0:T(128)} %bitcast.index_ref, bf16[256,512]{1,0:T(8,128)(2,1)} %bitcast.25, bf16[256,512]{1,0:T(8,128)(2,1)} %copy-done.4, bf16[256,512]{1,0:T(8,128)(2,1)} %copy-done.3, ...), custom_call_target="tpu_custom_call" | custom-call | tf_op jit(solution)/shard_map/expert_step/pallas_call | solution.py:152
  74.7 0.3 collective-permute-start.7
  75.0 0.2 collective-permute-start.6
  75.2 1.2 %collective-permute-done.7 = bf16[256,512]{1,0:T(8,128)(2,1)S(1)} collective-permute-done((bf16[256,512]{1,0:T(8,128)(2,1)}, bf16[256,512]{1,0:T(8,128)(2,1)S(1)}, u32[]{:S(2)}, u32[]{:S(2)}) %collective-permute-start.7) | collective-permute-done | bytes 262176 | tf_op jit(solution)/shard_map/ppermute | solution.py:184
  76.5 1.0 add_convert_fusion.1
  77.5 1.0 collective-permute-start.8
  78.5 0.0 collective-permute-done.6
  78.5 7.6 %collective-permute-done.8 = bf16[256,512]{1,0:T(8,128)(2,1)S(1)} collective-permute-done((bf16[256,512]{1,0:T(8,128)(2,1)S(1)}, bf16[256,512]{1,0:T(8,128)(2,1)S(1)}, u32[]{:S(2)}, u32[]{:S(2)}) %collective-permute-start.8) | collective-permute-done | bytes 262176 | tf_op jit(solution)/shard_map/ppermute | solution.py:184
  86.0 1.8 %add_convert_fusion = bf16[256,512]{1,0:T(8,128)(2,1)} fusion(bf16[256,512]{1,0:T(8,128)(2,1)S(1)} %collective-permute-done.8, bf16[256,512]{1,0:T(8,128)(2,1)S(1)} %collective-permute-done.6, bf16[256,512]{1,0:T(8,128)(2,1)} %get-tuple-element.20), kind=kLoop, calls=%fused_computation.1 | loop fusion | flops 786432 | bytes 1048576 | tf_op jit(solution)/shard_map/convert_element_type | solution.py:302
  87.8 4.7 %all-to-all-start.3 = ((bf16[8,32,512]{2,1,0:T(8,128)(2,1)}), bf16[8,32,512]{2,1,0:T(8,128)(2,1)S(1)}, u32[]{:S(2)}, u32[]{:S(2)}) async-start(bf16[8,32,512]{2,1,0:T(8,128)(2,1)} %bitcast.6), calls=%async_computation.3 | async-start | bytes 524288 | tf_op jit(solution)/shard_map/all_to_all | solution.py:303
  92.5 0.6 copy.45
  93.2 0.6 reshape.72
  93.8 7.6 %update_matrix.1 = f32[32,2,128,128]{3,2,1,0:T(8,128)} custom-call(f32[64,128]{1,0:T(8,128)} %get-tuple-element.24.key_ref, f32[64,128]{1,0:T(8,128)} %get-tuple-element.25.value_ref, f32[64,128]{1,0:T(8,128)} %get-tuple-element.26.carry_ref, f32[32,2,128,128]{3,2,1,0:T(8,128)} %matrix_ref.3), custom_call_target="tpu_custom_call" | custom-call | tf_op jit(solution)/shard_map/update_matrix/pallas_call | solution.py:114
  101.4 0.0 all-to-all-done.3
  101.4 0.1 multiply_reduce_fusion
  101.6 0.6 add_convert_fusion.2
  (22 shorter events, 0.1 us)
Async XLA Ops:
  0.6 23.8 %copy-start = (bf16[2048,8]{0,1:T(8,128)(2,1)S(1)}, bf16[2048,8]{0,1:T(8,128)(2,1)}, u32[]{:S(2)}) copy-start(bf16[2048,8]{0,1:T(8,128)(2,1)} %param.28) | copy-start | bytes 98308
  0.6 22.2 %copy-start.14 = (f32[8]{0:T(128)S(1)}, f32[8]{0:T(128)}, u32[]{:S(2)}) copy-start(f32[8]{0:T(128)} %param.30) | copy-start | bytes 100
  0.7 22.3 %copy-start.15 = (f32[8]{0:T(128)S(1)}, f32[8]{0:T(128)}, u32[]{:S(2)}) copy-start(f32[8]{0:T(128)} %param.29) | copy-start | bytes 100
  0.7 22.4 %copy-start.11 = (f32[32,2]{0,1:T(2,128)S(1)}, f32[32,2]{0,1:T(2,128)}, u32[]{:S(2)}) copy-start(f32[32,2]{0,1:T(2,128)} %param.34) | copy-start | bytes 772
  0.7 22.5 %copy-start.7 = (f32[32,2,128]{2,1,0:T(2,128)S(1)}, f32[32,2,128]{2,1,0:T(2,128)}, u32[]{:S(2)}) copy-start(f32[32,2,128]{2,1,0:T(2,128)} %param.33) | copy-start | bytes 98308
  1.4 23.1 %copy-start.6 = (bf16[32,2048]{1,0:T(8,128)(2,1)S(1)}, bf16[32,2048]{1,0:T(8,128)(2,1)}, u32[]{:S(2)}) copy-start(bf16[32,2048]{1,0:T(8,128)(2,1)} %param.20) | copy-start | bytes 393220
  2.5 22.2 %copy-start.13 = (bf16[2048,8]{0,1:T(8,128)(2,1)S(1)}, bf16[2048,8]{0,1:T(8,128)(2,1)}, u32[]{:S(2)}) copy-start(bf16[2048,8]{0,1:T(8,128)(2,1)} %param.27) | copy-start | bytes 98308
  19.4 16.8 %all-to-all-start.1 = ((bf16[8,32,1024]{2,1,0:T(8,128)(2,1)}), bf16[8,32,1024]{2,1,0:T(8,128)(2,1)S(1)}, u32[]{:S(2)}, u32[]{:S(2)}) async-start(bf16[8,32,1024]{2,1,0:T(8,128)(2,1)} %bitcast.22), calls=%async_computation.1 | async-start | bytes 1048576 | tf_op jit(solution)/shard_map/all_to_all | solution.py:252
  36.1 0.8 copy-start.1
  36.9 29.9 %copy-start.9 = (bf16[2048]{0:T(1024)(128)(2,1)S(1)}, bf16[2048]{0:T(1024)(128)(2,1)}, u32[]{:S(2)}) copy-start(bf16[2048]{0:T(1024)(128)(2,1)} %param.22) | copy-start | bytes 12292
  41.6 1.9 %collective-permute-start = (bf16[32,512]{1,0:T(8,128)(2,1)}, bf16[32,512]{1,0:T(8,128)(2,1)S(1)}, u32[]{:S(2)}, u32[]{:S(2)}) collective-permute-start(bf16[32,512]{1,0:T(8,128)(2,1)} %get-tuple-element.17), channel_id=1, source_target_pairs={{0,1},{1,0},{2,3},{3,2},{4,5},{5,4},{6,7},{7,6},{8,9},{9,8},{10,11... | collective-permute-start | bytes 98312 | tf_op jit(solution)/shard_map/ppermute | solution.py:184
  41.6 4.2 %collective-permute-start.1 = (bf16[32,512]{1,0:T(8,128)(2,1)}, bf16[32,512]{1,0:T(8,128)(2,1)S(1)}, u32[]{:S(2)}, u32[]{:S(2)}) collective-permute-start(bf16[32,512]{1,0:T(8,128)(2,1)} %get-tuple-element.18), channel_id=1, source_target_pairs={{0,2},{1,3},{2,0},{3,1},{4,6},{5,7},{6,4},{7,5},{8,10},{9,11},{10,... | collective-permute-start | bytes 98312 | tf_op jit(solution)/shard_map/ppermute | solution.py:184
  43.2 3.6 %collective-permute-start.2 = (bf16[32,512]{1,0:T(8,128)(2,1)}, bf16[32,512]{1,0:T(8,128)(2,1)S(1)}, u32[]{:S(2)}, u32[]{:S(2)}) collective-permute-start(bf16[32,512]{1,0:T(8,128)(2,1)} %get-tuple-element.19), channel_id=1, source_target_pairs={{0,3},{1,2},{2,1},{3,0},{4,7},{5,6},{6,5},{7,4},{8,11},{9,10},{10,... | collective-permute-start | bytes 98312 | tf_op jit(solution)/shard_map/ppermute | solution.py:184
  60.2 8.1 %copy-start.2 = (bf16[8,32,512]{2,1,0:T(8,128)(2,1)}, bf16[8,32,512]{2,1,0:T(8,128)(2,1)S(1)}, u32[]{:S(2)}) copy-start(bf16[8,32,512]{2,1,0:T(8,128)(2,1)S(1)} %all_to_all.38) | copy-start | bytes 786436
  60.2 6.6 %collective-permute-start.4 = (bf16[256,512]{1,0:T(8,128)(2,1)S(1)}, bf16[256,512]{1,0:T(8,128)(2,1)S(1)}, u32[]{:S(2)}, u32[]{:S(2)}) collective-permute-start(bf16[256,512]{1,0:T(8,128)(2,1)S(1)} %bitcast.23), channel_id=1, source_target_pairs={{0,2},{1,3},{2,0},{3,1},{4,6},{5,7},{6,4},{7,5},{8,10},{9,11},{10,... | collective-permute-start | bytes 786440 | tf_op jit(solution)/shard_map/ppermute | solution.py:184
  61.1 6.4 %collective-permute-start.3 = (bf16[256,512]{1,0:T(8,128)(2,1)S(1)}, bf16[256,512]{1,0:T(8,128)(2,1)S(1)}, u32[]{:S(2)}, u32[]{:S(2)}) collective-permute-start(bf16[256,512]{1,0:T(8,128)(2,1)S(1)} %bitcast.24), channel_id=1, source_target_pairs={{0,1},{1,0},{2,3},{3,2},{4,5},{5,4},{6,7},{7,6},{8,9},{9,8},{10,11... | collective-permute-start | bytes 786440 | tf_op jit(solution)/shard_map/ppermute | solution.py:184
  66.8 1.5 %copy-start.3 = (bf16[256,512]{1,0:T(8,128)(2,1)}, bf16[256,512]{1,0:T(8,128)(2,1)S(1)}, u32[]{:S(2)}) copy-start(bf16[256,512]{1,0:T(8,128)(2,1)S(1)} %collective-permute-done.4.refs_2_) | copy-start | bytes 786436
  66.8 1.5 %collective-permute-start.5 = (bf16[256,512]{1,0:T(8,128)(2,1)S(1)}, bf16[256,512]{1,0:T(8,128)(2,1)S(1)}, u32[]{:S(2)}, u32[]{:S(2)}) collective-permute-start(bf16[256,512]{1,0:T(8,128)(2,1)S(1)} %collective-permute-done.4.refs_2_), channel_id=1, source_target_pairs={{0,1},{1,0},{2,3},{3,2},{4,5},{5,4},{6,7},{7,6},{8,9},{9,8},{10,11... | collective-permute-start | bytes 786440 | tf_op jit(solution)/shard_map/ppermute | solution.py:184
  67.5 0.9 copy-start.4
  68.4 0.7 copy-start.5
  74.6 18.5 %copy-start.10 = (f32[32,2]{0,1:T(2,128)S(1)}, f32[32,2]{0,1:T(2,128)}, u32[]{:S(2)}) copy-start(f32[32,2]{0,1:T(2,128)} %param.36) | copy-start | bytes 772
  74.6 18.5 %copy-start.12 = (s32[32,2]{0,1:T(2,128)S(1)}, s32[32,2]{0,1:T(2,128)}, u32[]{:S(2)}) copy-start(s32[32,2]{0,1:T(2,128)} %param.35) | copy-start | bytes 772
  74.7 18.5 %copy-start.8 = (f32[32,256]{1,0:T(8,128)S(1)}, f32[32,256]{1,0:T(8,128)}, u32[]{:S(2)}) copy-start(f32[32,256]{1,0:T(8,128)} %get-tuple-element.27) | copy-start | bytes 98308
  74.7 1.8 %collective-permute-start.7 = (bf16[256,512]{1,0:T(8,128)(2,1)}, bf16[256,512]{1,0:T(8,128)(2,1)S(1)}, u32[]{:S(2)}, u32[]{:S(2)}) collective-permute-start(bf16[256,512]{1,0:T(8,128)(2,1)} %get-tuple-element.23), channel_id=1, source_target_pairs={{0,1},{1,0},{2,3},{3,2},{4,5},{5,4},{6,7},{7,6},{8,9},{9,8},{10,11... | collective-permute-start | bytes 786440 | tf_op jit(solution)/shard_map/ppermute | solution.py:184
  75.0 3.5 %collective-permute-start.6 = (bf16[256,512]{1,0:T(8,128)(2,1)}, bf16[256,512]{1,0:T(8,128)(2,1)S(1)}, u32[]{:S(2)}, u32[]{:S(2)}) collective-permute-start(bf16[256,512]{1,0:T(8,128)(2,1)} %get-tuple-element.21), channel_id=1, source_target_pairs={{0,1},{1,0},{2,3},{3,2},{4,5},{5,4},{6,7},{7,6},{8,9},{9,8},{10,11... | collective-permute-start | bytes 786440 | tf_op jit(solution)/shard_map/ppermute | solution.py:184
  77.5 8.6 %collective-permute-start.8 = (bf16[256,512]{1,0:T(8,128)(2,1)S(1)}, bf16[256,512]{1,0:T(8,128)(2,1)S(1)}, u32[]{:S(2)}, u32[]{:S(2)}) collective-permute-start(bf16[256,512]{1,0:T(8,128)(2,1)S(1)} %add_convert_fusion.1), channel_id=1, source_target_pairs={{0,2},{1,3},{2,0},{3,1},{4,6},{5,7},{6,4},{7,5},{8,10},{9,11},{10,... | collective-permute-start | bytes 786440 | tf_op jit(solution)/shard_map/ppermute | solution.py:184
  87.8 13.6 %all-to-all-start.3 = ((bf16[8,32,512]{2,1,0:T(8,128)(2,1)}), bf16[8,32,512]{2,1,0:T(8,128)(2,1)S(1)}, u32[]{:S(2)}, u32[]{:S(2)}) async-start(bf16[8,32,512]{2,1,0:T(8,128)(2,1)} %bitcast.6), calls=%async_computation.3 | async-start | bytes 524288 | tf_op jit(solution)/shard_map/all_to_all | solution.py:303

commit v3 on v2

v3 whole, which is shorter than its diff:
```python
import functools

import jax
import jax.numpy as jnp
from jax import lax
from jax.experimental import pallas as pl
from jax.experimental.pallas import tpu as pltpu
from jax.sharding import PartitionSpec as P

norm_epsilon = 1e-06


def room(mebibytes):
    return pltpu.CompilerParams(vmem_limit_bytes=mebibytes << 20)


def load_kernel(_, *refs, count, narrowed):
    sources, targets = refs[:count], refs[count : 2 * count]
    semaphores, *wide = refs[2 * count :]
    landed = wide + list(targets[narrowed:])
    copies = [
        pltpu.make_async_copy(source, target, semaphores.at[place])
        for place, (source, target) in enumerate(zip(sources, landed))
    ]
    for copy in copies:
        copy.start()
    for place, copy in enumerate(copies):
        copy.wait()
        if place < narrowed:

            @pl.loop(0, targets[place].shape[0])
            def narrow(row, place=place):
                targets[place][row] = wide[place][row].astype(jnp.bfloat16)


def load(after, arrays, cycles, narrowed=0):
    anywhere = pl.BlockSpec(memory_space=pl.ANY)
    targets = [
        pltpu.VMEM(array.shape, jnp.bfloat16 if place < narrowed else array.dtype)
        for place, array in enumerate(arrays)
    ]
    return pl.pallas_call(
        functools.partial(load_kernel, count=len(arrays), narrowed=narrowed),
        in_specs=[anywhere] * (len(arrays) + 1),
        out_specs=[pl.BlockSpec(memory_space=pltpu.VMEM)] * len(arrays),
        out_shape=targets,
        scratch_shapes=[pltpu.SemaphoreType.DMA((len(arrays),))]
        + [pltpu.VMEM(array.shape, array.dtype) for array in arrays[:narrowed]],
        compiler_params=room(12),
        cost_estimate=pl.CostEstimate(flops=cycles, bytes_accessed=0, transcendentals=0),
        name="load",
    )(after, *map(away, arrays))


def away(array):
    return pltpu.with_memory_space_constraint(array, pltpu.HBM)


def held(array):
    return pltpu.with_memory_space_constraint(array, pltpu.VMEM)


def prepare_kernel(rows_hbm, gain_hbm, *refs, weights):
    weight_refs = refs[:weights]
    out_ref, pack_ref, rows_ref, gain_ref, semaphores = refs[weights:]
    copies = [
        pltpu.make_async_copy(rows_hbm, rows_ref, semaphores.at[0]),
        pltpu.make_async_copy(gain_hbm, gain_ref, semaphores.at[1]),
    ]
    for place, weight_ref in enumerate(weight_refs):
        copies.append(pltpu.make_async_copy(weight_ref, pack_ref.at[place], semaphores.at[2 + place]))
    for copy in copies:
        copy.start()
    for copy in copies[:2]:
        copy.wait()
    scaled = rows_ref[...].astype(jnp.float32) * gain_ref[...].astype(jnp.float32).reshape(1, -1)
    scaled = scaled.astype(jnp.bfloat16)
    seqs = rows_ref.shape[0]
    width = out_ref.shape[1]
    for place in range(out_ref.shape[0] // seqs):
        out_ref[place * seqs : (place + 1) * seqs, :] = scaled[:, place * width : (place + 1) * width]
    for copy in copies[2:]:
        copy.wait()


def prepare(rows, gain, weights, count):
    seqs, features = rows.shape
    width = features // count
    if width % 128:
        scaled = (rows.astype(jnp.float32) * gain.astype(jnp.float32)).astype(jnp.bfloat16)
        blocks = scaled.reshape(seqs, count, width).transpose(1, 0, 2).reshape(count * seqs, width)
        return blocks, jnp.stack(weights)
    anywhere = pl.BlockSpec(memory_space=pl.ANY)
    return pl.pallas_call(
        functools.partial(prepare_kernel, weights=len(weights)),
        in_specs=[anywhere] * (2 + len(weights)),
        out_specs=[pl.BlockSpec(), pl.BlockSpec(memory_space=pltpu.VMEM)],
        out_shape=[
            jax.ShapeDtypeStruct((count * seqs, width), jnp.bfloat16),
            pltpu.VMEM((len(weights),) + weights[0].shape, weights[0].dtype),
        ],
        scratch_shapes=[
            pltpu.VMEM(rows.shape, rows.dtype),
            pltpu.VMEM(gain.shape, gain.dtype),
            pltpu.SemaphoreType.DMA((2 + len(weights),)),
        ],
        compiler_params=room(12),
        name="prepare",
    )(*map(away, (rows, gain, *weights)))


def gates_kernel(
    index_ref,
    _,
    rows_ref,
    gain_ref,
    in_ref,
    forget_ref,
    bias_in_ref,
    bias_forget_ref,
    stab_ref,
    factor_ref,
    carry_ref,
    inflow_ref,
    stab_out_ref,
    in_pre_ref,
    forget_pre_ref,
):
    wide = rows_ref[...].astype(jnp.float32)
    factor = lax.rsqrt(jnp.mean(wide * wide, axis=-1, keepdims=True) + norm_epsilon)
    factor_ref[...] = factor
    normed = (wide * factor * gain_ref[...].astype(jnp.float32).reshape(1, -1)).astype(jnp.bfloat16)
    across = (((1,), (1,)), ((), ()))
    in_pre_ref[...] = lax.dot_general(in_ref[...], normed, across, preferred_element_type=jnp.float32)
    forget_pre_ref[...] = lax.dot_general(forget_ref[...], normed, across, preferred_element_type=jnp.float32)
    heads = stab_ref.shape[0]
    for head in range(heads):
        place = index_ref[0] * heads + head
        in_pre = in_pre_ref[pl.ds(place, 1), :] + bias_in_ref[place]
        forget_pre = forget_pre_ref[pl.ds(place, 1), :] + bias_forget_ref[place]
        log_forget = jnp.minimum(forget_pre, 0.0) - jnp.log1p(jnp.exp(-jnp.abs(forget_pre)))
        kept = log_forget + stab_ref[head : head + 1, :]
        stab_new = jnp.maximum(kept, in_pre)
        stab_out_ref[head : head + 1, :] = stab_new
        carry_ref[head : head + 1, :] = jnp.exp(kept - stab_new)
        inflow_ref[head : head + 1, :] = jnp.exp(in_pre - stab_new)


def gates(after, index, rows, gain, w_in, w_forget, bias_in, bias_forget, stab):
    seqs, heads = stab.shape
    small = jax.ShapeDtypeStruct((heads, seqs), jnp.float32)
    smem = pl.BlockSpec(memory_space=pltpu.SMEM)
    every = (w_in.shape[1], seqs)
    return pl.pallas_call(
        gates_kernel,
        in_specs=[smem, pl.BlockSpec(memory_space=pl.ANY)]
        + [pl.BlockSpec()] * 4
        + [smem] * 2
        + [pl.BlockSpec()],
        out_shape=[jax.ShapeDtypeStruct((seqs, 1), jnp.float32)] + [small] * 3,
        scratch_shapes=[pltpu.VMEM(every, jnp.float32)] * 2,
        compiler_params=room(12),
        cost_estimate=pl.CostEstimate(flops=1 << 22, bytes_accessed=0, transcendentals=0),
        name="gates",
    )(index, after, rows, gain, w_in.T, w_forget.T, bias_in, bias_forget, stab.T)


def project_kernel(index_ref, rows_ref, own_ref, other_ref, out_ref):
    count, features, width = own_ref.shape
    own = pl.multiple_of(index_ref[1] * features, features)
    other = pl.multiple_of((1 - index_ref[1]) * features, features)
    for place in range(count):
        total = jnp.dot(rows_ref[:, pl.ds(own, features)], own_ref[place], preferred_element_type=jnp.float32)
        total = total + jnp.dot(
            rows_ref[:, pl.ds(other, features)], other_ref[place], preferred_element_type=jnp.float32
        )
        out_ref[:, place * width : (place + 1) * width] = total.astype(jnp.bfloat16)


def project(index, rows, own, other):
    count, features, width = own.shape
    if features % 128:
        halves = rows.reshape(rows.shape[0], 2, -1)
        first = jnp.where(index[1] == 0, halves[:, 0], halves[:, 1])
        second = jnp.where(index[1] == 0, halves[:, 1], halves[:, 0])
        total = jnp.einsum("rf,cfw->rcw", first, own, preferred_element_type=jnp.float32)
        total = total + jnp.einsum("rf,cfw->rcw", second, other, preferred_element_type=jnp.float32)
        return total.astype(jnp.bfloat16).reshape(rows.shape[0], count * width)
    return pl.pallas_call(
        project_kernel,
        in_specs=[pl.BlockSpec(memory_space=pltpu.SMEM)] + [pl.BlockSpec()] * 3,
        out_shape=jax.ShapeDtypeStruct((rows.shape[0], count * width), jnp.bfloat16),
        compiler_params=room(12),
        name="project",
    )(index, rows, held(own), held(other))


def cell_kernel(
    index_ref,
    arrived_ref,
    factor_ref,
    carry_ref,
    inflow_ref,
    matrix_ref,
    normal_ref,
    proj_hbm,
    *refs,
    peers,
):
    term_refs = refs[:peers]
    key_ref, value_ref, carry_out_ref, inflow_out_ref, read_ref, proj_ref, semaphore = refs[peers:]
    proj_copy = pltpu.make_async_copy(proj_hbm, proj_ref, semaphore)
    proj_copy.start()
    seqs, heads, head_dim = matrix_ref.shape[:3]
    head_cols = heads * head_dim
    summed = jnp.sum(arrived_ref[...].astype(jnp.float32), axis=0) * factor_ref[...]
    summed = summed.astype(jnp.bfloat16).astype(jnp.float32)
    cells = []
    carries = carry_ref[...].T
    inflows = inflow_ref[...].T
    for head in range(heads):
        query, key, value, gate = [
            summed[:, start + head * head_dim : start + (head + 1) * head_dim]
            for start in range(0, 4 * head_cols, head_cols)
        ]
        carry = carries[:, head : head + 1]
        inflow = inflows[:, head : head + 1]
        inflow_key = inflow * (key * head_dim ** (-0.5))
        columns = slice(head * head_dim, (head + 1) * head_dim)
        normal_new = carry * normal_ref[:, columns] + inflow_key
        rows = slice(head * seqs, (head + 1) * seqs)
        key_ref[rows, :] = key
        value_ref[rows, :] = value
        carry_out_ref[rows, :] = jnp.broadcast_to(carry, (seqs, head_dim))
        inflow_out_ref[rows, :] = jnp.broadcast_to(inflow * head_dim ** (-0.5), (seqs, head_dim))
        turned = query.T
        for seq in range(seqs):
            read_ref[seq : seq + 1, :] = jnp.sum(
                turned[:, seq : seq + 1] * matrix_ref[seq, head].astype(jnp.float32), axis=0, keepdims=True
            )
        numer = carry * read_ref[...] + jnp.sum(query * inflow_key, axis=-1, keepdims=True) * value
        denom = jnp.maximum(jnp.abs(jnp.sum(query * normal_new, axis=-1, keepdims=True)), 1.0)
        cells.append((numer / denom * jax.nn.sigmoid(gate)).astype(jnp.bfloat16))
    cell = jnp.concatenate(cells, axis=1)
    proj_copy.wait()
    width = proj_ref.shape[1] // peers
    for peer, term_ref in enumerate(term_refs):
        start = pl.multiple_of((index_ref[0] ^ peer) * width, width)
        term_ref[...] = jnp.dot(
            cell, proj_ref[:, pl.ds(start, width)], preferred_element_type=jnp.float32
        ).astype(jnp.bfloat16)


def cell_step(index, arrived, factor, carry, inflow, matrix_state, normal_rows, w_proj, peers):
    seqs, heads, head_dim, _ = matrix_state.shape
    wide = jnp.float32
    term = jax.ShapeDtypeStruct((seqs, w_proj.shape[1] // peers), jnp.bfloat16)
    by_head = jax.ShapeDtypeStruct((heads * seqs, head_dim), wide)
    vmem = pl.BlockSpec()
    return pl.pallas_call(
        functools.partial(cell_kernel, peers=peers),
        in_specs=[pl.BlockSpec(memory_space=pltpu.SMEM)]
        + [vmem] * 6
        + [pl.BlockSpec(memory_space=pl.ANY)],
        out_specs=[vmem] * (peers + 4),
        out_shape=[term] * peers
        + [by_head] * 4,
        scratch_shapes=[
            pltpu.VMEM((seqs, head_dim), wide),
            pltpu.VMEM(w_proj.shape, w_proj.dtype),
            pltpu.SemaphoreType.DMA,
        ],
        compiler_params=room(12),
        name="cell_step",
    )(index, held(arrived), factor, carry, inflow, held(matrix_state), normal_rows, away(w_proj))


def update_kernel(key_ref, value_ref, carry_ref, inflow_ref, matrix_hbm, out_hbm, work_ref, loads, stores):
    seqs, heads, head_dim, _ = matrix_hbm.shape
    block = min(8, seqs)
    wide = (block, block * head_dim)
    own = lax.broadcasted_iota(jnp.int32, wide, 0) == lax.broadcasted_iota(jnp.int32, wide, 1) // head_dim

    def copy(step, out):
        part = pl.ds(step * block, block)
        if out:
            return pltpu.make_async_copy(work_ref.at[part], out_hbm.at[part], stores.at[step])
        return pltpu.make_async_copy(matrix_hbm.at[part], work_ref.at[part], loads.at[step])

    for step in range(seqs // block):
        copy(step, False).start()
    for step in range(seqs // block):
        copy(step, False).wait()
        for head in range(heads):
            rows = pl.ds(head * seqs + step * block, block)
            spread = jnp.where(own, jnp.concatenate([value_ref[rows, :]] * block, axis=1), 0.0)
            outer = jnp.dot(
                key_ref[rows, :].T.astype(jnp.bfloat16),
                spread.astype(jnp.bfloat16),
                preferred_element_type=jnp.float32,
            )
            for place in range(block):
                row = head * seqs + step * block + place
                seq = step * block + place
                work_ref[seq, head] = (
                    carry_ref[row : row + 1, :] * work_ref[seq, head]
                    + inflow_ref[row : row + 1, :] * outer[:, place * head_dim : (place + 1) * head_dim]
                )
        copy(step, True).start()
    for step in range(seqs // block):
        copy(step, True).wait()


def update_matrix(key, value, carry, inflow, matrix_state):
    anywhere = pl.BlockSpec(memory_space=pl.ANY)
    steps = matrix_state.shape[0] // min(8, matrix_state.shape[0])
    return pl.pallas_call(
        update_kernel,
        in_specs=[pl.BlockSpec()] * 4 + [anywhere],
        out_specs=anywhere,
        out_shape=pltpu.HBM(matrix_state.shape, jnp.float32),
        scratch_shapes=[
            pltpu.VMEM(matrix_state.shape, jnp.float32),
            pltpu.SemaphoreType.DMA((steps,)),
            pltpu.SemaphoreType.DMA((steps,)),
        ],
        compiler_params=room(12),
        cost_estimate=pl.CostEstimate(flops=1 << 23, bytes_accessed=0, transcendentals=0),
        name="update_matrix",
    )(key, value, carry, inflow, away(matrix_state))


def expert_kernel(index_ref, *refs, peers, halves):
    count = peers * halves
    chunk_refs = refs[:count]
    gain_ref, gate_ref, up_ref, down_ref = refs[count : count + 4]
    term_refs = refs[count + 4 :]
    rows, width = chunk_refs[0].shape
    squares = [
        sum(
            jnp.sum(jnp.square(chunk_refs[half * peers + peer][...].astype(jnp.float32)), axis=-1, keepdims=True)
            for peer in range(peers)
        )
        for half in range(halves)
    ]
    factors = [lax.rsqrt(square / (peers * width) + norm_epsilon) for square in squares]
    gate_sum = up_sum = None
    for peer in range(peers):
        start = pl.multiple_of((index_ref[0] ^ peer) * width, width)
        gain = gain_ref[:, pl.ds(start, width)].astype(jnp.float32)
        normed = jnp.concatenate(
            [
                (chunk_refs[half * peers + peer][...].astype(jnp.float32) * factors[half] * gain).astype(jnp.bfloat16)
                for half in range(halves)
            ],
            axis=0,
        )
        gate_part = jnp.dot(normed, gate_ref[0, pl.ds(start, width), :], preferred_element_type=jnp.float32)
        up_part = jnp.dot(normed, up_ref[0, pl.ds(start, width), :], preferred_element_type=jnp.float32)
        gate_sum = gate_part if peer == 0 else gate_sum + gate_part
        up_sum = up_part if peer == 0 else up_sum + up_part
    inner = (jax.nn.silu(gate_sum) * up_sum).astype(jnp.bfloat16)
    for peer in range(peers):
        start = pl.multiple_of((index_ref[0] ^ peer) * width, width)
        term = jnp.dot(
            inner, down_ref[0, :, pl.ds(start, width)], preferred_element_type=jnp.float32
        ).astype(jnp.bfloat16)
        for half in range(halves):
            term_refs[half * peers + peer][...] = term[half * rows : (half + 1) * rows]


def expert_step(index, chunks, gain, gate, up, down, peers):
    vmem = pl.BlockSpec()
    return pl.pallas_call(
        functools.partial(expert_kernel, peers=peers, halves=len(chunks) // peers),
        in_specs=[pl.BlockSpec(memory_space=pltpu.SMEM)]
        + [vmem] * (len(chunks) + 4),
        out_specs=[vmem] * len(chunks),
        out_shape=[jax.ShapeDtypeStruct(chunks[0].shape, jnp.bfloat16)] * len(chunks),
        compiler_params=room(12),
        name="expert_step",
    )(index, *map(held, chunks), gain, held(gate), held(up), held(down))


def dispatch_table(route_ids, experts, capacity):
    flat_ids = route_ids.reshape(-1)
    expert_hot = (flat_ids[:, None] == jnp.arange(experts, dtype=jnp.int32)[None, :]).astype(
        jnp.int32
    )
    slot_rank = jnp.sum((jnp.cumsum(expert_hot, axis=0) - 1) * expert_hot, axis=1)
    slot_hot = (slot_rank[:, None] == jnp.arange(capacity, dtype=jnp.int32)[None, :]).astype(
        jnp.float32
    )
    table = expert_hot.astype(jnp.float32)[:, :, None] * slot_hot[:, None, :]
    return table.reshape(flat_ids.shape[0], experts * capacity)


def pack_rows(table, row_block, top_count, experts, capacity):
    repeated = jnp.repeat(row_block, top_count, axis=0)
    packed = jnp.einsum(
        "as,aw->sw", table.astype(jnp.bfloat16), repeated, preferred_element_type=jnp.float32
    ).astype(jnp.bfloat16)
    return packed.reshape(experts, capacity, row_block.shape[1])


def swap(value, half, peer):
    ep_count, tp_count = lax.axis_size("ep"), lax.axis_size("tp")
    away = half * tp_count + peer
    return lax.ppermute(value, ("ep", "tp"), [(i, i ^ away) for i in range(ep_count * tp_count)])


def far_places(peers):
    return [(half, peer) for half in range(2) for peer in range(0, peers, 2)]


def gather_chunks(own, peers, beside):
    chunks = {}
    for half, peer in far_places(peers):
        chunks[half, peer] = swap(own, half, peer) if half or peer else own
    first = (0, 2) if peers > 2 else (1, 0)
    chunks[first], beside = lax.optimization_barrier((chunks[first], beside))
    for half, peer in far_places(peers):
        chunks[half, peer ^ 1] = swap(chunks[half, peer], 0, 1)
    return [chunks[half, peer] for half in range(2) for peer in range(peers)], beside


def sum_chunks(terms, peers):
    left = {(place // peers, place % peers): term for place, term in enumerate(terms)}
    places = far_places(peers)
    for half, peer in places[1:] + places[:1]:
        other = swap(left[half, peer ^ 1], 0, 1)
        left[half, peer] = left[half, peer].astype(jnp.float32) + other.astype(jnp.float32)
    total = left[0, 0]
    for half, peer in places[1:]:
        total = total + swap(left[half, peer].astype(jnp.bfloat16), half, peer).astype(jnp.float32)
    return total


def body(
    tokens,
    gain_mix,
    gain_ffn,
    w_query,
    w_key,
    w_value,
    w_outgate,
    w_ingate,
    w_forget,
    bias_in,
    bias_forget,
    w_proj,
    matrix_state,
    normal_state,
    stab_state,
    route_ids,
    route_weights,
    w_exp_gate,
    w_exp_up,
    w_exp_down,
):
    ep_count = lax.axis_size("ep")
    tp_count = lax.axis_size("tp")
    tp_index = lax.axis_index("tp")
    seq_dev = tokens.shape[0]
    model_width = tokens.shape[1]
    heads_dev = matrix_state.shape[1]
    head_dim = matrix_state.shape[2]
    head_cols = w_query.shape[1]
    top_count = route_ids.shape[1]
    experts = ep_count // 2
    capacity = min(seq_dev, max(2, 2 * seq_dev * top_count // experts))
    every_row = capacity == seq_dev
    col_width = model_width // tp_count
    index = jnp.stack([tp_index, lax.axis_index("ep") % 2]).astype(jnp.int32)
    blocks, own_weights = prepare(tokens, gain_mix, (w_query, w_key, w_value, w_outgate), experts)
    with jax.named_scope("pair"):
        other_weights = swap(own_weights, 1, 0)
    same_half = [list(range(half, ep_count, 2)) for half in range(2)]

    def exchange(rows):
        return lax.all_to_all(
            rows, "ep", split_axis=0, concat_axis=0, tiled=True, axis_index_groups=same_half
        )

    with jax.named_scope("spread"):
        foreign = exchange(blocks)
    terms = project(index, foreign, own_weights, other_weights)
    (held_state,) = load(terms, (matrix_state,), 1 << 22, narrowed=1)
    arrived = exchange(terms)
    factor, carry, inflow, stab_turned = gates(
        terms, index, tokens, gain_mix, w_ingate, w_forget, bias_in, bias_forget, stab_state
    )
    stab_new = stab_turned.T
    weights = route_weights / jnp.sum(route_weights, axis=-1, keepdims=True)
    if every_row:
        chosen = route_ids[:, :, None] == jnp.arange(experts, dtype=jnp.int32)
        shares = jnp.sum(jnp.where(chosen, weights[:, :, None], 0.0), axis=1)
    else:
        shares = weights
    factor, shares, stab_new = lax.optimization_barrier((factor, shares, stab_new))
    cell_outs = cell_step(
        index,
        arrived.reshape(experts, seq_dev, 4 * head_cols),
        factor,
        carry,
        inflow,
        held_state,
        normal_state.reshape(seq_dev, head_cols),
        w_proj,
        tp_count,
    )
    out_terms, state_rows = cell_outs[:tp_count], cell_outs[tp_count:]
    key_wide = (state_rows[3] * state_rows[0]).reshape(heads_dev, seq_dev, -1).transpose(1, 0, 2)
    normal_new = carry.T[:, :, None] * normal_state + key_wide
    matrix_new = update_matrix(*state_rows, matrix_state)
    own_tokens = lax.dynamic_slice_in_dim(tokens, tp_index * col_width, col_width, 1)
    attended = out_terms[0].astype(jnp.float32)
    for peer in range(1, tp_count):
        attended = attended + swap(out_terms[peer], 0, peer).astype(jnp.float32)
    own_resid = (own_tokens.astype(jnp.float32) + attended).astype(jnp.bfloat16)
    held_experts = load(held(state_rows[0]), (w_exp_gate, w_exp_up), 1 << 22)
    own_resid, *held_experts = lax.optimization_barrier((own_resid, *held_experts))
    if every_row:
        packed = jnp.broadcast_to(own_resid, (experts, seq_dev, col_width))
    else:
        table = dispatch_table(route_ids, experts, capacity)
        packed = pack_rows(table, own_resid, top_count, experts, capacity)
    received = exchange(packed.reshape(experts * capacity, col_width))
    (held_down,) = load(received, (w_exp_down,), 1 << 22)
    chunks, held_down = gather_chunks(received, tp_count, held_down)
    down_terms = expert_step(
        index,
        chunks,
        gain_ffn.reshape(1, model_width),
        *held_experts,
        held_down,
        tp_count,
    )
    half_share = sum_chunks(down_terms, tp_count).astype(jnp.bfloat16)
    half_share, matrix_new = lax.optimization_barrier((half_share, matrix_new))
    returned = exchange(half_share).astype(jnp.float32).reshape(experts, capacity, col_width)
    if every_row:
        routed = jnp.sum(returned * shares.T[:, :, None], axis=0)
    else:
        combine = jnp.sum(
            (table * shares.reshape(-1)[:, None]).reshape(
                seq_dev, top_count, experts * capacity
            ),
            axis=1,
        )
        routed = jnp.dot(
            combine, returned.reshape(experts * capacity, col_width), precision=lax.Precision.HIGHEST
        )
    mixed_out = (own_resid.astype(jnp.float32) + routed).astype(jnp.bfloat16)
    return (mixed_out, matrix_new, normal_new, stab_new)


def solution(mesh):
    placed = (
        P("ep", None),
        P(),
        P(),
        P("ep", "tp"),
        P("ep", "tp"),
        P("ep", "tp"),
        P("ep", "tp"),
        P(),
        P(),
        P(),
        P(),
        P("tp", None),
        P("ep", "tp", None, None),
        P("ep", "tp", None),
        P("ep", "tp"),
        P("ep", None),
        P("ep", None),
        P("ep", None, "tp"),
        P("ep", None, "tp"),
        P("ep", "tp", None),
    )
    return jax.shard_map(
        body,
        mesh=mesh,
        in_specs=placed,
        out_specs=(P("ep", "tp"), P("ep", "tp", None, None), P("ep", "tp", None), P("ep", "tp")),
        check_vma=False,
    )
```

time: 103 us -> 83.4 us (0.81)
  blocking collectives: 27.3 us -> 8.87 us
  starting transfers between devices: 12.5 us -> 26.6 us
  other arithmetic: 7.59 us -> 2.41 us
  local copies, waits for them, and re-layouts: 5.05 us -> 0.15 us
  waiting for transfers between devices: 28.5 us -> 24 us
    all_to_all x2 -> x1, blocking collectives: 27.3 us -> 8.87 us  [exchange(): lax.all_to_all(rows, 'ep', split_axis=0, concat_axis=0, tiled=True, axis_...]
    ppermute x9 -> x18, waiting for transfers between devices: 18.7 us -> 8.4 us  [swap(): lax.ppermute(value, ('ep', 'tp'), [(i, i ^ away) for i in range(ep_count...]
    ppermute x9 -> x18, starting transfers between devices: 4.3 us -> 13.2 us  [swap(): lax.ppermute(value, ('ep', 'tp'), [(i, i ^ away) for i in range(ep_count...]
    all_to_all x2 -> x3, waiting for transfers between devices: 9.8 us -> 15.6 us  [exchange(): lax.all_to_all(rows, 'ep', split_axis=0, concat_axis=0, tiled=True, axis_...]
    all_to_all x2 -> x3, starting transfers between devices: 8.19 us -> 13.3 us  [exchange(): lax.all_to_all(rows, 'ep', split_axis=0, concat_axis=0, tiled=True, axis_...]
    unnamed x35 -> x23, local copies, waits for them, and re-layouts: 2.89 us -> 0.05 us
    convert_element_type x3 -> x4, other arithmetic: 3.49 us -> 0.84 us  [the longest x1 0.74 us: body(): half_share = sum_chunks(down_terms, tp_count).astype(jnp.bfloat16)]
    pallas_call x1, Pallas kernels: 4.65 us -> 2.75 us  [cell_step(): pl.pallas_call(functools.partial(cell_kernel, peers=peers), in_specs=[pl....]
  transfers between devices with their start and end apart: 11 -> 21, of which waited for: 7 -> 11; matrix products, arithmetic and copies ran while one was open for 6% -> 1% of each run, Pallas kernels for 7% -> 13%
where the time goes in v3:
time: 83.4 us; the launch traced here: 82.8 us
  starting transfers between devices  26.6 us (32%)
  waiting for transfers between devices  24 us (29%)
  Pallas kernels  19.8 us (24%)
  blocking collectives  8.87 us (11%)
  other arithmetic  2.41 us (3%)
  between operations  0.97 us (1%)
    all_to_all x3, waiting for transfers between devices, exchange(): lax.all_to_all(rows, 'ep', split_axis=0, concat_axis=0, tiled=True, axis_...  15.6 us
    all_to_all x3, starting transfers between devices, exchange(): lax.all_to_all(rows, 'ep', split_axis=0, concat_axis=0, tiled=True, axis_...  13.3 us
    ppermute x18, starting transfers between devices, swap(): lax.ppermute(value, ('ep', 'tp'), [(i, i ^ away) for i in range(ep_count...  13.2 us
    all_to_all x1, blocking collectives, exchange(): lax.all_to_all(rows, 'ep', split_axis=0, concat_axis=0, tiled=True, axis_...  8.87 us
    ppermute x18, waiting for transfers between devices, swap(): lax.ppermute(value, ('ep', 'tp'), [(i, i ^ away) for i in range(ep_count...  8.4 us
    pallas_call x3, Pallas kernels, load(): pl.pallas_call(functools.partial(load_kernel, count=len(arrays), narrowed...  5.79 us
    pallas_call x1, Pallas kernels, update_matrix(): pl.pallas_call(update_kernel, in_specs=[pl.BlockSpec()] * 4 + [anywhere],...  3.65 us
    pallas_call x1, Pallas kernels, cell_step(): pl.pallas_call(functools.partial(cell_kernel, peers=peers), in_specs=[pl....  2.75 us
  transfers between devices with their start and end apart: 21, of which 11 were waited for; matrix products, arithmetic and copies ran while one was open for 1% of the time, Pallas kernels for 13%

profile of v3, /device:TPU:0, one launch (start us, length us, event | category | flops | bytes accessed | tf_op | source)
XLA Modules:
  0.0 82.8 jit_solution(14495835434201123572)
XLA Ops:
  0.6 0.0 copy-start
  0.6 0.0 copy-start.3
  0.7 0.0 copy-start.7
  0.7 0.0 copy-start.9
  0.7 0.0 copy-start.10
  0.7 2.0 %prepare.1 = (bf16[128,512]{1,0:T(8,128)(2,1)}, bf16[4,256,256]{2,1,0:T(8,128)(2,1)S(1)}) custom-call(bf16[32,2048]{1,0:T(8,128)(2,1)} %rows_ref.1, bf16[2048]{0:T(1024)(128)(2,1)} %gain_ref.1, bf16[256,256]{1,0:T(8,128)(2,1)} %refs_0_.4, bf16[256,256]{1,0:T(8,128)(2,1)} %refs_1_.2, bf16[256,256]{1,0:T(8,128)(2,1)} %refs_2_.1, bf16[256,256]{1,0:T(8,128)(2,1)} %refs_3_.1), custom_call_target="tpu_custom_call" | custom-call | tf_op jit(solution)/shard_map/prepare/pallas_call | solution.py:94
  2.7 3.1 %collective-permute-start = (bf16[4,256,256]{2,1,0:T(8,128)(2,1)S(1)}, bf16[4,256,256]{2,1,0:T(8,128)(2,1)S(1)}, u32[]{:S(2)}, u32[]{:S(2)}) collective-permute-start(bf16[4,256,256]{2,1,0:T(8,128)(2,1)S(1)} %get-tuple-element.39.own_ref), channel_id=1, source_target_pairs={{0,4},{1,5},{2,6},{3,7},{4,0},{5,1},{6,2},{7,3},{8,12},{9,13},{10,... | collective-permute-start | bytes 1572872 | tf_op jit(solution)/shard_map/pair/ppermute | solution.py:409
  5.8 4.9 %all-to-all-start = ((bf16[4,32,512]{2,1,0:T(8,128)(2,1)}), bf16[4,32,512]{2,1,0:T(8,128)(2,1)S(1)}, u32[]{:S(2)}, u32[]{:S(2)}) async-start(bf16[4,32,512]{2,1,0:T(8,128)(2,1)} %bitcast.2), calls=%async_computation | async-start | bytes 262144 | tf_op jit(solution)/shard_map/spread/all_to_all | solution.py:481
  10.6 0.1 pad_add_fusion.index_ref
  10.7 5.9 %all-to-all-done = bf16[4,32,512]{2,1,0:T(8,128)(2,1)S(1)} async-done(((bf16[4,32,512]{2,1,0:T(8,128)(2,1)}), bf16[4,32,512]{2,1,0:T(8,128)(2,1)S(1)}, u32[]{:S(2)}, u32[]{:S(2)}) %all-to-all-start) | async-done | bytes 131104 | tf_op jit(solution)/shard_map/spread/all_to_all | solution.py:481
  16.6 1.1 %collective-permute-done.other_ref = bf16[4,256,256]{2,1,0:T(8,128)(2,1)S(1)} collective-permute-done((bf16[4,256,256]{2,1,0:T(8,128)(2,1)S(1)}, bf16[4,256,256]{2,1,0:T(8,128)(2,1)S(1)}, u32[]{:S(2)}, u32[]{:S(2)}) %collective-permute-start) | collective-permute-done | bytes 524320 | tf_op jit(solution)/shard_map/pair/ppermute | solution.py:409
  17.7 1.6 %project.1._ = bf16[128,1024]{1,0:T(8,128)(2,1)} custom-call(s32[2]{0:T(128)S(1)} %pad_add_fusion.index_ref, bf16[128,512]{1,0:T(8,128)(2,1)S(1)} %bitcast.26, bf16[4,256,256]{2,1,0:T(8,128)(2,1)S(1)} %get-tuple-element.39.own_ref, bf16[4,256,256]{2,1,0:T(8,128)(2,1)S(1)} %collective-permute-done.other_ref), custom_call_target="tpu_custom_call" | custom-call | tf_op jit(solution)/shard_map/project/pallas_call | solution.py:189
  19.2 5.1 %all-to-all-start.1 = ((bf16[4,32,1024]{2,1,0:T(8,128)(2,1)}), bf16[4,32,1024]{2,1,0:T(8,128)(2,1)S(1)}, u32[]{:S(2)}, u32[]{:S(2)}) async-start(bf16[4,32,1024]{2,1,0:T(8,128)(2,1)} %bitcast.4), calls=%async_computation.1 | async-start | bytes 524288 | tf_op jit(solution)/shard_map/all_to_all | solution.py:481
  24.3 0.0 copy-done.7
  24.5 1.4 %gates.1 = (f32[32,1]{1,0:T(8,128)S(1)}, f32[2,32]{1,0:T(2,128)S(1)}, f32[2,32]{1,0:T(2,128)S(1)}, f32[2,32]{1,0:T(2,128)}) custom-call(s32[2]{0:T(128)S(1)} %pad_add_fusion.index_ref, bf16[128,1024]{1,0:T(8,128)(2,1)} %project.1._, bf16[32,2048]{1,0:T(8,128)(2,1)S(1)} %copy-done, bf16[2048]{0:T(1024)(128)(2,1)S(1)} %copy-done.3, ...), custom_call_target="tpu_custom_call" | custom-call | flops 4194304 | tf_op jit(solution)/shard_map/gates/pallas_call | solution.py:154
  25.9 2.5 %load.3.matrix_ref = bf16[32,2,128,128]{3,2,1,0:T(8,128)(2,1)S(1)} custom-call(bf16[128,1024]{1,0:T(8,128)(2,1)} %project.1._, f32[32,2,128,128]{3,2,1,0:T(8,128)} %matrix_hbm.1), custom_call_target="tpu_custom_call" | custom-call | flops 4194304 | tf_op jit(solution)/shard_map/load/pallas_call | solution.py:42
  28.4 4.1 %all-to-all-done.1.arrived_ref = bf16[4,32,1024]{2,1,0:T(8,128)(2,1)S(1)} async-done(((bf16[4,32,1024]{2,1,0:T(8,128)(2,1)}), bf16[4,32,1024]{2,1,0:T(8,128)(2,1)S(1)}, u32[]{:S(2)}, u32[]{:S(2)}) %all-to-all-start.1) | async-done | bytes 262176 | tf_op jit(solution)/shard_map/all_to_all | solution.py:481
  32.5 2.7 %cell_step.1 = (bf16[32,512]{1,0:T(8,128)(2,1)S(1)}, bf16[32,512]{1,0:T(8,128)(2,1)S(1)}, bf16[32,512]{1,0:T(8,128)(2,1)S(1)}, bf16[32,512]{1,0:T(8,128)(2,1)S(1...) custom-call(s32[2]{0:T(128)S(1)} %pad_add_fusion.index_ref, ...), custom_call_target="tpu_custom_call" | custom-call | tf_op jit(solution)/shard_map/cell_step/pallas_call | solution.py:260
  35.3 0.1 collective-permute-start.3
  35.3 1.6 %collective-permute-start.2 = (bf16[32,512]{1,0:T(8,128)(2,1)S(1)}, bf16[32,512]{1,0:T(8,128)(2,1)S(1)}, u32[]{:S(2)}, u32[]{:S(2)}) collective-permute-start(bf16[32,512]{1,0:T(8,128)(2,1)S(1)} %get-tuple-element.47), channel_id=1, source_target_pairs={{0,2},{1,3},{2,0},{3,1},{4,6},{5,7},{6,4},{7,5},{8,10},{9,11},{10,... | collective-permute-start | bytes 98312 | tf_op jit(solution)/shard_map/ppermute | solution.py:409
  36.9 0.3 collective-permute-start.1
  37.2 1.9 %load.4 = (bf16[1,2048,384]{2,1,0:T(8,128)(2,1)S(1)}, bf16[1,2048,384]{2,1,0:T(8,128)(2,1)S(1)}) custom-call(f32[64,128]{1,0:T(8,128)S(1)} %get-tuple-element.49._.key_ref, bf16[1,2048,384]{2,1,0:T(8,128)(2,1)} %refs_0_.6, bf16[1,2048,384]{2,1,0:T(8,128)(2,1)} %refs_1_.3), custom_call_target="tpu_custom_call" | custom-call | flops 4194304 | tf_op jit(solution)/shard_map/load/pallas_call | solution.py:42
  39.1 0.0 collective-permute-done.3
  39.1 0.3 collective-permute-done.2
  39.4 0.0 collective-permute-done.1
  39.4 8.9 %all_to_all.37 = bf16[4,32,512]{2,1,0:T(8,128)(2,1)S(1)} all-to-all(bf16[4,32,512]{2,1,0:T(8,128)(2,1)S(1)} %broadcast_in_dim.23), channel_id=1, replica_groups={{0,8,16,24},{4,12,20,28},{1,9,17,25},{5,13,21,29},{2,10,18,26},{6,14,22..., dimensions={0} | all-to-all | bytes 262144 | tf_op jit(solution)/shard_map/all_to_all | solution.py:481
  48.3 1.2 %collective-permute-start.5 = (bf16[128,512]{1,0:T(8,128)(2,1)S(1)}, bf16[128,512]{1,0:T(8,128)(2,1)S(1)}, u32[]{:S(2)}, u32[]{:S(2)}) collective-permute-start(bf16[128,512]{1,0:T(8,128)(2,1)S(1)} %bitcast.20), channel_id=1, source_target_pairs={{0,2},{1,3},{2,0},{3,1},{4,6},{5,7},{6,4},{7,5},{8,10},{9,11},{10,... | collective-permute-start | bytes 393224 | tf_op jit(solution)/shard_map/ppermute | solution.py:409
  49.5 1.5 %collective-permute-start.7 = (bf16[128,512]{1,0:T(8,128)(2,1)S(1)}, bf16[128,512]{1,0:T(8,128)(2,1)S(1)}, u32[]{:S(2)}, u32[]{:S(2)}) collective-permute-start(bf16[128,512]{1,0:T(8,128)(2,1)S(1)} %bitcast.21), channel_id=1, source_target_pairs={{0,4},{1,5},{2,6},{3,7},{4,0},{5,1},{6,2},{7,3},{8,12},{9,13},{10,... | collective-permute-start | bytes 393224 | tf_op jit(solution)/shard_map/ppermute | solution.py:409
  51.0 0.8 collective-permute-start.9
  51.8 0.0 collective-permute-start.4
  51.8 1.4 %load.5.refs_11_ = bf16[1,384,2048]{2,1,0:T(8,128)(2,1)S(1)} custom-call(bf16[128,512]{1,0:T(8,128)(2,1)S(1)} %bitcast.24, bf16[1,384,2048]{2,1,0:T(8,128)(2,1)} %refs_0_.7), custom_call_target="tpu_custom_call" | custom-call | flops 4194304 | tf_op jit(solution)/shard_map/load/pallas_call | solution.py:42
  53.2 1.0 %collective-permute-done.5.refs_2_ = bf16[128,512]{1,0:T(8,128)(2,1)S(1)} collective-permute-done((bf16[128,512]{1,0:T(8,128)(2,1)S(1)}, bf16[128,512]{1,0:T(8,128)(2,1)S(1)}, u32[]{:S(2)}, u32[]{:S(2)}) %collective-permute-start.5) | collective-permute-done | bytes 131104 | tf_op jit(solution)/shard_map/ppermute | solution.py:409
  54.2 0.0 collective-permute-start.6
  54.2 1.1 %collective-permute-done.7.refs_4_ = bf16[128,512]{1,0:T(8,128)(2,1)S(1)} collective-permute-done((bf16[128,512]{1,0:T(8,128)(2,1)S(1)}, bf16[128,512]{1,0:T(8,128)(2,1)S(1)}, u32[]{:S(2)}, u32[]{:S(2)}) %collective-permute-start.7) | collective-permute-done | bytes 131104 | tf_op jit(solution)/shard_map/ppermute | solution.py:409
  55.3 0.0 collective-permute-start.8
  55.3 1.6 %collective-permute-done.9.refs_6_ = bf16[128,512]{1,0:T(8,128)(2,1)S(1)} collective-permute-done((bf16[128,512]{1,0:T(8,128)(2,1)S(1)}, bf16[128,512]{1,0:T(8,128)(2,1)S(1)}, u32[]{:S(2)}, u32[]{:S(2)}) %collective-permute-start.9) | collective-permute-done | bytes 131104 | tf_op jit(solution)/shard_map/ppermute | solution.py:409
  56.9 0.0 collective-permute-start.10
  56.9 0.0 collective-permute-done.4.refs_1_
  56.9 0.0 collective-permute-done.6.refs_3_
  56.9 0.0 collective-permute-done.8.refs_5_
  56.9 1.3 %collective-permute-done.10.refs_7_ = bf16[128,512]{1,0:T(8,128)(2,1)S(1)} collective-permute-done((bf16[128,512]{1,0:T(8,128)(2,1)S(1)}, bf16[128,512]{1,0:T(8,128)(2,1)S(1)}, u32[]{:S(2)}, u32[]{:S(2)}) %collective-permute-start.10) | collective-permute-done | bytes 131104 | tf_op jit(solution)/shard_map/ppermute | solution.py:409
  58.2 2.7 %expert_step.1 = (bf16[128,512]{1,0:T(8,128)(2,1)S(1)}, bf16[128,512]{1,0:T(8,128)(2,1)S(1)}, bf16[128,512]{1,0:T(8,128)(2,1)S(1)}, bf16[128,512]{1,0:T(8,128)(2...) custom-call(s32[2]{0:T(128)S(1)} %pad_add_fusion.index_ref, ...), custom_call_target="tpu_custom_call" | custom-call | tf_op jit(solution)/shard_map/expert_step/pallas_call | solution.py:374
  60.9 0.2 collective-permute-start.16
  61.1 0.4 collective-permute-start.14
  61.5 0.1 collective-permute-start.12
  61.6 0.4 collective-permute-start.11
  62.0 0.3 collective-permute-done.16
  62.3 1.5 %collective-permute-start.17 = (bf16[128,512]{1,0:T(8,128)(2,1)S(1)}, bf16[128,512]{1,0:T(8,128)(2,1)S(1)}, u32[]{:S(2)}, u32[]{:S(2)}) collective-permute-start(bf16[128,512]{1,0:T(8,128)(2,1)S(1)} %add_convert_fusion.1), channel_id=1, source_target_pairs={{0,6},{1,7},{2,4},{3,5},{4,2},{5,3},{6,0},{7,1},{8,14},{9,15},{10,... | collective-permute-start | bytes 393224 | tf_op jit(solution)/shard_map/ppermute | solution.py:409
  63.8 0.0 collective-permute-done.14
  63.9 0.9 %collective-permute-start.15 = (bf16[128,512]{1,0:T(8,128)(2,1)S(1)}, bf16[128,512]{1,0:T(8,128)(2,1)S(1)}, u32[]{:S(2)}, u32[]{:S(2)}) collective-permute-start(bf16[128,512]{1,0:T(8,128)(2,1)S(1)} %add_convert_fusion.2), channel_id=1, source_target_pairs={{0,4},{1,5},{2,6},{3,7},{4,0},{5,1},{6,2},{7,3},{8,12},{9,13},{10,... | collective-permute-start | bytes 393224 | tf_op jit(solution)/shard_map/ppermute | solution.py:409
  64.8 0.0 collective-permute-done.12
  64.9 1.2 %collective-permute-start.13 = (bf16[128,512]{1,0:T(8,128)(2,1)S(1)}, bf16[128,512]{1,0:T(8,128)(2,1)S(1)}, u32[]{:S(2)}, u32[]{:S(2)}) collective-permute-start(bf16[128,512]{1,0:T(8,128)(2,1)S(1)} %add_convert_fusion.3), channel_id=1, source_target_pairs={{0,2},{1,3},{2,0},{3,1},{4,6},{5,7},{6,4},{7,5},{8,10},{9,11},{10,... | collective-permute-start | bytes 393224 | tf_op jit(solution)/shard_map/ppermute | solution.py:409
  66.1 0.1 copy.28
  66.2 3.7 %update_matrix.1 = f32[32,2,128,128]{3,2,1,0:T(8,128)} custom-call(f32[64,128]{1,0:T(8,128)S(1)} %get-tuple-element.49._.key_ref, f32[64,128]{1,0:T(8,128)S(1)} %get-tuple-element.65.value_ref, f32[64,128]{1,0:T(8,128)S(1)} %get-tuple-element.66.carry_ref, f32[64,128]{1,0:T(8,128)S(1)} %get-tuple-element.67.inflow_ref, f32[32,2,128,128]{3,2,1,0:T(8,128)} %matrix_hbm.1), custom_call_target="tpu_custom_call" | custom-call | flops 8388608 | tf_op jit(solution)/shard_map/update_matrix/pallas_call | solution.py:317
  69.9 0.0 collective-permute-done.11
  69.9 0.0 collective-permute-done.17
  69.9 1.8 %collective-permute-done.15 = bf16[128,512]{1,0:T(8,128)(2,1)S(1)} collective-permute-done((bf16[128,512]{1,0:T(8,128)(2,1)S(1)}, bf16[128,512]{1,0:T(8,128)(2,1)S(1)}, u32[]{:S(2)}, u32[]{:S(2)}) %collective-permute-start.15) | collective-permute-done | bytes 131104 | tf_op jit(solution)/shard_map/ppermute | solution.py:409
  71.7 0.0 collective-permute-done.13
  71.7 0.7 add_convert_fusion
  72.4 3.4 %all-to-all-start.3 = ((bf16[4,32,512]{2,1,0:T(8,128)(2,1)}), bf16[4,32,512]{2,1,0:T(8,128)(2,1)S(1)}, u32[]{:S(2)}, u32[]{:S(2)}) async-start(bf16[4,32,512]{2,1,0:T(8,128)(2,1)} %bitcast.10), calls=%async_computation.3 | async-start | bytes 262144 | tf_op jit(solution)/shard_map/all_to_all | solution.py:481
  75.8 0.7 bitcast_add_fusion
  76.5 5.6 %all-to-all-done.3 = bf16[4,32,512]{2,1,0:T(8,128)(2,1)S(1)} async-done(((bf16[4,32,512]{2,1,0:T(8,128)(2,1)}), bf16[4,32,512]{2,1,0:T(8,128)(2,1)S(1)}, u32[]{:S(2)}, u32[]{:S(2)}) %all-to-all-start.3) | async-done | bytes 131104 | tf_op jit(solution)/shard_map/all_to_all | solution.py:481
  82.1 0.1 multiply_reduce_fusion
  82.2 0.6 add_convert_fusion.4
  (27 shorter events, 0.2 us)
Async XLA Ops:
  0.6 23.8 %copy-start = (bf16[32,2048]{1,0:T(8,128)(2,1)S(1)}, bf16[32,2048]{1,0:T(8,128)(2,1)}, u32[]{:S(2)}) copy-start(bf16[32,2048]{1,0:T(8,128)(2,1)} %rows_ref.1) | copy-start | bytes 393220
  0.6 23.8 %copy-start.3 = (bf16[2048]{0:T(1024)(128)(2,1)S(1)}, bf16[2048]{0:T(1024)(128)(2,1)}, u32[]{:S(2)}) copy-start(bf16[2048]{0:T(1024)(128)(2,1)} %gain_ref.1) | copy-start | bytes 12292
  0.7 23.7 %copy-start.7 = (f32[32,2,128]{2,1,0:T(2,128)S(1)}, f32[32,2,128]{2,1,0:T(2,128)}, u32[]{:S(2)}) copy-start(f32[32,2,128]{2,1,0:T(2,128)} %param.33) | copy-start | bytes 98308
  0.7 23.7 %copy-start.9 = (f32[32,2]{0,1:T(2,128)S(1)}, f32[32,2]{0,1:T(2,128)}, u32[]{:S(2)}) copy-start(f32[32,2]{0,1:T(2,128)} %param.36) | copy-start | bytes 772
  0.7 23.7 %copy-start.10 = (s32[32,2]{0,1:T(2,128)S(1)}, s32[32,2]{0,1:T(2,128)}, u32[]{:S(2)}) copy-start(s32[32,2]{0,1:T(2,128)} %param.35) | copy-start | bytes 772
  0.7 23.7 %copy-start.1 = (bf16[2048,8]{0,1:T(8,128)(2,1)S(1)}, bf16[2048,8]{0,1:T(8,128)(2,1)}, u32[]{:S(2)}) copy-start(bf16[2048,8]{0,1:T(8,128)(2,1)} %param.27) | copy-start | bytes 98308
  0.7 23.7 %copy-start.2 = (bf16[2048,8]{0,1:T(8,128)(2,1)S(1)}, bf16[2048,8]{0,1:T(8,128)(2,1)}, u32[]{:S(2)}) copy-start(bf16[2048,8]{0,1:T(8,128)(2,1)} %param.28) | copy-start | bytes 98308
  0.7 23.7 %copy-start.5 = (f32[8]{0:T(128)S(1)}, f32[8]{0:T(128)}, u32[]{:S(2)}) copy-start(f32[8]{0:T(128)} %bias_in_ref.1) | copy-start | bytes 100
  0.7 23.7 %copy-start.6 = (f32[8]{0:T(128)S(1)}, f32[8]{0:T(128)}, u32[]{:S(2)}) copy-start(f32[8]{0:T(128)} %bias_forget_ref.1) | copy-start | bytes 100
  0.7 23.7 %copy-start.4 = (f32[32,2]{0,1:T(2,128)S(1)}, f32[32,2]{0,1:T(2,128)}, u32[]{:S(2)}) copy-start(f32[32,2]{0,1:T(2,128)} %param.34) | copy-start | bytes 772
  2.7 15.0 %collective-permute-start = (bf16[4,256,256]{2,1,0:T(8,128)(2,1)S(1)}, bf16[4,256,256]{2,1,0:T(8,128)(2,1)S(1)}, u32[]{:S(2)}, u32[]{:S(2)}) collective-permute-start(bf16[4,256,256]{2,1,0:T(8,128)(2,1)S(1)} %get-tuple-element.39.own_ref), channel_id=1, source_target_pairs={{0,4},{1,5},{2,6},{3,7},{4,0},{5,1},{6,2},{7,3},{8,12},{9,13},{10,... | collective-permute-start | bytes 1572872 | tf_op jit(solution)/shard_map/pair/ppermute | solution.py:409
  5.8 10.9 %all-to-all-start = ((bf16[4,32,512]{2,1,0:T(8,128)(2,1)}), bf16[4,32,512]{2,1,0:T(8,128)(2,1)S(1)}, u32[]{:S(2)}, u32[]{:S(2)}) async-start(bf16[4,32,512]{2,1,0:T(8,128)(2,1)} %bitcast.2), calls=%async_computation | async-start | bytes 262144 | tf_op jit(solution)/shard_map/spread/all_to_all | solution.py:481
  19.2 13.3 %all-to-all-start.1 = ((bf16[4,32,1024]{2,1,0:T(8,128)(2,1)}), bf16[4,32,1024]{2,1,0:T(8,128)(2,1)S(1)}, u32[]{:S(2)}, u32[]{:S(2)}) async-start(bf16[4,32,1024]{2,1,0:T(8,128)(2,1)} %bitcast.4), calls=%async_computation.1 | async-start | bytes 524288 | tf_op jit(solution)/shard_map/all_to_all | solution.py:481
  35.3 3.8 %collective-permute-start.3 = (bf16[32,512]{1,0:T(8,128)(2,1)S(1)}, bf16[32,512]{1,0:T(8,128)(2,1)S(1)}, u32[]{:S(2)}, u32[]{:S(2)}) collective-permute-start(bf16[32,512]{1,0:T(8,128)(2,1)S(1)} %get-tuple-element.48), channel_id=1, source_target_pairs={{0,3},{1,2},{2,1},{3,0},{4,7},{5,6},{6,5},{7,4},{8,11},{9,10},{10,... | collective-permute-start | bytes 98312 | tf_op jit(solution)/shard_map/ppermute | solution.py:409
  35.3 4.0 %collective-permute-start.2 = (bf16[32,512]{1,0:T(8,128)(2,1)S(1)}, bf16[32,512]{1,0:T(8,128)(2,1)S(1)}, u32[]{:S(2)}, u32[]{:S(2)}) collective-permute-start(bf16[32,512]{1,0:T(8,128)(2,1)S(1)} %get-tuple-element.47), channel_id=1, source_target_pairs={{0,2},{1,3},{2,0},{3,1},{4,6},{5,7},{6,4},{7,5},{8,10},{9,11},{10,... | collective-permute-start | bytes 98312 | tf_op jit(solution)/shard_map/ppermute | solution.py:409
  36.9 2.5 %collective-permute-start.1 = (bf16[32,512]{1,0:T(8,128)(2,1)S(1)}, bf16[32,512]{1,0:T(8,128)(2,1)S(1)}, u32[]{:S(2)}, u32[]{:S(2)}) collective-permute-start(bf16[32,512]{1,0:T(8,128)(2,1)S(1)} %get-tuple-element.46), channel_id=1, source_target_pairs={{0,1},{1,0},{2,3},{3,2},{4,5},{5,4},{6,7},{7,6},{8,9},{9,8},{10,11... | collective-permute-start | bytes 98312 | tf_op jit(solution)/shard_map/ppermute | solution.py:409
  48.3 8.6 %copy-start.8 = (bf16[2048]{0:T(1024)(128)(2,1)S(1)}, bf16[2048]{0:T(1024)(128)(2,1)}, u32[]{:S(2)}) copy-start(bf16[2048]{0:T(1024)(128)(2,1)} %param.22) | copy-start | bytes 12292
  48.3 5.9 %collective-permute-start.5 = (bf16[128,512]{1,0:T(8,128)(2,1)S(1)}, bf16[128,512]{1,0:T(8,128)(2,1)S(1)}, u32[]{:S(2)}, u32[]{:S(2)}) collective-permute-start(bf16[128,512]{1,0:T(8,128)(2,1)S(1)} %bitcast.20), channel_id=1, source_target_pairs={{0,2},{1,3},{2,0},{3,1},{4,6},{5,7},{6,4},{7,5},{8,10},{9,11},{10,... | collective-permute-start | bytes 393224 | tf_op jit(solution)/shard_map/ppermute | solution.py:409
  49.5 5.8 %collective-permute-start.7 = (bf16[128,512]{1,0:T(8,128)(2,1)S(1)}, bf16[128,512]{1,0:T(8,128)(2,1)S(1)}, u32[]{:S(2)}, u32[]{:S(2)}) collective-permute-start(bf16[128,512]{1,0:T(8,128)(2,1)S(1)} %bitcast.21), channel_id=1, source_target_pairs={{0,4},{1,5},{2,6},{3,7},{4,0},{5,1},{6,2},{7,3},{8,12},{9,13},{10,... | collective-permute-start | bytes 393224 | tf_op jit(solution)/shard_map/ppermute | solution.py:409
  51.0 5.9 %collective-permute-start.9 = (bf16[128,512]{1,0:T(8,128)(2,1)S(1)}, bf16[128,512]{1,0:T(8,128)(2,1)S(1)}, u32[]{:S(2)}, u32[]{:S(2)}) collective-permute-start(bf16[128,512]{1,0:T(8,128)(2,1)S(1)} %bitcast.22), channel_id=1, source_target_pairs={{0,6},{1,7},{2,4},{3,5},{4,2},{5,3},{6,0},{7,1},{8,14},{9,15},{10,... | collective-permute-start | bytes 393224 | tf_op jit(solution)/shard_map/ppermute | solution.py:409
  51.8 5.1 %collective-permute-start.4 = (bf16[128,512]{1,0:T(8,128)(2,1)S(1)}, bf16[128,512]{1,0:T(8,128)(2,1)S(1)}, u32[]{:S(2)}, u32[]{:S(2)}) collective-permute-start(bf16[128,512]{1,0:T(8,128)(2,1)S(1)} %bitcast.23), channel_id=1, source_target_pairs={{0,1},{1,0},{2,3},{3,2},{4,5},{5,4},{6,7},{7,6},{8,9},{9,8},{10,11... | collective-permute-start | bytes 393224 | tf_op jit(solution)/shard_map/ppermute | solution.py:409
  54.2 2.7 %collective-permute-start.6 = (bf16[128,512]{1,0:T(8,128)(2,1)S(1)}, bf16[128,512]{1,0:T(8,128)(2,1)S(1)}, u32[]{:S(2)}, u32[]{:S(2)}) collective-permute-start(bf16[128,512]{1,0:T(8,128)(2,1)S(1)} %collective-permute-done.5.refs_2_), channel_id=1, source_target_pairs={{0,1},{1,0},{2,3},{3,2},{4,5},{5,4},{6,7},{7,6},{8,9},{9,8},{10,11... | collective-permute-start | bytes 393224 | tf_op jit(solution)/shard_map/ppermute | solution.py:409
  55.3 1.6 %collective-permute-start.8 = (bf16[128,512]{1,0:T(8,128)(2,1)S(1)}, bf16[128,512]{1,0:T(8,128)(2,1)S(1)}, u32[]{:S(2)}, u32[]{:S(2)}) collective-permute-start(bf16[128,512]{1,0:T(8,128)(2,1)S(1)} %collective-permute-done.7.refs_4_), channel_id=1, source_target_pairs={{0,1},{1,0},{2,3},{3,2},{4,5},{5,4},{6,7},{7,6},{8,9},{9,8},{10,11... | collective-permute-start | bytes 393224 | tf_op jit(solution)/shard_map/ppermute | solution.py:409
  56.9 1.3 %collective-permute-start.10 = (bf16[128,512]{1,0:T(8,128)(2,1)S(1)}, bf16[128,512]{1,0:T(8,128)(2,1)S(1)}, u32[]{:S(2)}, u32[]{:S(2)}) collective-permute-start(bf16[128,512]{1,0:T(8,128)(2,1)S(1)} %collective-permute-done.9.refs_6_), channel_id=1, source_target_pairs={{0,1},{1,0},{2,3},{3,2},{4,5},{5,4},{6,7},{7,6},{8,9},{9,8},{10,11... | collective-permute-start | bytes 393224 | tf_op jit(solution)/shard_map/ppermute | solution.py:409
  60.9 1.4 %collective-permute-start.16 = (bf16[128,512]{1,0:T(8,128)(2,1)S(1)}, bf16[128,512]{1,0:T(8,128)(2,1)S(1)}, u32[]{:S(2)}, u32[]{:S(2)}) collective-permute-start(bf16[128,512]{1,0:T(8,128)(2,1)S(1)} %get-tuple-element.64), channel_id=1, source_target_pairs={{0,1},{1,0},{2,3},{3,2},{4,5},{5,4},{6,7},{7,6},{8,9},{9,8},{10,11... | collective-permute-start | bytes 393224 | tf_op jit(solution)/shard_map/ppermute | solution.py:409
  61.1 2.8 %collective-permute-start.14 = (bf16[128,512]{1,0:T(8,128)(2,1)S(1)}, bf16[128,512]{1,0:T(8,128)(2,1)S(1)}, u32[]{:S(2)}, u32[]{:S(2)}) collective-permute-start(bf16[128,512]{1,0:T(8,128)(2,1)S(1)} %get-tuple-element.62), channel_id=1, source_target_pairs={{0,1},{1,0},{2,3},{3,2},{4,5},{5,4},{6,7},{7,6},{8,9},{9,8},{10,11... | collective-permute-start | bytes 393224 | tf_op jit(solution)/shard_map/ppermute | solution.py:409
  61.5 3.4 %collective-permute-start.12 = (bf16[128,512]{1,0:T(8,128)(2,1)S(1)}, bf16[128,512]{1,0:T(8,128)(2,1)S(1)}, u32[]{:S(2)}, u32[]{:S(2)}) collective-permute-start(bf16[128,512]{1,0:T(8,128)(2,1)S(1)} %get-tuple-element.60), channel_id=1, source_target_pairs={{0,1},{1,0},{2,3},{3,2},{4,5},{5,4},{6,7},{7,6},{8,9},{9,8},{10,11... | collective-permute-start | bytes 393224 | tf_op jit(solution)/shard_map/ppermute | solution.py:409
  61.6 8.3 %collective-permute-start.11 = (bf16[128,512]{1,0:T(8,128)(2,1)S(1)}, bf16[128,512]{1,0:T(8,128)(2,1)S(1)}, u32[]{:S(2)}, u32[]{:S(2)}) collective-permute-start(bf16[128,512]{1,0:T(8,128)(2,1)S(1)} %get-tuple-element.58), channel_id=1, source_target_pairs={{0,1},{1,0},{2,3},{3,2},{4,5},{5,4},{6,7},{7,6},{8,9},{9,8},{10,11... | collective-permute-start | bytes 393224 | tf_op jit(solution)/shard_map/ppermute | solution.py:409
  62.3 7.5 %collective-permute-start.17 = (bf16[128,512]{1,0:T(8,128)(2,1)S(1)}, bf16[128,512]{1,0:T(8,128)(2,1)S(1)}, u32[]{:S(2)}, u32[]{:S(2)}) collective-permute-start(bf16[128,512]{1,0:T(8,128)(2,1)S(1)} %add_convert_fusion.1), channel_id=1, source_target_pairs={{0,6},{1,7},{2,4},{3,5},{4,2},{5,3},{6,0},{7,1},{8,14},{9,15},{10,... | collective-permute-start | bytes 393224 | tf_op jit(solution)/shard_map/ppermute | solution.py:409
  63.9 7.8 %collective-permute-start.15 = (bf16[128,512]{1,0:T(8,128)(2,1)S(1)}, bf16[128,512]{1,0:T(8,128)(2,1)S(1)}, u32[]{:S(2)}, u32[]{:S(2)}) collective-permute-start(bf16[128,512]{1,0:T(8,128)(2,1)S(1)} %add_convert_fusion.2), channel_id=1, source_target_pairs={{0,4},{1,5},{2,6},{3,7},{4,0},{5,1},{6,2},{7,3},{8,12},{9,13},{10,... | collective-permute-start | bytes 393224 | tf_op jit(solution)/shard_map/ppermute | solution.py:409
  64.9 6.8 %collective-permute-start.13 = (bf16[128,512]{1,0:T(8,128)(2,1)S(1)}, bf16[128,512]{1,0:T(8,128)(2,1)S(1)}, u32[]{:S(2)}, u32[]{:S(2)}) collective-permute-start(bf16[128,512]{1,0:T(8,128)(2,1)S(1)} %add_convert_fusion.3), channel_id=1, source_target_pairs={{0,2},{1,3},{2,0},{3,1},{4,6},{5,7},{6,4},{7,5},{8,10},{9,11},{10,... | collective-permute-start | bytes 393224 | tf_op jit(solution)/shard_map/ppermute | solution.py:409
  72.4 9.7 %all-to-all-start.3 = ((bf16[4,32,512]{2,1,0:T(8,128)(2,1)}), bf16[4,32,512]{2,1,0:T(8,128)(2,1)S(1)}, u32[]{:S(2)}, u32[]{:S(2)}) async-start(bf16[4,32,512]{2,1,0:T(8,128)(2,1)} %bitcast.10), calls=%async_computation.3 | async-start | bytes 262144 | tf_op jit(solution)/shard_map/all_to_all | solution.py:481

commit v4 on v3

--- a/solution.py
+++ b/solution.py
@@ -6,6 +6,7 @@
 from jax.experimental import pallas as pl
 from jax.experimental.pallas import tpu as pltpu
 from jax.sharding import PartitionSpec as P
+
 
 norm_epsilon = 1e-06
 
@@ -33,7 +34,7 @@
                 targets[place][row] = wide[place][row].astype(jnp.bfloat16)
 
 
-def load(after, arrays, cycles, narrowed=0):
+def load(after, arrays, narrowed=0):
     anywhere = pl.BlockSpec(memory_space=pl.ANY)
     targets = [
         pltpu.VMEM(array.shape, jnp.bfloat16 if place < narrowed else array.dtype)
@@ -47,7 +48,7 @@
         scratch_shapes=[pltpu.SemaphoreType.DMA((len(arrays),))]
         + [pltpu.VMEM(array.shape, array.dtype) for array in arrays[:narrowed]],
         compiler_params=room(12),
-        cost_estimate=pl.CostEstimate(flops=cycles, bytes_accessed=0, transcendentals=0),
+        cost_estimate=pl.CostEstimate(flops=1 << 22, bytes_accessed=0, transcendentals=0),
         name="load",
     )(after, *map(away, arrays))
 
@@ -60,18 +61,38 @@
     return pltpu.with_memory_space_constraint(array, pltpu.VMEM)
 
 
-def prepare_kernel(rows_hbm, gain_hbm, *refs, weights):
-    weight_refs = refs[:weights]
-    out_ref, pack_ref, rows_ref, gain_ref, semaphores = refs[weights:]
+def pack_kernel(*refs):
+    *sources, target, semaphores = refs
+    copies = [
+        pltpu.make_async_copy(source, target.at[place], semaphores.at[place])
+        for place, source in enumerate(sources)
+    ]
+    for copy in copies:
+        copy.start()
+    for copy in copies:
+        copy.wait()
+
+
+def pack(weights):
+    return pl.pallas_call(
+        pack_kernel,
+        in_specs=[pl.BlockSpec(memory_space=pl.ANY)] * len(weights),
+        out_specs=pl.BlockSpec(memory_space=pltpu.VMEM),
+        out_shape=pltpu.VMEM((len(weights),) + weights[0].shape, weights[0].dtype),
+        scratch_shapes=[pltpu.SemaphoreType.DMA((len(weights),))],
+        compiler_params=room(12),
+        name="pack",
+    )(*map(away, weights))
+
+
+def split_kernel(rows_hbm, gain_hbm, out_ref, rows_ref, gain_ref, semaphores):
     copies = [
         pltpu.make_async_copy(rows_hbm, rows_ref, semaphores.at[0]),
         pltpu.make_async_copy(gain_hbm, gain_ref, semaphores.at[1]),
     ]
-    for place, weight_ref in enumerate(weight_refs):
-        copies.append(pltpu.make_async_copy(weight_ref, pack_ref.at[place], semaphores.at[2 + place]))
     for copy in copies:
         copy.start()
-    for copy in copies[:2]:
+    for copy in copies:
         copy.wait()
     scaled = rows_ref[...].astype(jnp.float32) * gain_ref[...].astype(jnp.float32).reshape(1, -1)
     scaled = scaled.astype(jnp.bfloat16)
@@ -79,34 +100,26 @@
     width = out_ref.shape[1]
     for place in range(out_ref.shape[0] // seqs):
         out_ref[place * seqs : (place + 1) * seqs, :] = scaled[:, place * width : (place + 1) * width]
-    for copy in copies[2:]:
-        copy.wait()
-
-
-def prepare(rows, gain, weights, count):
+
+
+def split_features(rows, gain, count):
     seqs, features = rows.shape
     width = features // count
     if width % 128:
         scaled = (rows.astype(jnp.float32) * gain.astype(jnp.float32)).astype(jnp.bfloat16)
-        blocks = scaled.reshape(seqs, count, width).transpose(1, 0, 2).reshape(count * seqs, width)
-        return blocks, jnp.stack(weights)
-    anywhere = pl.BlockSpec(memory_space=pl.ANY)
-    return pl.pallas_call(
-        functools.partial(prepare_kernel, weights=len(weights)),
-        in_specs=[anywhere] * (2 + len(weights)),
-        out_specs=[pl.BlockSpec(), pl.BlockSpec(memory_space=pltpu.VMEM)],
-        out_shape=[
-            jax.ShapeDtypeStruct((count * seqs, width), jnp.bfloat16),
-            pltpu.VMEM((len(weights),) + weights[0].shape, weights[0].dtype),
-        ],
+        return scaled.reshape(seqs, count, width).transpose(1, 0, 2).reshape(count * seqs, width)
+    return pl.pallas_call(
+        split_kernel,
+        in_specs=[pl.BlockSpec(memory_space=pl.ANY)] * 2,
+        out_shape=jax.ShapeDtypeStruct((count * seqs, width), jnp.bfloat16),
         scratch_shapes=[
             pltpu.VMEM(rows.shape, rows.dtype),
             pltpu.VMEM(gain.shape, gain.dtype),
-            pltpu.SemaphoreType.DMA((2 + len(weights),)),
+            pltpu.SemaphoreType.DMA((2,)),
         ],
         compiler_params=room(12),
-        name="prepare",
-    )(*map(away, (rows, gain, *weights)))
+        name="split_features",
+    )(away(rows), away(gain))
 
 
 def gates_kernel(
@@ -208,13 +221,35 @@
     peers,
 ):
     term_refs = refs[:peers]
-    key_ref, value_ref, carry_out_ref, inflow_out_ref, read_ref, proj_ref, semaphore = refs[peers:]
+    rows_ref, proj_ref, semaphore = refs[peers:]
     proj_copy = pltpu.make_async_copy(proj_hbm, proj_ref, semaphore)
     proj_copy.start()
     seqs, heads, head_dim = matrix_ref.shape[:3]
     head_cols = heads * head_dim
     summed = jnp.sum(arrived_ref[...].astype(jnp.float32), axis=0) * factor_ref[...]
     summed = summed.astype(jnp.bfloat16).astype(jnp.float32)
+    queries = jnp.concatenate(
+        [
+            jnp.concatenate(
+                [
+                    summed[:, head * head_dim : (head + 1) * head_dim]
+                    if place == head
+                    else jnp.zeros((seqs, head_dim), jnp.float32)
+                    for place in range(heads)
+                ],
+                axis=1,
+            )
+            for head in range(heads)
+        ],
+        axis=0,
+    ).astype(jnp.bfloat16)
+    owner = lax.broadcasted_iota(jnp.int32, (heads * seqs, head_dim), 0) % seqs
+    reads = jnp.zeros((heads * seqs, head_dim), jnp.float32)
+    for seq in range(seqs):
+        product = jnp.dot(
+            queries, matrix_ref[seq].reshape(heads * head_dim, head_dim), preferred_element_type=jnp.float32
+        )
+        reads = jnp.where(owner == seq, product, reads)
     cells = []
     carries = carry_ref[...].T
     inflows = inflow_ref[...].T
@@ -226,19 +261,13 @@
         carry = carries[:, head : head + 1]
         inflow = inflows[:, head : head + 1]
         inflow_key = inflow * (key * head_dim ** (-0.5))
-        columns = slice(head * head_dim, (head + 1) * head_dim)
-        normal_new = carry * normal_ref[:, columns] + inflow_key
+        normal_new = carry * normal_ref[:, head, :] + inflow_key
         rows = slice(head * seqs, (head + 1) * seqs)
-        key_ref[rows, :] = key
-        value_ref[rows, :] = value
-        carry_out_ref[rows, :] = jnp.broadcast_to(carry, (seqs, head_dim))
-        inflow_out_ref[rows, :] = jnp.broadcast_to(inflow * head_dim ** (-0.5), (seqs, head_dim))
-        turned = query.T
-        for seq in range(seqs):
-            read_ref[seq : seq + 1, :] = jnp.sum(
-                turned[:, seq : seq + 1] * matrix_ref[seq, head].astype(jnp.float32), axis=0, keepdims=True
-            )
-        numer = carry * read_ref[...] + jnp.sum(query * inflow_key, axis=-1, keepdims=True) * value
+        rows_ref[0, rows, :] = key
+        rows_ref[1, rows, :] = value
+        rows_ref[2, rows, :] = jnp.broadcast_to(carry, (seqs, head_dim))
+        rows_ref[3, rows, :] = jnp.broadcast_to(inflow * head_dim ** (-0.5), (seqs, head_dim))
+        numer = carry * reads[rows] + jnp.sum(query * inflow_key, axis=-1, keepdims=True) * value
         denom = jnp.maximum(jnp.abs(jnp.sum(query * normal_new, axis=-1, keepdims=True)), 1.0)
         cells.append((numer / denom * jax.nn.sigmoid(gate)).astype(jnp.bfloat16))
     cell = jnp.concatenate(cells, axis=1)
@@ -255,18 +284,17 @@
     seqs, heads, head_dim, _ = matrix_state.shape
     wide = jnp.float32
     term = jax.ShapeDtypeStruct((seqs, w_proj.shape[1] // peers), jnp.bfloat16)
-    by_head = jax.ShapeDtypeStruct((heads * seqs, head_dim), wide)
+    by_head = jax.ShapeDtypeStruct((4, heads * seqs, head_dim), wide)
     vmem = pl.BlockSpec()
     return pl.pallas_call(
         functools.partial(cell_kernel, peers=peers),
         in_specs=[pl.BlockSpec(memory_space=pltpu.SMEM)]
         + [vmem] * 6
         + [pl.BlockSpec(memory_space=pl.ANY)],
-        out_specs=[vmem] * (peers + 4),
+        out_specs=[vmem] * (peers + 1),
         out_shape=[term] * peers
-        + [by_head] * 4,
+        + [by_head],
         scratch_shapes=[
-            pltpu.VMEM((seqs, head_dim), wide),
             pltpu.VMEM(w_proj.shape, w_proj.dtype),
             pltpu.SemaphoreType.DMA,
         ],
@@ -275,7 +303,16 @@
     )(index, held(arrived), factor, carry, inflow, held(matrix_state), normal_rows, away(w_proj))
 
 
-def update_kernel(key_ref, value_ref, carry_ref, inflow_ref, matrix_hbm, out_hbm, work_ref, loads, stores):
+def update_kernel(
+    rows_ref,
+    normal_ref,
+    matrix_hbm,
+    normal_out_ref,
+    out_hbm,
+    work_ref,
+    loads,
+    stores,
+):
     seqs, heads, head_dim, _ = matrix_hbm.shape
     block = min(8, seqs)
     wide = (block, block * head_dim)
@@ -289,13 +326,18 @@
 
     for step in range(seqs // block):
         copy(step, False).start()
+    for head in range(heads):
+        rows = slice(head * seqs, (head + 1) * seqs)
+        normal_out_ref[:, head, :] = (
+            rows_ref[2, rows, :] * normal_ref[:, head, :] + rows_ref[3, rows, :] * rows_ref[0, rows, :]
+        )
     for step in range(seqs // block):
         copy(step, False).wait()
         for head in range(heads):
             rows = pl.ds(head * seqs + step * block, block)
-            spread = jnp.where(own, jnp.concatenate([value_ref[rows, :]] * block, axis=1), 0.0)
+            spread = jnp.where(own, jnp.concatenate([rows_ref[1, rows, :]] * block, axis=1), 0.0)
             outer = jnp.dot(
-                key_ref[rows, :].T.astype(jnp.bfloat16),
+                rows_ref[0, rows, :].T.astype(jnp.bfloat16),
                 spread.astype(jnp.bfloat16),
                 preferred_element_type=jnp.float32,
             )
@@ -303,22 +345,25 @@
                 row = head * seqs + step * block + place
                 seq = step * block + place
                 work_ref[seq, head] = (
-                    carry_ref[row : row + 1, :] * work_ref[seq, head]
-                    + inflow_ref[row : row + 1, :] * outer[:, place * head_dim : (place + 1) * head_dim]
+                    rows_ref[2, row : row + 1, :] * work_ref[seq, head]
+                    + rows_ref[3, row : row + 1, :] * outer[:, place * head_dim : (place + 1) * head_dim]
                 )
         copy(step, True).start()
     for step in range(seqs // block):
         copy(step, True).wait()
 
 
-def update_matrix(key, value, carry, inflow, matrix_state):
+def update_states(rows, normal_state, matrix_state):
     anywhere = pl.BlockSpec(memory_space=pl.ANY)
     steps = matrix_state.shape[0] // min(8, matrix_state.shape[0])
     return pl.pallas_call(
         update_kernel,
-        in_specs=[pl.BlockSpec()] * 4 + [anywhere],
-        out_specs=anywhere,
-        out_shape=pltpu.HBM(matrix_state.shape, jnp.float32),
+        in_specs=[pl.BlockSpec()] * 2 + [anywhere],
+        out_specs=[pl.BlockSpec(), anywhere],
+        out_shape=[
+            jax.ShapeDtypeStruct(normal_state.shape, jnp.float32),
+            pltpu.HBM(matrix_state.shape, jnp.float32),
+        ],
         scratch_shapes=[
             pltpu.VMEM(matrix_state.shape, jnp.float32),
             pltpu.SemaphoreType.DMA((steps,)),
@@ -326,8 +371,8 @@
         ],
         compiler_params=room(12),
         cost_estimate=pl.CostEstimate(flops=1 << 23, bytes_accessed=0, transcendentals=0),
-        name="update_matrix",
-    )(key, value, carry, inflow, away(matrix_state))
+        name="update_states",
+    )(rows, normal_state, away(matrix_state))
 
 
 def expert_kernel(index_ref, *refs, peers, halves):
@@ -335,7 +380,7 @@
     chunk_refs = refs[:count]
     gain_ref, gate_ref, up_ref, down_ref = refs[count : count + 4]
     term_refs = refs[count + 4 :]
-    rows, width = chunk_refs[0].shape
+    _, width = chunk_refs[0].shape
     squares = [
         sum(
             jnp.sum(jnp.square(chunk_refs[half * peers + peer][...].astype(jnp.float32)), axis=-1, keepdims=True)
@@ -344,29 +389,23 @@
         for half in range(halves)
     ]
     factors = [lax.rsqrt(square / (peers * width) + norm_epsilon) for square in squares]
-    gate_sum = up_sum = None
-    for peer in range(peers):
-        start = pl.multiple_of((index_ref[0] ^ peer) * width, width)
-        gain = gain_ref[:, pl.ds(start, width)].astype(jnp.float32)
-        normed = jnp.concatenate(
-            [
-                (chunk_refs[half * peers + peer][...].astype(jnp.float32) * factors[half] * gain).astype(jnp.bfloat16)
-                for half in range(halves)
-            ],
-            axis=0,
-        )
-        gate_part = jnp.dot(normed, gate_ref[0, pl.ds(start, width), :], preferred_element_type=jnp.float32)
-        up_part = jnp.dot(normed, up_ref[0, pl.ds(start, width), :], preferred_element_type=jnp.float32)
-        gate_sum = gate_part if peer == 0 else gate_sum + gate_part
-        up_sum = up_part if peer == 0 else up_sum + up_part
-    inner = (jax.nn.silu(gate_sum) * up_sum).astype(jnp.bfloat16)
-    for peer in range(peers):
-        start = pl.multiple_of((index_ref[0] ^ peer) * width, width)
-        term = jnp.dot(
-            inner, down_ref[0, :, pl.ds(start, width)], preferred_element_type=jnp.float32
-        ).astype(jnp.bfloat16)
-        for half in range(halves):
-            term_refs[half * peers + peer][...] = term[half * rows : (half + 1) * rows]
+    for half in range(halves):
+        gate_sum = up_sum = None
+        for peer in range(peers):
+            columns = pl.ds(pl.multiple_of((index_ref[0] ^ peer) * width, width), width)
+            gain = gain_ref[:, columns].astype(jnp.float32)
+            chunk = chunk_refs[half * peers + peer][...].astype(jnp.float32)
+            normed = (chunk * factors[half] * gain).astype(jnp.bfloat16)
+            gate_part = jnp.dot(normed, gate_ref[0, columns, :], preferred_element_type=jnp.float32)
+            up_part = jnp.dot(normed, up_ref[0, columns, :], preferred_element_type=jnp.float32)
+            gate_sum = gate_part if peer == 0 else gate_sum + gate_part
+            up_sum = up_part if peer == 0 else up_sum + up_part
+        inner = (jax.nn.silu(gate_sum) * up_sum).astype(jnp.bfloat16)
+        for peer in range(peers):
+            columns = pl.ds(pl.multiple_of((index_ref[0] ^ peer) * width, width), width)
+            term_refs[half * peers + peer][...] = jnp.dot(
+                inner, down_ref[0, :, columns], preferred_element_type=jnp.float32
+            ).astype(jnp.bfloat16)
 
 
 def expert_step(index, chunks, gain, gate, up, down, peers):
@@ -463,8 +502,6 @@
     tp_index = lax.axis_index("tp")
     seq_dev = tokens.shape[0]
     model_width = tokens.shape[1]
-    heads_dev = matrix_state.shape[1]
-    head_dim = matrix_state.shape[2]
     head_cols = w_query.shape[1]
     top_count = route_ids.shape[1]
     experts = ep_count // 2
@@ -472,9 +509,9 @@
     every_row = capacity == seq_dev
     col_width = model_width // tp_count
     index = jnp.stack([tp_index, lax.axis_index("ep") % 2]).astype(jnp.int32)
-    blocks, own_weights = prepare(tokens, gain_mix, (w_query, w_key, w_value, w_outgate), experts)
-    with jax.named_scope("pair"):
-        other_weights = swap(own_weights, 1, 0)
+    own_weights = pack((w_query, w_key, w_value, w_outgate))
+    other_weights = swap(own_weights, 1, 0)
+    blocks = split_features(tokens, gain_mix, experts)
     same_half = [list(range(half, ep_count, 2)) for half in range(2)]
 
     def exchange(rows):
@@ -482,10 +519,10 @@
             rows, "ep", split_axis=0, concat_axis=0, tiled=True, axis_index_groups=same_half
         )
 
-    with jax.named_scope("spread"):
-        foreign = exchange(blocks)
+    blocks, index = lax.optimization_barrier((blocks, index))
+    foreign = exchange(blocks)
     terms = project(index, foreign, own_weights, other_weights)
-    (held_state,) = load(terms, (matrix_state,), 1 << 22, narrowed=1)
+    (held_state,) = load(terms, (matrix_state,), narrowed=1)
     arrived = exchange(terms)
     factor, carry, inflow, stab_turned = gates(
         terms, index, tokens, gain_mix, w_ingate, w_forget, bias_in, bias_forget, stab_state
@@ -505,20 +542,18 @@
         carry,
         inflow,
         held_state,
-        normal_state.reshape(seq_dev, head_cols),
+        normal_state,
         w_proj,
         tp_count,
     )
-    out_terms, state_rows = cell_outs[:tp_count], cell_outs[tp_count:]
-    key_wide = (state_rows[3] * state_rows[0]).reshape(heads_dev, seq_dev, -1).transpose(1, 0, 2)
-    normal_new = carry.T[:, :, None] * normal_state + key_wide
-    matrix_new = update_matrix(*state_rows, matrix_state)
+    *out_terms, state_rows = cell_outs
+    normal_new, matrix_new = update_states(state_rows, normal_state, matrix_state)
     own_tokens = lax.dynamic_slice_in_dim(tokens, tp_index * col_width, col_width, 1)
     attended = out_terms[0].astype(jnp.float32)
     for peer in range(1, tp_count):
         attended = attended + swap(out_terms[peer], 0, peer).astype(jnp.float32)
     own_resid = (own_tokens.astype(jnp.float32) + attended).astype(jnp.bfloat16)
-    held_experts = load(held(state_rows[0]), (w_exp_gate, w_exp_up), 1 << 22)
+    held_experts = load(held(state_rows), (w_exp_gate, w_exp_up))
     own_resid, *held_experts = lax.optimization_barrier((own_resid, *held_experts))
     if every_row:
         packed = jnp.broadcast_to(own_resid, (experts, seq_dev, col_width))
@@ -526,7 +561,7 @@
         table = dispatch_table(route_ids, experts, capacity)
         packed = pack_rows(table, own_resid, top_count, experts, capacity)
     received = exchange(packed.reshape(experts * capacity, col_width))
-    (held_down,) = load(received, (w_exp_down,), 1 << 22)
+    (held_down,) = load(received, (w_exp_down,))
     chunks, held_down = gather_chunks(received, tp_count, held_down)
     down_terms = expert_step(
         index,
@@ -537,7 +572,7 @@
         tp_count,
     )
     half_share = sum_chunks(down_terms, tp_count).astype(jnp.bfloat16)
-    half_share, matrix_new = lax.optimization_barrier((half_share, matrix_new))
+    half_share, matrix_new, normal_new = lax.optimization_barrier((half_share, matrix_new, normal_new))
     returned = exchange(half_share).astype(jnp.float32).reshape(experts, capacity, col_width)
     if every_row:
         routed = jnp.sum(returned * shares.T[:, :, None], axis=0)

time: 83.4 us -> 82.7 us (level)
  blocking collectives: 8.87 us -> 29 us
  waiting for transfers between devices: 24 us -> 12.4 us
  starting transfers between devices: 26.6 us -> 18.8 us
  other arithmetic: 2.41 us -> 1.04 us
    all_to_all x1 -> x3, blocking collectives: 8.87 us -> 29 us  [exchange(): lax.all_to_all(rows, 'ep', split_axis=0, concat_axis=0, tiled=True, axis_...]
    all_to_all x3 -> x1, waiting for transfers between devices: 15.6 us -> 4.12 us  [exchange(): lax.all_to_all(rows, 'ep', split_axis=0, concat_axis=0, tiled=True, axis_...]
    all_to_all x3 -> x1, starting transfers between devices: 13.3 us -> 5.09 us  [exchange(): lax.all_to_all(rows, 'ep', split_axis=0, concat_axis=0, tiled=True, axis_...]
    pallas_call x2 -> x3, Pallas kernels: 5.61 us -> 6.44 us  [the longest x1 4.26 us: update_states(): pl.pallas_call(update_kernel, in_specs=[pl.BlockSpec()] * 2 + [anywhere],...]
  transfers between devices with their start and end apart: 21 -> 19, of which waited for: 11 -> 11; matrix products, arithmetic and copies ran while one was open for 1% -> 0% of each run, Pallas kernels for 13% -> 15%
where the time goes in v4:
time: 82.7 us; the launch traced here: 82.3 us
  blocking collectives  29 us (35%)
  Pallas kernels  20.1 us (24%)
  starting transfers between devices  18.8 us (23%)
  waiting for transfers between devices  12.4 us (15%)
  other arithmetic  1.04 us (1%)
  between operations  0.94 us (1%)
    all_to_all x3, blocking collectives, exchange(): lax.all_to_all(rows, 'ep', split_axis=0, concat_axis=0, tiled=True, axis_...  29 us
    ppermute x18, starting transfers between devices, swap(): lax.ppermute(value, ('ep', 'tp'), [(i, i ^ away) for i in range(ep_count...  13.8 us
    ppermute x18, waiting for transfers between devices, swap(): lax.ppermute(value, ('ep', 'tp'), [(i, i ^ away) for i in range(ep_count...  8.24 us
    pallas_call x3, Pallas kernels, load(): pl.pallas_call(functools.partial(load_kernel, count=len(arrays), narrowed...  5.8 us
    all_to_all x1, starting transfers between devices, exchange(): lax.all_to_all(rows, 'ep', split_axis=0, concat_axis=0, tiled=True, axis_...  5.09 us
    pallas_call x1, Pallas kernels, update_states(): pl.pallas_call(update_kernel, in_specs=[pl.BlockSpec()] * 2 + [anywhere],...  4.26 us
    all_to_all x1, waiting for transfers between devices, exchange(): lax.all_to_all(rows, 'ep', split_axis=0, concat_axis=0, tiled=True, axis_...  4.12 us
    pallas_call x1, Pallas kernels, expert_step(): pl.pallas_call(functools.partial(expert_kernel, peers=peers, halves=len(c...  2.75 us
  transfers between devices with their start and end apart: 19, of which 11 were waited for; matrix products, arithmetic and copies ran while one was open for 0% of the time, Pallas kernels for 15%

profile of v4, /device:TPU:0, one launch (start us, length us, event | category | flops | bytes accessed | tf_op | source)
XLA Modules:
  0.0 82.3 jit_solution(3651692541751639586)
XLA Ops:
  0.6 0.0 copy-start
  0.6 0.0 copy-start.4
  0.7 0.0 copy-start.9
  0.7 0.0 copy-start.10
  0.7 0.0 copy-start.5
  0.7 0.0 copy-start.7
  0.7 0.0 copy-start.6
  0.7 0.0 copy-start.3
  0.7 1.2 %pack.1.own_ref = bf16[4,256,256]{2,1,0:T(8,128)(2,1)S(1)} custom-call(bf16[256,256]{1,0:T(8,128)(2,1)} %refs_0_.4, bf16[256,256]{1,0:T(8,128)(2,1)} %refs_1_.2, bf16[256,256]{1,0:T(8,128)(2,1)} %refs_2_.1, bf16[256,256]{1,0:T(8,128)(2,1)} %refs_3_.1), custom_call_target="tpu_custom_call" | custom-call | tf_op jit(solution)/shard_map/pack/pallas_call | solution.py:77
  2.0 3.1 %collective-permute-start = (bf16[4,256,256]{2,1,0:T(8,128)(2,1)S(1)}, bf16[4,256,256]{2,1,0:T(8,128)(2,1)S(1)}, u32[]{:S(2)}, u32[]{:S(2)}) collective-permute-start(bf16[4,256,256]{2,1,0:T(8,128)(2,1)S(1)} %pack.1.own_ref), channel_id=1, source_target_pairs={{0,4},{1,5},{2,6},{3,7},{4,0},{5,1},{6,2},{7,3},{8,12},{9,13},{10,... | collective-permute-start | bytes 1572872 | tf_op jit(solution)/shard_map/ppermute | solution.py:448
  5.0 1.0 %split_features.1 = bf16[128,512]{1,0:T(8,128)(2,1)S(1)} custom-call(bf16[32,2048]{1,0:T(8,128)(2,1)} %rows_ref.1, bf16[2048]{0:T(1024)(128)(2,1)} %gain_ref.1), custom_call_target="tpu_custom_call" | custom-call | tf_op jit(solution)/shard_map/split_features/pallas_call | solution.py:111
  6.0 0.1 pad_add_fusion.index_ref
  6.1 10.6 %all_to_all.37 = bf16[4,32,512]{2,1,0:T(8,128)(2,1)S(1)} all-to-all(bf16[4,32,512]{2,1,0:T(8,128)(2,1)S(1)} %bitcast.18), channel_id=1, replica_groups={{0,8,16,24},{4,12,20,28},{1,9,17,25},{5,13,21,29},{2,10,18,26},{6,14,22..., dimensions={0} | all-to-all | bytes 262144 | tf_op jit(solution)/shard_map/all_to_all | solution.py:518
  16.7 0.2 collective-permute-done.other_ref
  16.9 1.6 %project.1._ = bf16[128,1024]{1,0:T(8,128)(2,1)} custom-call(s32[2]{0:T(128)S(1)} %pad_add_fusion.index_ref, bf16[128,512]{1,0:T(8,128)(2,1)S(1)} %bitcast.19, bf16[4,256,256]{2,1,0:T(8,128)(2,1)S(1)} %pack.1.own_ref, bf16[4,256,256]{2,1,0:T(8,128)(2,1)S(1)} %collective-permute-done.other_ref), custom_call_target="tpu_custom_call" | custom-call | tf_op jit(solution)/shard_map/project/pallas_call | solution.py:202
  18.5 5.1 %all-to-all-start.1 = ((bf16[4,32,1024]{2,1,0:T(8,128)(2,1)}), bf16[4,32,1024]{2,1,0:T(8,128)(2,1)S(1)}, u32[]{:S(2)}, u32[]{:S(2)}) async-start(bf16[4,32,1024]{2,1,0:T(8,128)(2,1)} %bitcast.4), calls=%async_computation.1 | async-start | bytes 524288 | tf_op jit(solution)/shard_map/all_to_all | solution.py:518
  23.6 0.0 copy-done.10
  23.7 1.4 %gates.1 = (f32[32,1]{1,0:T(8,128)S(1)}, f32[2,32]{1,0:T(2,128)S(1)}, f32[2,32]{1,0:T(2,128)S(1)}, f32[2,32]{1,0:T(2,128)}) custom-call(s32[2]{0:T(128)S(1)} %pad_add_fusion.index_ref, bf16[128,1024]{1,0:T(8,128)(2,1)} %project.1._, bf16[32,2048]{1,0:T(8,128)(2,1)S(1)} %copy-done, bf16[2048]{0:T(1024)(128)(2,1)S(1)} %copy-done.4, ...), custom_call_target="tpu_custom_call" | custom-call | flops 4194304 | tf_op jit(solution)/shard_map/gates/pallas_call | solution.py:167
  25.2 2.5 %load.3.matrix_ref = bf16[32,2,128,128]{3,2,1,0:T(8,128)(2,1)S(1)} custom-call(bf16[128,1024]{1,0:T(8,128)(2,1)} %project.1._, f32[32,2,128,128]{3,2,1,0:T(8,128)} %matrix_hbm.1), custom_call_target="tpu_custom_call" | custom-call | flops 4194304 | tf_op jit(solution)/shard_map/load/pallas_call | solution.py:43
  27.7 4.1 %all-to-all-done.1.arrived_ref = bf16[4,32,1024]{2,1,0:T(8,128)(2,1)S(1)} async-done(((bf16[4,32,1024]{2,1,0:T(8,128)(2,1)}), bf16[4,32,1024]{2,1,0:T(8,128)(2,1)S(1)}, u32[]{:S(2)}, u32[]{:S(2)}) %all-to-all-start.1) | async-done | bytes 262176 | tf_op jit(solution)/shard_map/all_to_all | solution.py:518
  31.8 2.1 %cell_step.1 = (bf16[32,512]{1,0:T(8,128)(2,1)S(1)}, bf16[32,512]{1,0:T(8,128)(2,1)S(1)}, bf16[32,512]{1,0:T(8,128)(2,1)S(1)}, bf16[32,512]{1,0:T(8,128)(2,1)S(1)}, f32[4,64,128]{2,1,0:T(8,128)S(1)}) custom-call(s32[2]{0:T(128)S(1)} %pad_add_fusion.index_ref, bf16[4,32,1024]{2,1,0:T(8,128)(2,1)S(1)} %all-to-all-done.1.arrived_ref, ...), custom_call_target="tpu_custom_call" | custom-call | tf_op jit(solution)/shard_map/cell_step/pallas_call | solution.py:289
  33.9 0.1 collective-permute-start.1
  33.9 1.6 %collective-permute-start.2 = (bf16[32,512]{1,0:T(8,128)(2,1)S(1)}, bf16[32,512]{1,0:T(8,128)(2,1)S(1)}, u32[]{:S(2)}, u32[]{:S(2)}) collective-permute-start(bf16[32,512]{1,0:T(8,128)(2,1)S(1)} %get-tuple-element.47), channel_id=1, source_target_pairs={{0,2},{1,3},{2,0},{3,1},{4,6},{5,7},{6,4},{7,5},{8,10},{9,11},{10,... | collective-permute-start | bytes 98312 | tf_op jit(solution)/shard_map/ppermute | solution.py:448
  35.5 0.3 collective-permute-start.3
  35.8 1.9 %load.4 = (bf16[1,2048,384]{2,1,0:T(8,128)(2,1)S(1)}, bf16[1,2048,384]{2,1,0:T(8,128)(2,1)S(1)}) custom-call(f32[4,64,128]{2,1,0:T(8,128)S(1)} %get-tuple-element.49._.rows_ref, bf16[1,2048,384]{2,1,0:T(8,128)(2,1)} %refs_0_.6, bf16[1,2048,384]{2,1,0:T(8,128)(2,1)} %refs_1_.3), custom_call_target="tpu_custom_call" | custom-call | flops 4194304 | tf_op jit(solution)/shard_map/load/pallas_call | solution.py:43
  37.7 0.0 collective-permute-done.1
  37.7 0.2 collective-permute-done.2
  37.9 0.9 %collective-permute-done.3 = bf16[32,512]{1,0:T(8,128)(2,1)S(1)} collective-permute-done((bf16[32,512]{1,0:T(8,128)(2,1)S(1)}, bf16[32,512]{1,0:T(8,128)(2,1)S(1)}, u32[]{:S(2)}, u32[]{:S(2)}) %collective-permute-start.3) | collective-permute-done | bytes 32800 | tf_op jit(solution)/shard_map/ppermute | solution.py:448
  38.9 8.8 %all_to_all.38 = bf16[4,32,512]{2,1,0:T(8,128)(2,1)S(1)} all-to-all(bf16[4,32,512]{2,1,0:T(8,128)(2,1)S(1)} %broadcast_in_dim.22), channel_id=1, replica_groups={{0,8,16,24},{4,12,20,28},{1,9,17,25},{5,13,21,29},{2,10,18,26},{6,14,22..., dimensions={0} | all-to-all | bytes 262144 | tf_op jit(solution)/shard_map/all_to_all | solution.py:518
  47.7 0.9 %collective-permute-start.5 = (bf16[128,512]{1,0:T(8,128)(2,1)S(1)}, bf16[128,512]{1,0:T(8,128)(2,1)S(1)}, u32[]{:S(2)}, u32[]{:S(2)}) collective-permute-start(bf16[128,512]{1,0:T(8,128)(2,1)S(1)} %bitcast.12), channel_id=1, source_target_pairs={{0,2},{1,3},{2,0},{3,1},{4,6},{5,7},{6,4},{7,5},{8,10},{9,11},{10,... | collective-permute-start | bytes 393224 | tf_op jit(solution)/shard_map/ppermute | solution.py:448
  48.6 2.1 %collective-permute-start.9 = (bf16[128,512]{1,0:T(8,128)(2,1)S(1)}, bf16[128,512]{1,0:T(8,128)(2,1)S(1)}, u32[]{:S(2)}, u32[]{:S(2)}) collective-permute-start(bf16[128,512]{1,0:T(8,128)(2,1)S(1)} %bitcast.13), channel_id=1, source_target_pairs={{0,6},{1,7},{2,4},{3,5},{4,2},{5,3},{6,0},{7,1},{8,14},{9,15},{10,... | collective-permute-start | bytes 393224 | tf_op jit(solution)/shard_map/ppermute | solution.py:448
  50.7 0.5 collective-permute-start.7
  51.2 0.0 collective-permute-start.4
  51.2 1.4 %load.5.refs_11_ = bf16[1,384,2048]{2,1,0:T(8,128)(2,1)S(1)} custom-call(bf16[128,512]{1,0:T(8,128)(2,1)S(1)} %bitcast.16, bf16[1,384,2048]{2,1,0:T(8,128)(2,1)} %refs_0_.7), custom_call_target="tpu_custom_call" | custom-call | flops 4194304 | tf_op jit(solution)/shard_map/load/pallas_call | solution.py:43
  52.6 0.7 collective-permute-done.5.refs_2_
  53.3 2.3 %collective-permute-done.9.refs_6_ = bf16[128,512]{1,0:T(8,128)(2,1)S(1)} collective-permute-done((bf16[128,512]{1,0:T(8,128)(2,1)S(1)}, bf16[128,512]{1,0:T(8,128)(2,1)S(1)}, u32[]{:S(2)}, u32[]{:S(2)}) %collective-permute-start.9) | collective-permute-done | bytes 131104 | tf_op jit(solution)/shard_map/ppermute | solution.py:448
  55.6 0.0 collective-permute-start.10
  55.6 1.3 %collective-permute-done.7.refs_4_ = bf16[128,512]{1,0:T(8,128)(2,1)S(1)} collective-permute-done((bf16[128,512]{1,0:T(8,128)(2,1)S(1)}, bf16[128,512]{1,0:T(8,128)(2,1)S(1)}, u32[]{:S(2)}, u32[]{:S(2)}) %collective-permute-start.7) | collective-permute-done | bytes 131104 | tf_op jit(solution)/shard_map/ppermute | solution.py:448
  56.9 0.0 collective-permute-start.8
  56.9 0.5 collective-permute-start.6
  57.4 0.0 collective-permute-done.4.refs_1_
  57.4 0.0 collective-permute-done.10.refs_7_
  57.4 0.8 collective-permute-done.8.refs_5_
  58.2 0.2 collective-permute-done.6.refs_3_
  58.4 2.7 %expert_step.1 = (bf16[128,512]{1,0:T(8,128)(2,1)S(1)}, bf16[128,512]{1,0:T(8,128)(2,1)S(1)}, bf16[128,512]{1,0:T(8,128)(2,1)S(1)}, bf16[128,512]{1,0:T(8,128)(2...) custom-call(s32[2]{0:T(128)S(1)} %pad_add_fusion.index_ref, ...), custom_call_target="tpu_custom_call" | custom-call | tf_op jit(solution)/shard_map/expert_step/pallas_call | solution.py:413
  61.2 0.4 collective-permute-start.12
  61.6 0.2 collective-permute-start.11
  61.7 0.3 collective-permute-start.14
  62.1 0.2 collective-permute-start.16
  62.3 0.3 collective-permute-done.12
  62.6 1.0 %collective-permute-start.13 = (bf16[128,512]{1,0:T(8,128)(2,1)S(1)}, bf16[128,512]{1,0:T(8,128)(2,1)S(1)}, u32[]{:S(2)}, u32[]{:S(2)}) collective-permute-start(bf16[128,512]{1,0:T(8,128)(2,1)S(1)} %add_convert_fusion.3), channel_id=1, source_target_pairs={{0,2},{1,3},{2,0},{3,1},{4,6},{5,7},{6,4},{7,5},{8,10},{9,11},{10,... | collective-permute-start | bytes 393224 | tf_op jit(solution)/shard_map/ppermute | solution.py:448
  63.6 0.0 collective-permute-done.14
  63.6 0.7 collective-permute-start.15
  64.4 0.0 collective-permute-done.16
  64.4 2.0 %collective-permute-start.17 = (bf16[128,512]{1,0:T(8,128)(2,1)S(1)}, bf16[128,512]{1,0:T(8,128)(2,1)S(1)}, u32[]{:S(2)}, u32[]{:S(2)}) collective-permute-start(bf16[128,512]{1,0:T(8,128)(2,1)S(1)} %add_convert_fusion.1), channel_id=1, source_target_pairs={{0,6},{1,7},{2,4},{3,5},{4,2},{5,3},{6,0},{7,1},{8,14},{9,15},{10,... | collective-permute-start | bytes 393224 | tf_op jit(solution)/shard_map/ppermute | solution.py:448
  66.4 4.3 %update_states.1 = (f32[32,2,128]{2,1,0:T(2,128)}, f32[32,2,128,128]{3,2,1,0:T(8,128)}) custom-call(f32[4,64,128]{2,1,0:T(8,128)S(1)} %get-tuple-element.49._.rows_ref, f32[32,2,128]{2,1,0:T(2,128)S(1)} %copy-done.1, f32[32,2,128,128]{3,2,1,0:T(8,128)} %matrix_hbm.1), custom_call_target="tpu_custom_call" | custom-call | flops 8388608 | tf_op jit(solution)/shard_map/update_states/pallas_call | solution.py:359
  70.7 0.0 collective-permute-done.11
  70.7 0.0 collective-permute-done.13
  70.7 1.3 %collective-permute-done.15 = bf16[128,512]{1,0:T(8,128)(2,1)S(1)} collective-permute-done((bf16[128,512]{1,0:T(8,128)(2,1)S(1)}, bf16[128,512]{1,0:T(8,128)(2,1)S(1)}, u32[]{:S(2)}, u32[]{:S(2)}) %collective-permute-start.15) | collective-permute-done | bytes 131104 | tf_op jit(solution)/shard_map/ppermute | solution.py:448
  71.9 0.0 collective-permute-done.17
  71.9 0.1 add_convert_fusion
  72.0 9.5 %all_to_all.39 = bf16[4,32,512]{2,1,0:T(8,128)(2,1)S(1)} all-to-all(bf16[4,32,512]{2,1,0:T(8,128)(2,1)S(1)} %bitcast.23), channel_id=1, replica_groups={{0,8,16,24},{4,12,20,28},{1,9,17,25},{5,13,21,29},{2,10,18,26},{6,14,22..., dimensions={0} | all-to-all | bytes 262144 | tf_op jit(solution)/shard_map/all_to_all | solution.py:518
  81.6 0.1 multiply_reduce_fusion
  81.7 0.6 add_convert_fusion.4
  (22 shorter events, 0.2 us)
Async XLA Ops:
  0.6 23.0 %copy-start = (bf16[32,2048]{1,0:T(8,128)(2,1)S(1)}, bf16[32,2048]{1,0:T(8,128)(2,1)}, u32[]{:S(2)}) copy-start(bf16[32,2048]{1,0:T(8,128)(2,1)} %rows_ref.1) | copy-start | bytes 393220
  0.6 23.0 %copy-start.4 = (bf16[2048]{0:T(1024)(128)(2,1)S(1)}, bf16[2048]{0:T(1024)(128)(2,1)}, u32[]{:S(2)}) copy-start(bf16[2048]{0:T(1024)(128)(2,1)} %gain_ref.1) | copy-start | bytes 12292
  0.7 22.9 %copy-start.9 = (f32[32,2]{0,1:T(2,128)S(1)}, f32[32,2]{0,1:T(2,128)}, u32[]{:S(2)}) copy-start(f32[32,2]{0,1:T(2,128)} %param.36) | copy-start | bytes 772
  0.7 23.0 %copy-start.10 = (s32[32,2]{0,1:T(2,128)S(1)}, s32[32,2]{0,1:T(2,128)}, u32[]{:S(2)}) copy-start(s32[32,2]{0,1:T(2,128)} %param.35) | copy-start | bytes 772
  0.7 23.0 %copy-start.5 = (f32[32,2]{0,1:T(2,128)S(1)}, f32[32,2]{0,1:T(2,128)}, u32[]{:S(2)}) copy-start(f32[32,2]{0,1:T(2,128)} %param.34) | copy-start | bytes 772
  0.7 23.0 %copy-start.7 = (f32[8]{0:T(128)S(1)}, f32[8]{0:T(128)}, u32[]{:S(2)}) copy-start(f32[8]{0:T(128)} %bias_forget_ref.1) | copy-start | bytes 100
  0.7 23.0 %copy-start.6 = (f32[8]{0:T(128)S(1)}, f32[8]{0:T(128)}, u32[]{:S(2)}) copy-start(f32[8]{0:T(128)} %bias_in_ref.1) | copy-start | bytes 100
  0.7 23.0 %copy-start.3 = (bf16[2048,8]{0,1:T(8,128)(2,1)S(1)}, bf16[2048,8]{0,1:T(8,128)(2,1)}, u32[]{:S(2)}) copy-start(bf16[2048,8]{0,1:T(8,128)(2,1)} %param.28) | copy-start | bytes 98308
  0.7 23.0 %copy-start.2 = (bf16[2048,8]{0,1:T(8,128)(2,1)S(1)}, bf16[2048,8]{0,1:T(8,128)(2,1)}, u32[]{:S(2)}) copy-start(bf16[2048,8]{0,1:T(8,128)(2,1)} %param.27) | copy-start | bytes 98308
  2.0 15.0 %collective-permute-start = (bf16[4,256,256]{2,1,0:T(8,128)(2,1)S(1)}, bf16[4,256,256]{2,1,0:T(8,128)(2,1)S(1)}, u32[]{:S(2)}, u32[]{:S(2)}) collective-permute-start(bf16[4,256,256]{2,1,0:T(8,128)(2,1)S(1)} %pack.1.own_ref), channel_id=1, source_target_pairs={{0,4},{1,5},{2,6},{3,7},{4,0},{5,1},{6,2},{7,3},{8,12},{9,13},{10,... | collective-permute-start | bytes 1572872 | tf_op jit(solution)/shard_map/ppermute | solution.py:448
  18.5 13.3 %all-to-all-start.1 = ((bf16[4,32,1024]{2,1,0:T(8,128)(2,1)}), bf16[4,32,1024]{2,1,0:T(8,128)(2,1)S(1)}, u32[]{:S(2)}, u32[]{:S(2)}) async-start(bf16[4,32,1024]{2,1,0:T(8,128)(2,1)} %bitcast.4), calls=%async_computation.1 | async-start | bytes 524288 | tf_op jit(solution)/shard_map/all_to_all | solution.py:518
  25.2 6.6 %copy-start.1 = (f32[32,2,128]{2,1,0:T(2,128)S(1)}, f32[32,2,128]{2,1,0:T(2,128)}, u32[]{:S(2)}) copy-start(f32[32,2,128]{2,1,0:T(2,128)} %normal_ref.3) | copy-start | bytes 98308
  33.9 3.8 %collective-permute-start.1 = (bf16[32,512]{1,0:T(8,128)(2,1)S(1)}, bf16[32,512]{1,0:T(8,128)(2,1)S(1)}, u32[]{:S(2)}, u32[]{:S(2)}) collective-permute-start(bf16[32,512]{1,0:T(8,128)(2,1)S(1)} %get-tuple-element.46), channel_id=1, source_target_pairs={{0,1},{1,0},{2,3},{3,2},{4,5},{5,4},{6,7},{7,6},{8,9},{9,8},{10,11... | collective-permute-start | bytes 98312 | tf_op jit(solution)/shard_map/ppermute | solution.py:448
  33.9 4.0 %collective-permute-start.2 = (bf16[32,512]{1,0:T(8,128)(2,1)S(1)}, bf16[32,512]{1,0:T(8,128)(2,1)S(1)}, u32[]{:S(2)}, u32[]{:S(2)}) collective-permute-start(bf16[32,512]{1,0:T(8,128)(2,1)S(1)} %get-tuple-element.47), channel_id=1, source_target_pairs={{0,2},{1,3},{2,0},{3,1},{4,6},{5,7},{6,4},{7,5},{8,10},{9,11},{10,... | collective-permute-start | bytes 98312 | tf_op jit(solution)/shard_map/ppermute | solution.py:448
  35.5 3.4 %collective-permute-start.3 = (bf16[32,512]{1,0:T(8,128)(2,1)S(1)}, bf16[32,512]{1,0:T(8,128)(2,1)S(1)}, u32[]{:S(2)}, u32[]{:S(2)}) collective-permute-start(bf16[32,512]{1,0:T(8,128)(2,1)S(1)} %get-tuple-element.48), channel_id=1, source_target_pairs={{0,3},{1,2},{2,1},{3,0},{4,7},{5,6},{6,5},{7,4},{8,11},{9,10},{10,... | collective-permute-start | bytes 98312 | tf_op jit(solution)/shard_map/ppermute | solution.py:448
  47.7 9.7 %copy-start.8 = (bf16[2048]{0:T(1024)(128)(2,1)S(1)}, bf16[2048]{0:T(1024)(128)(2,1)}, u32[]{:S(2)}) copy-start(bf16[2048]{0:T(1024)(128)(2,1)} %param.22) | copy-start | bytes 12292
  47.7 5.6 %collective-permute-start.5 = (bf16[128,512]{1,0:T(8,128)(2,1)S(1)}, bf16[128,512]{1,0:T(8,128)(2,1)S(1)}, u32[]{:S(2)}, u32[]{:S(2)}) collective-permute-start(bf16[128,512]{1,0:T(8,128)(2,1)S(1)} %bitcast.12), channel_id=1, source_target_pairs={{0,2},{1,3},{2,0},{3,1},{4,6},{5,7},{6,4},{7,5},{8,10},{9,11},{10,... | collective-permute-start | bytes 393224 | tf_op jit(solution)/shard_map/ppermute | solution.py:448
  48.6 7.0 %collective-permute-start.9 = (bf16[128,512]{1,0:T(8,128)(2,1)S(1)}, bf16[128,512]{1,0:T(8,128)(2,1)S(1)}, u32[]{:S(2)}, u32[]{:S(2)}) collective-permute-start(bf16[128,512]{1,0:T(8,128)(2,1)S(1)} %bitcast.13), channel_id=1, source_target_pairs={{0,6},{1,7},{2,4},{3,5},{4,2},{5,3},{6,0},{7,1},{8,14},{9,15},{10,... | collective-permute-start | bytes 393224 | tf_op jit(solution)/shard_map/ppermute | solution.py:448
  50.7 6.2 %collective-permute-start.7 = (bf16[128,512]{1,0:T(8,128)(2,1)S(1)}, bf16[128,512]{1,0:T(8,128)(2,1)S(1)}, u32[]{:S(2)}, u32[]{:S(2)}) collective-permute-start(bf16[128,512]{1,0:T(8,128)(2,1)S(1)} %bitcast.14), channel_id=1, source_target_pairs={{0,4},{1,5},{2,6},{3,7},{4,0},{5,1},{6,2},{7,3},{8,12},{9,13},{10,... | collective-permute-start | bytes 393224 | tf_op jit(solution)/shard_map/ppermute | solution.py:448
  51.2 6.2 %collective-permute-start.4 = (bf16[128,512]{1,0:T(8,128)(2,1)S(1)}, bf16[128,512]{1,0:T(8,128)(2,1)S(1)}, u32[]{:S(2)}, u32[]{:S(2)}) collective-permute-start(bf16[128,512]{1,0:T(8,128)(2,1)S(1)} %bitcast.15), channel_id=1, source_target_pairs={{0,1},{1,0},{2,3},{3,2},{4,5},{5,4},{6,7},{7,6},{8,9},{9,8},{10,11... | collective-permute-start | bytes 393224 | tf_op jit(solution)/shard_map/ppermute | solution.py:448
  55.6 1.8 %collective-permute-start.10 = (bf16[128,512]{1,0:T(8,128)(2,1)S(1)}, bf16[128,512]{1,0:T(8,128)(2,1)S(1)}, u32[]{:S(2)}, u32[]{:S(2)}) collective-permute-start(bf16[128,512]{1,0:T(8,128)(2,1)S(1)} %collective-permute-done.9.refs_6_), channel_id=1, source_target_pairs={{0,1},{1,0},{2,3},{3,2},{4,5},{5,4},{6,7},{7,6},{8,9},{9,8},{10,11... | collective-permute-start | bytes 393224 | tf_op jit(solution)/shard_map/ppermute | solution.py:448
  56.9 1.3 %collective-permute-start.8 = (bf16[128,512]{1,0:T(8,128)(2,1)S(1)}, bf16[128,512]{1,0:T(8,128)(2,1)S(1)}, u32[]{:S(2)}, u32[]{:S(2)}) collective-permute-start(bf16[128,512]{1,0:T(8,128)(2,1)S(1)} %collective-permute-done.7.refs_4_), channel_id=1, source_target_pairs={{0,1},{1,0},{2,3},{3,2},{4,5},{5,4},{6,7},{7,6},{8,9},{9,8},{10,11... | collective-permute-start | bytes 393224 | tf_op jit(solution)/shard_map/ppermute | solution.py:448
  56.9 1.5 %collective-permute-start.6 = (bf16[128,512]{1,0:T(8,128)(2,1)S(1)}, bf16[128,512]{1,0:T(8,128)(2,1)S(1)}, u32[]{:S(2)}, u32[]{:S(2)}) collective-permute-start(bf16[128,512]{1,0:T(8,128)(2,1)S(1)} %collective-permute-done.5.refs_2_), channel_id=1, source_target_pairs={{0,1},{1,0},{2,3},{3,2},{4,5},{5,4},{6,7},{7,6},{8,9},{9,8},{10,11... | collective-permute-start | bytes 393224 | tf_op jit(solution)/shard_map/ppermute | solution.py:448
  61.2 1.4 %collective-permute-start.12 = (bf16[128,512]{1,0:T(8,128)(2,1)S(1)}, bf16[128,512]{1,0:T(8,128)(2,1)S(1)}, u32[]{:S(2)}, u32[]{:S(2)}) collective-permute-start(bf16[128,512]{1,0:T(8,128)(2,1)S(1)} %get-tuple-element.60), channel_id=1, source_target_pairs={{0,1},{1,0},{2,3},{3,2},{4,5},{5,4},{6,7},{7,6},{8,9},{9,8},{10,11... | collective-permute-start | bytes 393224 | tf_op jit(solution)/shard_map/ppermute | solution.py:448
  61.6 9.1 %collective-permute-start.11 = (bf16[128,512]{1,0:T(8,128)(2,1)S(1)}, bf16[128,512]{1,0:T(8,128)(2,1)S(1)}, u32[]{:S(2)}, u32[]{:S(2)}) collective-permute-start(bf16[128,512]{1,0:T(8,128)(2,1)S(1)} %get-tuple-element.58), channel_id=1, source_target_pairs={{0,1},{1,0},{2,3},{3,2},{4,5},{5,4},{6,7},{7,6},{8,9},{9,8},{10,11... | collective-permute-start | bytes 393224 | tf_op jit(solution)/shard_map/ppermute | solution.py:448
  61.7 1.8 %collective-permute-start.14 = (bf16[128,512]{1,0:T(8,128)(2,1)S(1)}, bf16[128,512]{1,0:T(8,128)(2,1)S(1)}, u32[]{:S(2)}, u32[]{:S(2)}) collective-permute-start(bf16[128,512]{1,0:T(8,128)(2,1)S(1)} %get-tuple-element.62), channel_id=1, source_target_pairs={{0,1},{1,0},{2,3},{3,2},{4,5},{5,4},{6,7},{7,6},{8,9},{9,8},{10,11... | collective-permute-start | bytes 393224 | tf_op jit(solution)/shard_map/ppermute | solution.py:448
  62.1 2.3 %collective-permute-start.16 = (bf16[128,512]{1,0:T(8,128)(2,1)S(1)}, bf16[128,512]{1,0:T(8,128)(2,1)S(1)}, u32[]{:S(2)}, u32[]{:S(2)}) collective-permute-start(bf16[128,512]{1,0:T(8,128)(2,1)S(1)} %get-tuple-element.64), channel_id=1, source_target_pairs={{0,1},{1,0},{2,3},{3,2},{4,5},{5,4},{6,7},{7,6},{8,9},{9,8},{10,11... | collective-permute-start | bytes 393224 | tf_op jit(solution)/shard_map/ppermute | solution.py:448
  62.6 8.1 %collective-permute-start.13 = (bf16[128,512]{1,0:T(8,128)(2,1)S(1)}, bf16[128,512]{1,0:T(8,128)(2,1)S(1)}, u32[]{:S(2)}, u32[]{:S(2)}) collective-permute-start(bf16[128,512]{1,0:T(8,128)(2,1)S(1)} %add_convert_fusion.3), channel_id=1, source_target_pairs={{0,2},{1,3},{2,0},{3,1},{4,6},{5,7},{6,4},{7,5},{8,10},{9,11},{10,... | collective-permute-start | bytes 393224 | tf_op jit(solution)/shard_map/ppermute | solution.py:448
  63.6 8.3 %collective-permute-start.15 = (bf16[128,512]{1,0:T(8,128)(2,1)S(1)}, bf16[128,512]{1,0:T(8,128)(2,1)S(1)}, u32[]{:S(2)}, u32[]{:S(2)}) collective-permute-start(bf16[128,512]{1,0:T(8,128)(2,1)S(1)} %add_convert_fusion.2), channel_id=1, source_target_pairs={{0,4},{1,5},{2,6},{3,7},{4,0},{5,1},{6,2},{7,3},{8,12},{9,13},{10,... | collective-permute-start | bytes 393224 | tf_op jit(solution)/shard_map/ppermute | solution.py:448
  64.4 7.5 %collective-permute-start.17 = (bf16[128,512]{1,0:T(8,128)(2,1)S(1)}, bf16[128,512]{1,0:T(8,128)(2,1)S(1)}, u32[]{:S(2)}, u32[]{:S(2)}) collective-permute-start(bf16[128,512]{1,0:T(8,128)(2,1)S(1)} %add_convert_fusion.1), channel_id=1, source_target_pairs={{0,6},{1,7},{2,4},{3,5},{4,2},{5,3},{6,0},{7,1},{8,14},{9,15},{10,... | collective-permute-start | bytes 393224 | tf_op jit(solution)/shard_map/ppermute | solution.py:448

commit v5 on v4

--- a/solution.py
+++ b/solution.py
@@ -471,7 +471,8 @@
         left[half, peer] = left[half, peer].astype(jnp.float32) + other.astype(jnp.float32)
     total = left[0, 0]
     for half, peer in places[1:]:
-        total = total + swap(left[half, peer].astype(jnp.bfloat16), half, peer).astype(jnp.float32)
+        other = swap(left[half, peer].astype(jnp.bfloat16), half, peer)
+        total = total + other.astype(jnp.float32)
     return total
 
 
@@ -563,14 +564,16 @@
     received = exchange(packed.reshape(experts * capacity, col_width))
     (held_down,) = load(received, (w_exp_down,))
     chunks, held_down = gather_chunks(received, tp_count, held_down)
-    down_terms = expert_step(
-        index,
-        chunks,
-        gain_ffn.reshape(1, model_width),
-        *held_experts,
-        held_down,
-        tp_count,
-    )
+    down_terms = []
+    for half in range(2):
+        down_terms += expert_step(
+            index,
+            chunks[half * tp_count : (half + 1) * tp_count],
+            gain_ffn.reshape(1, model_width),
+            *held_experts,
+            held_down,
+            tp_count,
+        )
     half_share = sum_chunks(down_terms, tp_count).astype(jnp.bfloat16)
     half_share, matrix_new, normal_new = lax.optimization_barrier((half_share, matrix_new, normal_new))
     returned = exchange(half_share).astype(jnp.float32).reshape(experts, capacity, col_width)

time: 82.7 us -> 82.2 us (level)
  waiting for transfers between devices: 12.4 us -> 10.4 us
    ppermute x18, waiting for transfers between devices: 8.24 us -> 6.24 us  [swap(): lax.ppermute(value, ('ep', 'tp'), [(i, i ^ away) for i in range(ep_count...]
    pallas_call x1 -> x2, Pallas kernels: 2.75 us -> 3.63 us  [expert_step(): pl.pallas_call(functools.partial(expert_kernel, peers=peers, halves=len(c...]
  transfers between devices with their start and end apart: 19 -> 19, of which waited for: 11 -> 6; matrix products, arithmetic and copies ran while one was open for 0% -> 0% of each run, Pallas kernels for 15% -> 20%
where the time goes in v5:
time: 82.2 us; the launch traced here: 81.7 us
  blocking collectives  29.3 us (36%)
  Pallas kernels  20.9 us (25%)
  starting transfers between devices  19.1 us (23%)
  waiting for transfers between devices  10.4 us (13%)
  other arithmetic  1.04 us (1%)
  between operations  0.96 us (1%)
    all_to_all x3, blocking collectives, exchange(): lax.all_to_all(rows, 'ep', split_axis=0, concat_axis=0, tiled=True, axis_...  29.3 us
    ppermute x18, starting transfers between devices, swap(): lax.ppermute(value, ('ep', 'tp'), [(i, i ^ away) for i in range(ep_count...  14 us
    ppermute x18, waiting for transfers between devices, swap(): lax.ppermute(value, ('ep', 'tp'), [(i, i ^ away) for i in range(ep_count...  6.24 us
    pallas_call x3, Pallas kernels, load(): pl.pallas_call(functools.partial(load_kernel, count=len(arrays), narrowed...  5.81 us
    all_to_all x1, starting transfers between devices, exchange(): lax.all_to_all(rows, 'ep', split_axis=0, concat_axis=0, tiled=True, axis_...  5.09 us
    pallas_call x1, Pallas kernels, update_states(): pl.pallas_call(update_kernel, in_specs=[pl.BlockSpec()] * 2 + [anywhere],...  4.26 us
    all_to_all x1, waiting for transfers between devices, exchange(): lax.all_to_all(rows, 'ep', split_axis=0, concat_axis=0, tiled=True, axis_...  4.12 us
    pallas_call x2, Pallas kernels, expert_step(): pl.pallas_call(functools.partial(expert_kernel, peers=peers, halves=len(c...  3.63 us
  transfers between devices with their start and end apart: 19, of which 6 were waited for; matrix products, arithmetic and copies ran while one was open for 0% of the time, Pallas kernels for 20%

profile of v5, /device:TPU:0, one launch (start us, length us, event | category | flops | bytes accessed | tf_op | source)
XLA Modules:
  0.0 81.7 jit_solution(11936555695148105126)
XLA Ops:
  0.6 0.0 copy-start
  0.6 0.0 copy-start.4
  0.7 1.2 %pack.1.own_ref = bf16[4,256,256]{2,1,0:T(8,128)(2,1)S(1)} custom-call(bf16[256,256]{1,0:T(8,128)(2,1)} %refs_0_.4, bf16[256,256]{1,0:T(8,128)(2,1)} %refs_1_.2, bf16[256,256]{1,0:T(8,128)(2,1)} %refs_2_.1, bf16[256,256]{1,0:T(8,128)(2,1)} %refs_3_.1), custom_call_target="tpu_custom_call" | custom-call | tf_op jit(solution)/shard_map/pack/pallas_call | solution.py:77
  1.9 3.1 %collective-permute-start = (bf16[4,256,256]{2,1,0:T(8,128)(2,1)S(1)}, bf16[4,256,256]{2,1,0:T(8,128)(2,1)S(1)}, u32[]{:S(2)}, u32[]{:S(2)}) collective-permute-start(bf16[4,256,256]{2,1,0:T(8,128)(2,1)S(1)} %pack.1.own_ref), channel_id=1, source_target_pairs={{0,4},{1,5},{2,6},{3,7},{4,0},{5,1},{6,2},{7,3},{8,12},{9,13},{10,... | collective-permute-start | bytes 1572872 | tf_op jit(solution)/shard_map/ppermute | solution.py:448
  5.0 1.0 %split_features.1 = bf16[128,512]{1,0:T(8,128)(2,1)S(1)} custom-call(bf16[32,2048]{1,0:T(8,128)(2,1)} %rows_ref.1, bf16[2048]{0:T(1024)(128)(2,1)} %gain_ref.1), custom_call_target="tpu_custom_call" | custom-call | tf_op jit(solution)/shard_map/split_features/pallas_call | solution.py:111
  6.0 0.1 pad_add_fusion.index_ref
  6.1 10.6 %all_to_all.37 = bf16[4,32,512]{2,1,0:T(8,128)(2,1)S(1)} all-to-all(bf16[4,32,512]{2,1,0:T(8,128)(2,1)S(1)} %bitcast.18), channel_id=1, replica_groups={{0,8,16,24},{4,12,20,28},{1,9,17,25},{5,13,21,29},{2,10,18,26},{6,14,22..., dimensions={0} | all-to-all | bytes 262144 | tf_op jit(solution)/shard_map/all_to_all | solution.py:519
  16.7 0.2 collective-permute-done.other_ref
  16.9 1.6 %project.1._ = bf16[128,1024]{1,0:T(8,128)(2,1)} custom-call(s32[2]{0:T(128)S(1)} %pad_add_fusion.index_ref, bf16[128,512]{1,0:T(8,128)(2,1)S(1)} %bitcast.19, bf16[4,256,256]{2,1,0:T(8,128)(2,1)S(1)} %pack.1.own_ref, bf16[4,256,256]{2,1,0:T(8,128)(2,1)S(1)} %collective-permute-done.other_ref), custom_call_target="tpu_custom_call" | custom-call | tf_op jit(solution)/shard_map/project/pallas_call | solution.py:202
  18.5 5.1 %all-to-all-start.1 = ((bf16[4,32,1024]{2,1,0:T(8,128)(2,1)}), bf16[4,32,1024]{2,1,0:T(8,128)(2,1)S(1)}, u32[]{:S(2)}, u32[]{:S(2)}) async-start(bf16[4,32,1024]{2,1,0:T(8,128)(2,1)} %bitcast.4), calls=%async_computation.1 | async-start | bytes 524288 | tf_op jit(solution)/shard_map/all_to_all | solution.py:519
  23.6 0.0 copy-done.9
  23.6 0.0 copy-done
  23.6 0.0 copy-done.4
  23.7 0.0 copy-done.2
  23.7 0.0 copy-done.3
  23.7 0.0 copy-done.6
  23.7 1.4 %gates.1 = (f32[32,1]{1,0:T(8,128)S(1)}, f32[2,32]{1,0:T(2,128)S(1)}, f32[2,32]{1,0:T(2,128)S(1)}, f32[2,32]{1,0:T(2,128)}) custom-call(s32[2]{0:T(128)S(1)} %pad_add_fusion.index_ref, bf16[128,1024]{1,0:T(8,128)(2,1)} %project.1._, bf16[32,2048]{1,0:T(8,128)(2,1)S(1)} %copy-done, bf16[2048]{0:T(1024)(128)(2,1)S(1)} %copy-done.4, ...), custom_call_target="tpu_custom_call" | custom-call | flops 4194304 | tf_op jit(solution)/shard_map/gates/pallas_call | solution.py:167
  25.2 2.5 %load.3.matrix_ref = bf16[32,2,128,128]{3,2,1,0:T(8,128)(2,1)S(1)} custom-call(bf16[128,1024]{1,0:T(8,128)(2,1)} %project.1._, f32[32,2,128,128]{3,2,1,0:T(8,128)} %matrix_hbm.1), custom_call_target="tpu_custom_call" | custom-call | flops 4194304 | tf_op jit(solution)/shard_map/load/pallas_call | solution.py:43
  27.6 4.1 %all-to-all-done.1.arrived_ref = bf16[4,32,1024]{2,1,0:T(8,128)(2,1)S(1)} async-done(((bf16[4,32,1024]{2,1,0:T(8,128)(2,1)}), bf16[4,32,1024]{2,1,0:T(8,128)(2,1)S(1)}, u32[]{:S(2)}, u32[]{:S(2)}) %all-to-all-start.1) | async-done | bytes 262176 | tf_op jit(solution)/shard_map/all_to_all | solution.py:519
  31.8 2.1 %cell_step.1 = (bf16[32,512]{1,0:T(8,128)(2,1)S(1)}, bf16[32,512]{1,0:T(8,128)(2,1)S(1)}, bf16[32,512]{1,0:T(8,128)(2,1)S(1)}, bf16[32,512]{1,0:T(8,128)(2,1)S(1)}, f32[4,64,128]{2,1,0:T(8,128)S(1)}) custom-call(s32[2]{0:T(128)S(1)} %pad_add_fusion.index_ref, bf16[4,32,1024]{2,1,0:T(8,128)(2,1)S(1)} %all-to-all-done.1.arrived_ref, ...), custom_call_target="tpu_custom_call" | custom-call | tf_op jit(solution)/shard_map/cell_step/pallas_call | solution.py:289
  33.8 0.1 collective-permute-start.3
  33.9 1.6 %collective-permute-start.2 = (bf16[32,512]{1,0:T(8,128)(2,1)S(1)}, bf16[32,512]{1,0:T(8,128)(2,1)S(1)}, u32[]{:S(2)}, u32[]{:S(2)}) collective-permute-start(bf16[32,512]{1,0:T(8,128)(2,1)S(1)} %get-tuple-element.47), channel_id=1, source_target_pairs={{0,2},{1,3},{2,0},{3,1},{4,6},{5,7},{6,4},{7,5},{8,10},{9,11},{10,... | collective-permute-start | bytes 98312 | tf_op jit(solution)/shard_map/ppermute | solution.py:448
  35.5 0.3 collective-permute-start.1
  35.8 1.9 %load.4 = (bf16[1,2048,384]{2,1,0:T(8,128)(2,1)S(1)}, bf16[1,2048,384]{2,1,0:T(8,128)(2,1)S(1)}) custom-call(f32[4,64,128]{2,1,0:T(8,128)S(1)} %get-tuple-element.49._.rows_ref, bf16[1,2048,384]{2,1,0:T(8,128)(2,1)} %refs_0_.6, bf16[1,2048,384]{2,1,0:T(8,128)(2,1)} %refs_1_.3), custom_call_target="tpu_custom_call" | custom-call | flops 4194304 | tf_op jit(solution)/shard_map/load/pallas_call | solution.py:43
  37.7 0.0 collective-permute-done.3
  37.7 0.2 collective-permute-done.2
  38.0 0.0 collective-permute-done.1
  38.0 8.9 %all_to_all.38 = bf16[4,32,512]{2,1,0:T(8,128)(2,1)S(1)} all-to-all(bf16[4,32,512]{2,1,0:T(8,128)(2,1)S(1)} %broadcast_in_dim.22), channel_id=1, replica_groups={{0,8,16,24},{4,12,20,28},{1,9,17,25},{5,13,21,29},{2,10,18,26},{6,14,22..., dimensions={0} | all-to-all | bytes 262144 | tf_op jit(solution)/shard_map/all_to_all | solution.py:519
  46.9 1.5 %collective-permute-start.10 = (bf16[128,512]{1,0:T(8,128)(2,1)S(1)}, bf16[128,512]{1,0:T(8,128)(2,1)S(1)}, u32[]{:S(2)}, u32[]{:S(2)}) collective-permute-start(bf16[128,512]{1,0:T(8,128)(2,1)S(1)} %bitcast.12), channel_id=1, source_target_pairs={{0,4},{1,5},{2,6},{3,7},{4,0},{5,1},{6,2},{7,3},{8,12},{9,13},{10,... | collective-permute-start | bytes 393224 | tf_op jit(solution)/shard_map/ppermute | solution.py:448
  48.4 1.1 %collective-permute-start.12 = (bf16[128,512]{1,0:T(8,128)(2,1)S(1)}, bf16[128,512]{1,0:T(8,128)(2,1)S(1)}, u32[]{:S(2)}, u32[]{:S(2)}) collective-permute-start(bf16[128,512]{1,0:T(8,128)(2,1)S(1)} %bitcast.13), channel_id=1, source_target_pairs={{0,6},{1,7},{2,4},{3,5},{4,2},{5,3},{6,0},{7,1},{8,14},{9,15},{10,... | collective-permute-start | bytes 393224 | tf_op jit(solution)/shard_map/ppermute | solution.py:448
  49.5 0.9 %collective-permute-start.5 = (bf16[128,512]{1,0:T(8,128)(2,1)S(1)}, bf16[128,512]{1,0:T(8,128)(2,1)S(1)}, u32[]{:S(2)}, u32[]{:S(2)}) collective-permute-start(bf16[128,512]{1,0:T(8,128)(2,1)S(1)} %bitcast.14), channel_id=1, source_target_pairs={{0,2},{1,3},{2,0},{3,1},{4,6},{5,7},{6,4},{7,5},{8,10},{9,11},{10,... | collective-permute-start | bytes 393224 | tf_op jit(solution)/shard_map/ppermute | solution.py:448
  50.4 3.0 %collective-permute-done.10.refs_0_ = bf16[128,512]{1,0:T(8,128)(2,1)S(1)} collective-permute-done((bf16[128,512]{1,0:T(8,128)(2,1)S(1)}, bf16[128,512]{1,0:T(8,128)(2,1)S(1)}, u32[]{:S(2)}, u32[]{:S(2)}) %collective-permute-start.10) | collective-permute-done | bytes 131104 | tf_op jit(solution)/shard_map/ppermute | solution.py:448
  53.4 0.0 collective-permute-start.11
  53.4 1.1 %collective-permute-done.12.refs_2_ = bf16[128,512]{1,0:T(8,128)(2,1)S(1)} collective-permute-done((bf16[128,512]{1,0:T(8,128)(2,1)S(1)}, bf16[128,512]{1,0:T(8,128)(2,1)S(1)}, u32[]{:S(2)}, u32[]{:S(2)}) %collective-permute-start.12) | collective-permute-done | bytes 131104 | tf_op jit(solution)/shard_map/ppermute | solution.py:448
  54.5 0.0 collective-permute-start.13
  54.6 0.6 collective-permute-start.4
  55.1 1.4 %load.5.refs_7_ = bf16[1,384,2048]{2,1,0:T(8,128)(2,1)S(1)} custom-call(bf16[128,512]{1,0:T(8,128)(2,1)S(1)} %bitcast.16, bf16[1,384,2048]{2,1,0:T(8,128)(2,1)} %refs_0_.7), custom_call_target="tpu_custom_call" | custom-call | flops 4194304 | tf_op jit(solution)/shard_map/load/pallas_call | solution.py:43
  56.6 0.0 collective-permute-done.5.refs_2_
  56.6 0.1 collective-permute-start.6
  56.6 0.0 collective-permute-done.11.refs_1_
  56.7 0.0 collective-permute-done.13.refs_3_
  56.7 1.8 %expert_step.3 = (bf16[128,512]{1,0:T(8,128)(2,1)S(1)}, bf16[128,512]{1,0:T(8,128)(2,1)S(1)}, bf16[128,512]{1,0:T(8,128)(2,1)S(1)}, bf16[128,512]{1,0:T(8,128)(2,1)S(1)}) custom-call(s32[2]{0:T(128)S(1)} %pad_add_fusion.index_ref, bf16[128,512]{1,0:T(8,128)(2,1)S(1)} %collective-permute-done.10.refs_0_, ...), custom_call_target="tpu_custom_call" | custom-call | tf_op jit(solution)/shard_map/expert_step/pallas_call | solution.py:413
  58.5 0.5 collective-permute-start.16
  59.0 0.1 collective-permute-start.14
  59.1 0.0 collective-permute-done.4.refs_1_
  59.1 0.0 collective-permute-done.6.refs_3_
  59.1 1.8 %expert_step.2 = (bf16[128,512]{1,0:T(8,128)(2,1)S(1)}, bf16[128,512]{1,0:T(8,128)(2,1)S(1)}, bf16[128,512]{1,0:T(8,128)(2,1)S(1)}, bf16[128,512]{1,0:T(8,128)(2,1)S(1)}) custom-call(s32[2]{0:T(128)S(1)} %pad_add_fusion.index_ref, bf16[128,512]{1,0:T(8,128)(2,1)S(1)} %bitcast.17, bf16[128,512]{1,0:T(8,128)(2,1)S(1)} %collective-permute-done.4.refs_1_, ...), custom_call_target="tpu_custom_call" | custom-call | tf_op jit(solution)/shard_map/expert_step/pallas_call | solution.py:413
  60.9 0.5 collective-permute-start.8
  61.4 0.1 collective-permute-start.7
  61.5 0.0 collective-permute-done.16
  61.6 1.6 %collective-permute-start.17 = (bf16[128,512]{1,0:T(8,128)(2,1)S(1)}, bf16[128,512]{1,0:T(8,128)(2,1)S(1)}, u32[]{:S(2)}, u32[]{:S(2)}) collective-permute-start(bf16[128,512]{1,0:T(8,128)(2,1)S(1)} %add_convert_fusion.1), channel_id=1, source_target_pairs={{0,6},{1,7},{2,4},{3,5},{4,2},{5,3},{6,0},{7,1},{8,14},{9,15},{10,... | collective-permute-start | bytes 393224 | tf_op jit(solution)/shard_map/ppermute | solution.py:448
  63.1 0.0 collective-permute-done.14
  63.2 0.9 %collective-permute-start.15 = (bf16[128,512]{1,0:T(8,128)(2,1)S(1)}, bf16[128,512]{1,0:T(8,128)(2,1)S(1)}, u32[]{:S(2)}, u32[]{:S(2)}) collective-permute-start(bf16[128,512]{1,0:T(8,128)(2,1)S(1)} %add_convert_fusion.2), channel_id=1, source_target_pairs={{0,4},{1,5},{2,6},{3,7},{4,0},{5,1},{6,2},{7,3},{8,12},{9,13},{10,... | collective-permute-start | bytes 393224 | tf_op jit(solution)/shard_map/ppermute | solution.py:448
  64.1 0.0 collective-permute-done.8
  64.1 1.2 %collective-permute-start.9 = (bf16[128,512]{1,0:T(8,128)(2,1)S(1)}, bf16[128,512]{1,0:T(8,128)(2,1)S(1)}, u32[]{:S(2)}, u32[]{:S(2)}) collective-permute-start(bf16[128,512]{1,0:T(8,128)(2,1)S(1)} %add_convert_fusion.3), channel_id=1, source_target_pairs={{0,2},{1,3},{2,0},{3,1},{4,6},{5,7},{6,4},{7,5},{8,10},{9,11},{10,... | collective-permute-start | bytes 393224 | tf_op jit(solution)/shard_map/ppermute | solution.py:448
  65.3 4.3 %update_states.1 = (f32[32,2,128]{2,1,0:T(2,128)}, f32[32,2,128,128]{3,2,1,0:T(8,128)}) custom-call(f32[4,64,128]{2,1,0:T(8,128)S(1)} %get-tuple-element.49._.rows_ref, f32[32,2,128]{2,1,0:T(2,128)S(1)} %copy-done.1, f32[32,2,128,128]{3,2,1,0:T(8,128)} %matrix_hbm.1), custom_call_target="tpu_custom_call" | custom-call | flops 8388608 | tf_op jit(solution)/shard_map/update_states/pallas_call | solution.py:359
  69.6 0.0 collective-permute-done.7
  69.6 0.0 collective-permute-done.17
  69.6 1.5 %collective-permute-done.15 = bf16[128,512]{1,0:T(8,128)(2,1)S(1)} collective-permute-done((bf16[128,512]{1,0:T(8,128)(2,1)S(1)}, bf16[128,512]{1,0:T(8,128)(2,1)S(1)}, u32[]{:S(2)}, u32[]{:S(2)}) %collective-permute-start.15) | collective-permute-done | bytes 131104 | tf_op jit(solution)/shard_map/ppermute | solution.py:448
  71.2 0.0 collective-permute-done.9
  71.2 0.1 add_convert_fusion
  71.3 9.8 %all_to_all.39 = bf16[4,32,512]{2,1,0:T(8,128)(2,1)S(1)} all-to-all(bf16[4,32,512]{2,1,0:T(8,128)(2,1)S(1)} %bitcast.23), channel_id=1, replica_groups={{0,8,16,24},{4,12,20,28},{1,9,17,25},{5,13,21,29},{2,10,18,26},{6,14,22..., dimensions={0} | all-to-all | bytes 262144 | tf_op jit(solution)/shard_map/all_to_all | solution.py:519
  81.0 0.1 multiply_reduce_fusion
  81.1 0.6 add_convert_fusion.4
  (23 shorter events, 0.2 us)
Async XLA Ops:
  0.6 23.0 %copy-start = (bf16[32,2048]{1,0:T(8,128)(2,1)S(1)}, bf16[32,2048]{1,0:T(8,128)(2,1)}, u32[]{:S(2)}) copy-start(bf16[32,2048]{1,0:T(8,128)(2,1)} %rows_ref.1) | copy-start | bytes 393220
  0.6 23.0 %copy-start.4 = (bf16[2048]{0:T(1024)(128)(2,1)S(1)}, bf16[2048]{0:T(1024)(128)(2,1)}, u32[]{:S(2)}) copy-start(bf16[2048]{0:T(1024)(128)(2,1)} %gain_ref.1) | copy-start | bytes 12292
  0.7 22.9 %copy-start.9 = (f32[32,2]{0,1:T(2,128)S(1)}, f32[32,2]{0,1:T(2,128)}, u32[]{:S(2)}) copy-start(f32[32,2]{0,1:T(2,128)} %param.36) | copy-start | bytes 772
  0.7 22.9 %copy-start.10 = (s32[32,2]{0,1:T(2,128)S(1)}, s32[32,2]{0,1:T(2,128)}, u32[]{:S(2)}) copy-start(s32[32,2]{0,1:T(2,128)} %param.35) | copy-start | bytes 772
  0.7 23.0 %copy-start.2 = (bf16[2048,8]{0,1:T(8,128)(2,1)S(1)}, bf16[2048,8]{0,1:T(8,128)(2,1)}, u32[]{:S(2)}) copy-start(bf16[2048,8]{0,1:T(8,128)(2,1)} %param.27) | copy-start | bytes 98308
  0.7 23.0 %copy-start.3 = (bf16[2048,8]{0,1:T(8,128)(2,1)S(1)}, bf16[2048,8]{0,1:T(8,128)(2,1)}, u32[]{:S(2)}) copy-start(bf16[2048,8]{0,1:T(8,128)(2,1)} %param.28) | copy-start | bytes 98308
  0.7 23.0 %copy-start.6 = (f32[8]{0:T(128)S(1)}, f32[8]{0:T(128)}, u32[]{:S(2)}) copy-start(f32[8]{0:T(128)} %bias_in_ref.1) | copy-start | bytes 100
  0.7 23.0 %copy-start.7 = (f32[8]{0:T(128)S(1)}, f32[8]{0:T(128)}, u32[]{:S(2)}) copy-start(f32[8]{0:T(128)} %bias_forget_ref.1) | copy-start | bytes 100
  0.7 23.0 %copy-start.5 = (f32[32,2]{0,1:T(2,128)S(1)}, f32[32,2]{0,1:T(2,128)}, u32[]{:S(2)}) copy-start(f32[32,2]{0,1:T(2,128)} %param.34) | copy-start | bytes 772
  1.9 15.0 %collective-permute-start = (bf16[4,256,256]{2,1,0:T(8,128)(2,1)S(1)}, bf16[4,256,256]{2,1,0:T(8,128)(2,1)S(1)}, u32[]{:S(2)}, u32[]{:S(2)}) collective-permute-start(bf16[4,256,256]{2,1,0:T(8,128)(2,1)S(1)} %pack.1.own_ref), channel_id=1, source_target_pairs={{0,4},{1,5},{2,6},{3,7},{4,0},{5,1},{6,2},{7,3},{8,12},{9,13},{10,... | collective-permute-start | bytes 1572872 | tf_op jit(solution)/shard_map/ppermute | solution.py:448
  18.5 13.3 %all-to-all-start.1 = ((bf16[4,32,1024]{2,1,0:T(8,128)(2,1)}), bf16[4,32,1024]{2,1,0:T(8,128)(2,1)S(1)}, u32[]{:S(2)}, u32[]{:S(2)}) async-start(bf16[4,32,1024]{2,1,0:T(8,128)(2,1)} %bitcast.4), calls=%async_computation.1 | async-start | bytes 524288 | tf_op jit(solution)/shard_map/all_to_all | solution.py:519
  25.1 6.6 %copy-start.1 = (f32[32,2,128]{2,1,0:T(2,128)S(1)}, f32[32,2,128]{2,1,0:T(2,128)}, u32[]{:S(2)}) copy-start(f32[32,2,128]{2,1,0:T(2,128)} %normal_ref.3) | copy-start | bytes 98308
  33.8 3.9 %collective-permute-start.3 = (bf16[32,512]{1,0:T(8,128)(2,1)S(1)}, bf16[32,512]{1,0:T(8,128)(2,1)S(1)}, u32[]{:S(2)}, u32[]{:S(2)}) collective-permute-start(bf16[32,512]{1,0:T(8,128)(2,1)S(1)} %get-tuple-element.48), channel_id=1, source_target_pairs={{0,3},{1,2},{2,1},{3,0},{4,7},{5,6},{6,5},{7,4},{8,11},{9,10},{10,... | collective-permute-start | bytes 98312 | tf_op jit(solution)/shard_map/ppermute | solution.py:448
  33.9 4.0 %collective-permute-start.2 = (bf16[32,512]{1,0:T(8,128)(2,1)S(1)}, bf16[32,512]{1,0:T(8,128)(2,1)S(1)}, u32[]{:S(2)}, u32[]{:S(2)}) collective-permute-start(bf16[32,512]{1,0:T(8,128)(2,1)S(1)} %get-tuple-element.47), channel_id=1, source_target_pairs={{0,2},{1,3},{2,0},{3,1},{4,6},{5,7},{6,4},{7,5},{8,10},{9,11},{10,... | collective-permute-start | bytes 98312 | tf_op jit(solution)/shard_map/ppermute | solution.py:448
  35.5 2.5 %collective-permute-start.1 = (bf16[32,512]{1,0:T(8,128)(2,1)S(1)}, bf16[32,512]{1,0:T(8,128)(2,1)S(1)}, u32[]{:S(2)}, u32[]{:S(2)}) collective-permute-start(bf16[32,512]{1,0:T(8,128)(2,1)S(1)} %get-tuple-element.46), channel_id=1, source_target_pairs={{0,1},{1,0},{2,3},{3,2},{4,5},{5,4},{6,7},{7,6},{8,9},{9,8},{10,11... | collective-permute-start | bytes 98312 | tf_op jit(solution)/shard_map/ppermute | solution.py:448
  35.8 18.8 %copy-start.8 = (bf16[2048]{0:T(1024)(128)(2,1)S(1)}, bf16[2048]{0:T(1024)(128)(2,1)}, u32[]{:S(2)}) copy-start(bf16[2048]{0:T(1024)(128)(2,1)} %param.22) | copy-start | bytes 12292
  46.9 6.5 %collective-permute-start.10 = (bf16[128,512]{1,0:T(8,128)(2,1)S(1)}, bf16[128,512]{1,0:T(8,128)(2,1)S(1)}, u32[]{:S(2)}, u32[]{:S(2)}) collective-permute-start(bf16[128,512]{1,0:T(8,128)(2,1)S(1)} %bitcast.12), channel_id=1, source_target_pairs={{0,4},{1,5},{2,6},{3,7},{4,0},{5,1},{6,2},{7,3},{8,12},{9,13},{10,... | collective-permute-start | bytes 393224 | tf_op jit(solution)/shard_map/ppermute | solution.py:448
  48.4 6.1 %collective-permute-start.12 = (bf16[128,512]{1,0:T(8,128)(2,1)S(1)}, bf16[128,512]{1,0:T(8,128)(2,1)S(1)}, u32[]{:S(2)}, u32[]{:S(2)}) collective-permute-start(bf16[128,512]{1,0:T(8,128)(2,1)S(1)} %bitcast.13), channel_id=1, source_target_pairs={{0,6},{1,7},{2,4},{3,5},{4,2},{5,3},{6,0},{7,1},{8,14},{9,15},{10,... | collective-permute-start | bytes 393224 | tf_op jit(solution)/shard_map/ppermute | solution.py:448
  49.5 7.0 %collective-permute-start.5 = (bf16[128,512]{1,0:T(8,128)(2,1)S(1)}, bf16[128,512]{1,0:T(8,128)(2,1)S(1)}, u32[]{:S(2)}, u32[]{:S(2)}) collective-permute-start(bf16[128,512]{1,0:T(8,128)(2,1)S(1)} %bitcast.14), channel_id=1, source_target_pairs={{0,2},{1,3},{2,0},{3,1},{4,6},{5,7},{6,4},{7,5},{8,10},{9,11},{10,... | collective-permute-start | bytes 393224 | tf_op jit(solution)/shard_map/ppermute | solution.py:448
  53.4 3.2 %collective-permute-start.11 = (bf16[128,512]{1,0:T(8,128)(2,1)S(1)}, bf16[128,512]{1,0:T(8,128)(2,1)S(1)}, u32[]{:S(2)}, u32[]{:S(2)}) collective-permute-start(bf16[128,512]{1,0:T(8,128)(2,1)S(1)} %collective-permute-done.10.refs_0_), channel_id=1, source_target_pairs={{0,1},{1,0},{2,3},{3,2},{4,5},{5,4},{6,7},{7,6},{8,9},{9,8},{10,11... | collective-permute-start | bytes 393224 | tf_op jit(solution)/shard_map/ppermute | solution.py:448
  54.5 2.1 %collective-permute-start.13 = (bf16[128,512]{1,0:T(8,128)(2,1)S(1)}, bf16[128,512]{1,0:T(8,128)(2,1)S(1)}, u32[]{:S(2)}, u32[]{:S(2)}) collective-permute-start(bf16[128,512]{1,0:T(8,128)(2,1)S(1)} %collective-permute-done.12.refs_2_), channel_id=1, source_target_pairs={{0,1},{1,0},{2,3},{3,2},{4,5},{5,4},{6,7},{7,6},{8,9},{9,8},{10,11... | collective-permute-start | bytes 393224 | tf_op jit(solution)/shard_map/ppermute | solution.py:448
  54.6 4.6 %collective-permute-start.4 = (bf16[128,512]{1,0:T(8,128)(2,1)S(1)}, bf16[128,512]{1,0:T(8,128)(2,1)S(1)}, u32[]{:S(2)}, u32[]{:S(2)}) collective-permute-start(bf16[128,512]{1,0:T(8,128)(2,1)S(1)} %bitcast.15), channel_id=1, source_target_pairs={{0,1},{1,0},{2,3},{3,2},{4,5},{5,4},{6,7},{7,6},{8,9},{9,8},{10,11... | collective-permute-start | bytes 393224 | tf_op jit(solution)/shard_map/ppermute | solution.py:448
  56.6 2.6 %collective-permute-start.6 = (bf16[128,512]{1,0:T(8,128)(2,1)S(1)}, bf16[128,512]{1,0:T(8,128)(2,1)S(1)}, u32[]{:S(2)}, u32[]{:S(2)}) collective-permute-start(bf16[128,512]{1,0:T(8,128)(2,1)S(1)} %collective-permute-done.5.refs_2_), channel_id=1, source_target_pairs={{0,1},{1,0},{2,3},{3,2},{4,5},{5,4},{6,7},{7,6},{8,9},{9,8},{10,11... | collective-permute-start | bytes 393224 | tf_op jit(solution)/shard_map/ppermute | solution.py:448
  58.5 3.0 %collective-permute-start.16 = (bf16[128,512]{1,0:T(8,128)(2,1)S(1)}, bf16[128,512]{1,0:T(8,128)(2,1)S(1)}, u32[]{:S(2)}, u32[]{:S(2)}) collective-permute-start(bf16[128,512]{1,0:T(8,128)(2,1)S(1)} %get-tuple-element.64), channel_id=1, source_target_pairs={{0,1},{1,0},{2,3},{3,2},{4,5},{5,4},{6,7},{7,6},{8,9},{9,8},{10,11... | collective-permute-start | bytes 393224 | tf_op jit(solution)/shard_map/ppermute | solution.py:448
  59.0 4.1 %collective-permute-start.14 = (bf16[128,512]{1,0:T(8,128)(2,1)S(1)}, bf16[128,512]{1,0:T(8,128)(2,1)S(1)}, u32[]{:S(2)}, u32[]{:S(2)}) collective-permute-start(bf16[128,512]{1,0:T(8,128)(2,1)S(1)} %get-tuple-element.62), channel_id=1, source_target_pairs={{0,1},{1,0},{2,3},{3,2},{4,5},{5,4},{6,7},{7,6},{8,9},{9,8},{10,11... | collective-permute-start | bytes 393224 | tf_op jit(solution)/shard_map/ppermute | solution.py:448
  60.9 3.2 %collective-permute-start.8 = (bf16[128,512]{1,0:T(8,128)(2,1)S(1)}, bf16[128,512]{1,0:T(8,128)(2,1)S(1)}, u32[]{:S(2)}, u32[]{:S(2)}) collective-permute-start(bf16[128,512]{1,0:T(8,128)(2,1)S(1)} %get-tuple-element.60), channel_id=1, source_target_pairs={{0,1},{1,0},{2,3},{3,2},{4,5},{5,4},{6,7},{7,6},{8,9},{9,8},{10,11... | collective-permute-start | bytes 393224 | tf_op jit(solution)/shard_map/ppermute | solution.py:448
  61.4 8.2 %collective-permute-start.7 = (bf16[128,512]{1,0:T(8,128)(2,1)S(1)}, bf16[128,512]{1,0:T(8,128)(2,1)S(1)}, u32[]{:S(2)}, u32[]{:S(2)}) collective-permute-start(bf16[128,512]{1,0:T(8,128)(2,1)S(1)} %get-tuple-element.58), channel_id=1, source_target_pairs={{0,1},{1,0},{2,3},{3,2},{4,5},{5,4},{6,7},{7,6},{8,9},{9,8},{10,11... | collective-permute-start | bytes 393224 | tf_op jit(solution)/shard_map/ppermute | solution.py:448
  61.6 8.0 %collective-permute-start.17 = (bf16[128,512]{1,0:T(8,128)(2,1)S(1)}, bf16[128,512]{1,0:T(8,128)(2,1)S(1)}, u32[]{:S(2)}, u32[]{:S(2)}) collective-permute-start(bf16[128,512]{1,0:T(8,128)(2,1)S(1)} %add_convert_fusion.1), channel_id=1, source_target_pairs={{0,6},{1,7},{2,4},{3,5},{4,2},{5,3},{6,0},{7,1},{8,14},{9,15},{10,... | collective-permute-start | bytes 393224 | tf_op jit(solution)/shard_map/ppermute | solution.py:448
  63.2 8.0 %collective-permute-start.15 = (bf16[128,512]{1,0:T(8,128)(2,1)S(1)}, bf16[128,512]{1,0:T(8,128)(2,1)S(1)}, u32[]{:S(2)}, u32[]{:S(2)}) collective-permute-start(bf16[128,512]{1,0:T(8,128)(2,1)S(1)} %add_convert_fusion.2), channel_id=1, source_target_pairs={{0,4},{1,5},{2,6},{3,7},{4,0},{5,1},{6,2},{7,3},{8,12},{9,13},{10,... | collective-permute-start | bytes 393224 | tf_op jit(solution)/shard_map/ppermute | solution.py:448
  64.1 7.0 %collective-permute-start.9 = (bf16[128,512]{1,0:T(8,128)(2,1)S(1)}, bf16[128,512]{1,0:T(8,128)(2,1)S(1)}, u32[]{:S(2)}, u32[]{:S(2)}) collective-permute-start(bf16[128,512]{1,0:T(8,128)(2,1)S(1)} %add_convert_fusion.3), channel_id=1, source_target_pairs={{0,2},{1,3},{2,0},{3,1},{4,6},{5,7},{6,4},{7,5},{8,10},{9,11},{10,... | collective-permute-start | bytes 393224 | tf_op jit(solution)/shard_map/ppermute | solution.py:448
